TPU v7x, 256 devices: a whole 4x4x8 slice. The times are simulated.
256 devices in a mesh: fs: 64 (over z, x, core), tp: 4 (over y).
Axes of the slice: x: 4, y: 4, z: 8, core: 2. Of those that a mesh axis runs over, the one named last changes fastest.
Arguments:
- saved_input: bfloat16 [16384, 4096], P('fs'), may hold values from -16 to 16
- query_cotangent: bfloat16 [16384, 2048], P('fs', 'tp'), may hold values from -6 to 6
- layer_cotangent: bfloat16 [16384, 4096], P('fs'), may hold values from -16 to 16
- mixed_heads: bfloat16 [16384, 2048], P('fs', 'tp'), may hold values from -6 to 6
- query_basis: bfloat16 [4096, 256], P('fs'), may hold values from -0.25 to 0.25
- output_basis: bfloat16 [4096, 256], P('fs'), may hold values from -0.25 to 0.25
- query_master: float32 [4096, 2048], P('fs', 'tp'), may hold values from -3 to 3
- output_master: float32 [4096, 2048], P('fs', 'tp'), may hold values from -3 to 3
- query_first: float32 [256, 2048], P('fs', 'tp'), may hold values from -6 to 6
- query_second: float32 [256, 2048], P('fs', 'tp'), may hold values from 0.25 to 4
- output_first: float32 [256, 2048], P('fs', 'tp'), may hold values from -6 to 6
- output_second: float32 [256, 2048], P('fs', 'tp'), may hold values from 0.25 to 4
Outputs:
- query_weight: float32 [4096, 2048], P('fs', 'tp')
- output_weight: float32 [4096, 2048], P('fs', 'tp')
- query_step: float32 [4096, 2048], P('fs', 'tp')
- output_step: float32 [4096, 2048], P('fs', 'tp')
- query_first_new: float32 [256, 2048], P('fs', 'tp')
- query_second_new: float32 [256, 2048], P('fs', 'tp')
- output_first_new: float32 [256, 2048], P('fs', 'tp')
- output_second_new: float32 [256, 2048], P('fs', 'tp')
- query_copy: bfloat16 [4096, 2048], P(None, 'tp')
- output_copy: bfloat16 [4096, 2048], P(None, 'tp')
All inputs are finite; a program needn't handle non-finite values.
Results may differ from a plain program's by a relative error of at most 0.0028.
Values may be sent and summed in bfloat16 or wider, within the bound.
No kernel may reach another device: no remote copies, remote signals or barrier semaphores. Data moves between devices by JAX's collectives and lax.ppermute only.
A program may use at most 64 MiB of HBM per device.

v0:
```python
import jax
import jax.numpy as jnp
from jax import lax
from jax.experimental import pallas as pl
from jax.experimental.pallas import tpu as pltpu
from jax.sharding import Mesh
from jax.sharding import PartitionSpec as P

D = 4096
QW = 2048
RANK = 256
FS = ("fs_0", "fs_1", "fs_2")
CHIPS = ("fs_0", "fs_1")

beta_one = 0.8
beta_two = 0.9
rate = 0.1

f32 = jnp.float32
bf16 = jnp.bfloat16
f16 = jnp.float16

REACH = 85.0
SHRINK = 2.0**-10

MOMENTS_AT = 192
TOPS_AT = 224
BLOCK_ROWS = 232
GROUP = 4


VMEM = pl.BlockSpec(memory_space=pltpu.VMEM)
SMEM = pl.BlockSpec(memory_space=pltpu.SMEM)


def high_and_low(values):
    high = values.astype(bf16).astype(f32)
    return high, values - high


def pack_kernel(at, qb, ob, qm, om, q1, q2, o1, o2, qc, oc, block, send, cot):
    tp = at[1]
    picked = []
    for basis in (qb, ob):
        full = basis[...].astype(f32)
        part = full[:, :64]
        for t in range(1, 4):
            part = jnp.where(tp == t, full[:, 64 * t : 64 * t + 64], part)
        picked.append(part)
    send[...] = jnp.broadcast_to(jnp.concatenate(picked, axis=1).astype(bf16)[None], send.shape)
    tops = []
    for side, master in ((0, qm), (1, om)):
        values = master[...]
        top = jnp.max(jnp.abs(values), axis=(0, 1), keepdims=True) * 1.01 + 1e-30
        top = top.astype(bf16).astype(f32)
        block[64 * side : 64 * side + 64, :] = jnp.exp(values * (REACH / top)).astype(bf16)
        tops.append(top)
    block[128:192, :256] = qb[...]
    block[128:192, 256:] = ob[...]
    for side, (first, second) in enumerate(((q1, q2), (o1, o2))):
        first_high, first_low = high_and_low(first[...])
        second_high, second_low = high_and_low(second[...])
        at_row = MOMENTS_AT + 16 * side
        block[at_row : at_row + 16, :] = jnp.concatenate(
            [first_high, second_high, first_low, second_low], axis=0
        ).astype(bf16)
    row = lax.broadcasted_iota(jnp.int32, (8, 512), 0)
    block[TOPS_AT:, :] = jnp.where(row == 0, tops[0], tops[1]).astype(bf16)
    cot[:, :512] = qc[...]
    cot[:, 512:] = oc[...]


def project_kernel(at, saved, layer, mine, theirs, c0, c1, c2, c3, keep, give, saved_near, layer_near, sems):
    copies = [
        pltpu.make_async_copy(saved, saved_near, sems.at[0]),
        pltpu.make_async_copy(layer, layer_near, sems.at[1]),
    ]
    for copy in copies:
        copy.start()
    core = at[0]
    own, other = mine[...], theirs[...]
    first = jnp.where(core == 0, own, other)
    second = jnp.where(core == 0, other, own)
    basis = jnp.concatenate([first, second], axis=1).reshape(D, 128)
    for side, source in ((0, saved_near), (1, layer_near)):
        copies[side].wait()
        coords = jnp.dot(source[...], basis, preferred_element_type=f32)[:, 64 * side : 64 * side + 64]
        high, low = high_and_low(coords.T)
        left = jnp.concatenate([high, low], axis=0).astype(bf16)
        for k, cot in enumerate((c0, c1, c2, c3)):
            both = jnp.dot(left, cot[:, 512 * side : 512 * side + 512], preferred_element_type=f32)
            part = (both[:64] + both[64:]) * SHRINK
            lower, upper = part[:32], part[32:]
            kept = jnp.where(core == 0, lower, upper)
            given = jnp.where(core == 0, upper, lower)
            for j in range(4):
                slot = (side * 4 + k) * 4 + j
                keep[:, slot, :] = kept[:, 128 * j : 128 * j + 128]
                give[:, slot, :] = given[:, 128 * j : 128 * j + 128]


def spread_kernel(at, row, out):
    tp = at[1]
    values = row[...] * (1.0 / SHRINK)
    squares = jnp.broadcast_to(jnp.sum(values * values, axis=(0, 1), keepdims=True), (1, 128))
    for t in range(4):
        k = (tp + 4 - t) % 4
        pieces = []
        for side in range(2):
            for j in range(4):
                pieces.append(row[pl.ds((side * 4 + k) * 4 + j, 1), :] * (1.0 / SHRINK))
        line = jnp.concatenate(pieces + [squares], axis=1)

        def put(chip, carry):
            out[chip * 4 + t] = line
            return carry

        lax.fori_loop(0, 32, put, 0, unroll=True)


def update_kernel(at, mine, theirs, q1, q2, o1, o2, low, factor, qf, qs, of, os):
    core, fs = at[0], at[2]
    total = jnp.sum(mine[:, :, 1024:], axis=0) + jnp.sum(theirs[:, :, 1024:], axis=0)
    scale = lax.rsqrt(1.0 + total * (1.0 / (2.0 * RANK * QW)))
    factor[...] = jnp.broadcast_to(scale, (8, 128))
    is_first = core == 0
    for t in range(4):
        for chip in range(32):
            own, other = mine[chip * 4 + t, :, :1024], theirs[chip * 4 + t, :, :1024]
            low[64 * t + chip : 64 * t + chip + 1, :] = jnp.where(is_first, own, other)
            low[64 * t + 32 + chip : 64 * t + 33 + chip, :] = jnp.where(is_first, other, own)
    near = low[pl.ds(pl.multiple_of(fs // 2 * 8, 8), 8), :]
    own_rows = jnp.where(fs % 2 == 0, near[:4], near[4:]) * scale[:, :1]
    for side, first, second, first_new, second_new in ((0, q1, q2, qf, qs), (1, o1, o2, of, os)):
        scaled = own_rows[:, 512 * side : 512 * side + 512]
        first_new[...] = beta_one * first[...] + (1.0 - beta_one) * scaled
        second_new[...] = beta_two * second[...] + (1.0 - beta_two) * scaled * scaled


def finish_kernel(factor, low, qb, ob, qm, om, moments, block, tops, qw, ow, qs, os, qc, oc, direction):
    @pl.when(pl.program_id(0) == 0)
    def _():
        scale = factor[0:1, 0:1]

        def rows(i, carry):
            held = moments[pl.ds(4 * i, 4)].astype(f32)
            lows = low[pl.ds(16 * i, 16), :] * scale
            for side in range(2):
                sums = [held[j, 16 * side : 16 * side + 8] + held[j, 16 * side + 8 : 16 * side + 16] for j in range(4)]
                first = jnp.concatenate([s[:4] for s in sums], axis=0)
                second = jnp.concatenate([s[4:] for s in sums], axis=0)
                scaled = lows[:, 512 * side : 512 * side + 512]
                first = beta_one * first + (1.0 - beta_one) * scaled
                second = beta_two * second + (1.0 - beta_two) * scaled * scaled
                direction[pl.ds(16 * i, 16), 512 * side : 512 * side + 512] = (first / jnp.sqrt(second)).astype(bf16)
            return carry

        lax.fori_loop(0, 16, rows, 0)
        for side, basis, master, weight, step in ((0, qb, qm, qw, qs), (1, ob, om, ow, os)):
            moved = jnp.dot(basis[...], direction[:, 512 * side : 512 * side + 512], preferred_element_type=f32)
            step[...] = moved
            weight[...] = master[...] - rate * moved

    for side, copy in ((0, qc), (1, oc)):
        basis = block[:, 128:192, 256 * side : 256 * side + 256].reshape(GROUP * 64, 256)
        moved = jnp.dot(basis, direction[:, 512 * side : 512 * side + 512], preferred_element_type=f32)
        codes = block[:, 64 * side : 64 * side + 64, :].astype(f32)
        unit = tops[:, side : side + 1, :].astype(f32) * (1.0 / REACH)
        master = (jnp.log(codes) * unit).reshape(GROUP * 64, 512)
        copy[...] = (master - rate * moved).astype(bf16)


def near(*arrays):
    return [pltpu.with_memory_space_constraint(a, pltpu.VMEM) for a in arrays]


def far(*arrays):
    return [pltpu.with_memory_space_constraint(a, pltpu.HBM) for a in arrays]


def swapped(values):
    return lax.ppermute(values, "fs_2", [(0, 1), (1, 0)])


def per_device(
    saved_input,
    query_cotangent,
    layer_cotangent,
    mixed_heads,
    query_basis,
    output_basis,
    query_master,
    output_master,
    query_first,
    query_second,
    output_first,
    output_second,
):
    shape = jax.ShapeDtypeStruct
    at = jnp.stack([lax.axis_index("fs_2"), lax.axis_index("tp"), lax.axis_index(FS)]).astype(jnp.int32)
    moments = (query_first, query_second, output_first, output_second)
    block, send, cot = pl.pallas_call(
        pack_kernel,
        in_specs=[SMEM] + [VMEM] * 10,
        out_specs=[VMEM] * 3,
        out_shape=[shape((BLOCK_ROWS, 512), bf16), shape((32, 64, 128), bf16), shape((256, 1024), bf16)],
        compiler_params=pltpu.CompilerParams(vmem_limit_bytes=24 * 2**20),
        name="pack",
    )(
        at,
        *far(query_basis, output_basis, query_master, output_master, *moments),
        *far(query_cotangent, mixed_heads),
    )
    gathered = lax.all_gather(block, FS, axis=0, tiled=False)
    cots = [cot] + [lax.ppermute(cot, "tp", [(i, (i + k) % 4) for i in range(4)]) for k in (2, 1, 3)]
    cots = [cots[i] for i in (0, 2, 1, 3)]
    mine = lax.all_to_all(send, CHIPS, 0, 0, tiled=True)
    theirs = swapped(mine)
    keep, give = pl.pallas_call(
        project_kernel,
        in_specs=[SMEM] + [pl.BlockSpec(memory_space=pl.ANY)] * 2 + [VMEM] * 6,
        out_specs=[VMEM] * 2,
        scratch_shapes=[pltpu.VMEM((256, D), bf16)] * 2 + [pltpu.SemaphoreType.DMA((2,))],
        out_shape=[pltpu.VMEM((32, 32, 128), f32)] * 2,
        compiler_params=pltpu.CompilerParams(vmem_limit_bytes=20 * 2**20),
        name="project",
    )(at, *far(saved_input, layer_cotangent), *near(mine, theirs, *cots))
    pair = (keep + swapped(give.astype(f16)).astype(f32)).astype(f16)
    arrived = lax.all_to_all(pair, CHIPS, 0, 0, tiled=True)
    row = jnp.sum(arrived.astype(f32), axis=0)
    out = pl.pallas_call(
        spread_kernel,
        in_specs=[SMEM, VMEM],
        out_specs=VMEM,
        out_shape=pltpu.VMEM((128, 1, 1152), f32),
        compiler_params=pltpu.CompilerParams(vmem_limit_bytes=16 * 2**20),
        name="spread",
    )(at, *near(row))
    mine = lax.all_to_all(out, (*CHIPS, "tp"), 0, 0, tiled=True)
    theirs = swapped(mine)
    low, factor, qf, qs, of, osec = pl.pallas_call(
        update_kernel,
        in_specs=[SMEM] + [VMEM] * 6,
        out_specs=[VMEM] * 6,
        out_shape=[shape((RANK, 1024), f32), shape((8, 128), f32)] + [shape((4, 512), f32)] * 4,
        compiler_params=pltpu.CompilerParams(vmem_limit_bytes=16 * 2**20),
        name="update",
    )(at, *near(mine, theirs), *far(*moments))

    def whole(*dims):
        return pl.BlockSpec(dims, lambda i: (0,) * len(dims))

    local = whole(64, 512)
    query_weight, output_weight, query_step, output_step, query_copy, output_copy = pl.pallas_call(
        finish_kernel,
        grid=(64 // GROUP,),
        in_specs=[
            whole(8, 128),
            whole(RANK, 1024),
            whole(64, 256),
            whole(64, 256),
            local,
            local,
            pl.BlockSpec((64, 32, 512), lambda i: (0, MOMENTS_AT // 32, 0)),
            pl.BlockSpec((GROUP, 192, 512), lambda i: (i, 0, 0)),
            pl.BlockSpec((GROUP, 8, 512), lambda i: (i, TOPS_AT // 8, 0)),
        ],
        out_specs=[local] * 4 + [pl.BlockSpec((GROUP * 64, 512), lambda i: (i, 0))] * 2,
        out_shape=[shape((64, 512), f32)] * 4 + [shape((D, 512), bf16)] * 2,
        scratch_shapes=[pltpu.VMEM((RANK, 1024), bf16)],
        compiler_params=pltpu.CompilerParams(dimension_semantics=("arbitrary",)),
        name="finish",
    )(factor, low, query_basis, output_basis, query_master, output_master, gathered, gathered, gathered)
    return (
        query_weight,
        output_weight,
        query_step,
        output_step,
        qf,
        qs,
        of,
        osec,
        query_copy,
        output_copy,
    )


def solution(mesh):
    torus = Mesh(mesh.devices.reshape(8, 4, 2, mesh.shape["tp"]), (*FS, "tp"))
    return jax.shard_map(
        per_device,
        mesh=torus,
        in_specs=(
            P(FS, None),
            P(FS, "tp"),
            P(FS, None),
            P(FS, "tp"),
            P(FS, None),
            P(FS, None),
            *[P(FS, "tp")] * 6,
        ),
        out_specs=(*[P(FS, "tp")] * 8, P(None, "tp"), P(None, "tp")),
        check_vma=False,
    )
```

profile of v0, /device:TPU:1, one launch (start us, length us, event | category | flops | bytes accessed | tf_op | source)
XLA Modules:
  0.0 151.9 jit_solution(2571521889402365798)
XLA Ops:
  7.2 0.0 all-gather.3.cloned.1.call-start
  7.2 0.1 pad_add_fusion.at
  7.3 2.4 %pack.1 = (bf16[232,512]{1,0:T(8,128)(2,1)}, bf16[32,64,128]{2,1,0:T(8,128)(2,1)}, bf16[256,1024]{1,0:T(8,128)(2,1)S(1)}) custom-call(s32[3]{0:T(128)S(1)} %pad_add_fusion.at, bf16[64,256]{1,0:T(8,128)(2,1)} %qb.3, bf16[64,256]{1,0:T(8,128)(2,1)} %ob.3, f32[64,512]{1,0:T(8,128)} %qm.3, f32[64,512]{1,0:T(8,128)} %om.3, f32[4,512]{1,0:T(4,128)} %q1.3, ...), custom_call_target="tpu_custom_call" | custom-call | tf_op jit(solution)/shard_map/pack/pallas_call | solution.py:202
  9.8 11.9 %all-to-all-start = ((bf16[32,64,128]{2,1,0:T(8,128)(2,1)}), bf16[32,64,128]{2,1,0:T(8,128)(2,1)S(1)}, u32[]{:S(2)}, u32[]{:S(2)}) async-start(bf16[32,64,128]{2,1,0:T(8,128)(2,1)} %get-tuple-element.27), calls=%async_computation | async-start | bytes 1048576 | tf_op jit(solution)/shard_map/all_to_all | solution.py:217
  21.6 2.8 %collective-permute-start.3 = (bf16[256,1024]{1,0:T(8,128)(2,1)S(1)}, bf16[256,1024]{1,0:T(8,128)(2,1)S(1)}, u32[]{:S(2)}, u32[]{:S(2)}) collective-permute-start(bf16[256,1024]{1,0:T(8,128)(2,1)S(1)} %get-tuple-element.28.c0), channel_id=1, source_target_pairs={{0,3},{1,0},{2,1},{3,2},{4,7},{5,4},{6,5},{7,6},{8,11},{9,8},{10,9... | collective-permute-start | bytes 1572872 | tf_op jit(solution)/shard_map/ppermute | solution.py:215
  24.4 0.3 collective-permute-start.2
  24.8 0.7 collective-permute-start.1
  25.5 13.3 %all-to-all-done.mine = bf16[32,64,128]{2,1,0:T(8,128)(2,1)S(1)} async-done(((bf16[32,64,128]{2,1,0:T(8,128)(2,1)}), bf16[32,64,128]{2,1,0:T(8,128)(2,1)S(1)}, u32[]{:S(2)}, u32[]{:S(2)}) %all-to-all-start) | async-done | bytes 524320 | tf_op jit(solution)/shard_map/all_to_all | solution.py:217
  38.8 3.9 %collective-permute-start = (bf16[32,64,128]{2,1,0:T(8,128)(2,1)S(1)}, bf16[32,64,128]{2,1,0:T(8,128)(2,1)S(1)}, u32[]{:S(2)}, u32[]{:S(2)}) collective-permute-start(bf16[32,64,128]{2,1,0:T(8,128)(2,1)S(1)} %all-to-all-done.mine), channel_id=1, source_target_pairs={{0,4},{4,0},{1,5},{5,1},{2,6},{6,2},{3,7},{7,3},{8,12},{12,8},{9,1... | collective-permute-start | bytes 1572872 | tf_op jit(solution)/shard_map/ppermute | solution.py:182
  42.7 8.3 %collective-permute-done.1.c1 = bf16[256,1024]{1,0:T(8,128)(2,1)S(1)} collective-permute-done((bf16[256,1024]{1,0:T(8,128)(2,1)S(1)}, bf16[256,1024]{1,0:T(8,128)(2,1)S(1)}, u32[]{:S(2)}, u32[]{:S(2)}) %collective-permute-start.1) | collective-permute-done | bytes 524320 | tf_op jit(solution)/shard_map/ppermute | solution.py:215
  51.0 5.0 %project.1 = (f32[32,32,128]{2,1,0:T(8,128)S(1)}, f32[32,32,128]{2,1,0:T(8,128)S(1)}) custom-call(s32[3]{0:T(128)S(1)} %pad_add_fusion.at, bf16[256,4096]{1,0:T(8,128)(2,1)} %saved.1, bf16[256,4096]{1,0:T(8,128)(2,1)} %layer.1, bf16[32,64,128]{2,1,0:T(8,128)(2,1)S(1)} %all-to-all-done.mine, bf16[32,64,128]{2,1,0:T(8,128)(2,1)S(1)} %collective-permute-done.theirs, ...), custom_call_target="tpu_custom_call" | custom-call | tf_op jit(solution)/shard_map/project/pallas_call | solution.py:219
  56.0 0.6 collective-permute-start.4
  56.6 1.2 collective-permute-done.4
  57.8 0.1 add_convert_fusion
  57.9 23.8 %all_to_all.15 = f16[32,32,128]{2,1,0:T(8,128)(2,1)S(1)} all-to-all(f16[32,32,128]{2,1,0:T(8,128)(2,1)S(1)} %add_convert_fusion), channel_id=1, replica_groups=mesh['fs_0'=8,'fs_1'=4,'fs_2'=2,'tp'=4] {'fs_0','fs_1'}, dimensions={0} | all-to-all | bytes 524288 | tf_op jit(solution)/shard_map/all_to_all | solution.py:229
  81.8 0.7 spread.1
  82.5 32.7 %all_to_all.16.mine = f32[128,1,1152]{2,1,0:T(1,128)S(1)} all-to-all(f32[128,1,1152]{2,1,0:T(1,128)S(1)} %spread.1), channel_id=1, replica_groups=mesh['fs_0'=8,'fs_1'=4,'fs_2'=2,'tp'=4] {'fs_0','fs_1','tp'}, dimensions={0} | all-to-all | bytes 1179648 | tf_op jit(solution)/shard_map/all_to_all | solution.py:239
  115.2 3.2 %collective-permute-start.5 = (f32[128,1,1152]{2,1,0:T(1,128)S(1)}, f32[128,1,1152]{2,1,0:T(1,128)S(1)}, u32[]{:S(2)}, u32[]{:S(2)}) collective-permute-start(f32[128,1,1152]{2,1,0:T(1,128)S(1)} %all_to_all.16.mine), channel_id=1, source_target_pairs={{0,4},{4,0},{1,5},{5,1},{2,6},{6,2},{3,7},{7,3},{8,12},{12,8},{9,1... | collective-permute-start | bytes 1769480 | tf_op jit(solution)/shard_map/ppermute | solution.py:182
  118.4 1.8 %collective-permute-done.5.theirs = f32[128,1,1152]{2,1,0:T(1,128)S(1)} collective-permute-done((f32[128,1,1152]{2,1,0:T(1,128)S(1)}, f32[128,1,1152]{2,1,0:T(1,128)S(1)}, u32[]{:S(2)}, u32[]{:S(2)}) %collective-permute-start.5) | collective-permute-done | bytes 589856 | tf_op jit(solution)/shard_map/ppermute | solution.py:182
  120.2 1.7 %update.1 = (f32[256,1024]{1,0:T(8,128)S(1)}, f32[8,128]{1,0:T(8,128)S(1)}, f32[4,512]{1,0:T(4,128)}, f32[4,512]{1,0:T(4,128)}, f32[4,512]{1,0:T(4,128)}, /*index=5*/f32[4,512]{1,0:T(4,128)}) custom-call(s32[3]{0:T(128)S(1)} %pad_add_fusion.at, f32[128,1,1152]{2,1,0:T(1,128)S(1)} %all_to_all.16.mine, f32[128,1,1152]{2,1,0:T(1,128)S(1)} %collective-permute-done.5.theirs, ...), custom_call_target="tpu_custom_call" | custom-call | tf_op jit(solution)/shard_map/update/pallas_call | solution.py:241
  121.9 1.0 copy-done
  122.9 0.6 copy-done.1
  123.5 4.5 %all-gather.3.cloned.1.call-done = bf16[14848,512]{1,0:T(8,128)(2,1)} async-done(((bf16[232,512]{1,0:T(8,128)(2,1)}), bf16[14848,512]{1,0:T(8,128)(2,1)}) %all-gather.3.cloned.1.call-update) | async-done | bytes 15204368 | tf_op jit(solution)/shard_map/all_gather | solution.py:214
  128.0 17.1 %finish.1 = (f32[64,512]{1,0:T(8,128)}, f32[64,512]{1,0:T(8,128)}, f32[64,512]{1,0:T(8,128)}, f32[64,512]{1,0:T(8,128)}, bf16[4096,512]{1,0:T(8,128)(2,1)}, /*index=5*/bf16[4096,512]{1,0:T(8,128)(2,1)}) custom-call(f32[8,128]{1,0:T(8,128)} %copy-done.1, f32[256,1024]{1,0:T(8,128)} %copy-done, bf16[64,256]{1,0:T(8,128)(2,1)} %qb.3, bf16[64,256]{1,0:T(8,128)(2,1)} %ob.3, ...), custom_call_target="tpu_custom_call" | custom-call | tf_op jit(solution)/shard_map/finish/pallas_call | solution.py:254
  (8 shorter events, 0.1 us)
Async XLA Ops:
  7.2 120.8 %all-gather.3.cloned.1.call-start = ((), (), s32[]{:S(2)}) async-start(), calls=%async_computation.3 | async-start | bytes 15441920 | tf_op jit(solution)/shard_map/all_gather | solution.py:214
  9.8 29.0 %all-to-all-start = ((bf16[32,64,128]{2,1,0:T(8,128)(2,1)}), bf16[32,64,128]{2,1,0:T(8,128)(2,1)S(1)}, u32[]{:S(2)}, u32[]{:S(2)}) async-start(bf16[32,64,128]{2,1,0:T(8,128)(2,1)} %get-tuple-element.27), calls=%async_computation | async-start | bytes 1048576 | tf_op jit(solution)/shard_map/all_to_all | solution.py:217
  21.6 21.1 %collective-permute-start.3 = (bf16[256,1024]{1,0:T(8,128)(2,1)S(1)}, bf16[256,1024]{1,0:T(8,128)(2,1)S(1)}, u32[]{:S(2)}, u32[]{:S(2)}) collective-permute-start(bf16[256,1024]{1,0:T(8,128)(2,1)S(1)} %get-tuple-element.28.c0), channel_id=1, source_target_pairs={{0,3},{1,0},{2,1},{3,2},{4,7},{5,4},{6,5},{7,6},{8,11},{9,8},{10,9... | collective-permute-start | bytes 1572872 | tf_op jit(solution)/shard_map/ppermute | solution.py:215
  24.4 18.3 %collective-permute-start.2 = (bf16[256,1024]{1,0:T(8,128)(2,1)S(1)}, bf16[256,1024]{1,0:T(8,128)(2,1)S(1)}, u32[]{:S(2)}, u32[]{:S(2)}) collective-permute-start(bf16[256,1024]{1,0:T(8,128)(2,1)S(1)} %get-tuple-element.28.c0), channel_id=1, source_target_pairs={{0,2},{1,3},{2,0},{3,1},{4,6},{5,7},{6,4},{7,5},{8,10},{9,11},{10,... | collective-permute-start | bytes 1572872 | tf_op jit(solution)/shard_map/ppermute | solution.py:215
  24.8 26.2 %collective-permute-start.1 = (bf16[256,1024]{1,0:T(8,128)(2,1)S(1)}, bf16[256,1024]{1,0:T(8,128)(2,1)S(1)}, u32[]{:S(2)}, u32[]{:S(2)}) collective-permute-start(bf16[256,1024]{1,0:T(8,128)(2,1)S(1)} %get-tuple-element.28.c0), channel_id=1, source_target_pairs={{0,1},{1,2},{2,3},{3,0},{4,5},{5,6},{6,7},{7,4},{8,9},{9,10},{10,1... | collective-permute-start | bytes 1572872 | tf_op jit(solution)/shard_map/ppermute | solution.py:215
  38.8 12.3 %collective-permute-start = (bf16[32,64,128]{2,1,0:T(8,128)(2,1)S(1)}, bf16[32,64,128]{2,1,0:T(8,128)(2,1)S(1)}, u32[]{:S(2)}, u32[]{:S(2)}) collective-permute-start(bf16[32,64,128]{2,1,0:T(8,128)(2,1)S(1)} %all-to-all-done.mine), channel_id=1, source_target_pairs={{0,4},{4,0},{1,5},{5,1},{2,6},{6,2},{3,7},{7,3},{8,12},{12,8},{9,1... | collective-permute-start | bytes 1572872 | tf_op jit(solution)/shard_map/ppermute | solution.py:182
  56.0 1.7 %collective-permute-start.4 = (f16[32,32,128]{2,1,0:T(8,128)(2,1)S(1)}, f16[32,32,128]{2,1,0:T(8,128)(2,1)S(1)}, u32[]{:S(2)}, u32[]{:S(2)}) collective-permute-start(f16[32,32,128]{2,1,0:T(8,128)(2,1)S(1)} %convert_element_type.12), channel_id=1, source_target_pairs={{0,4},{4,0},{1,5},{5,1},{2,6},{6,2},{3,7},{7,3},{8,12},{12,8},{9,1... | collective-permute-start | bytes 786440 | tf_op jit(solution)/shard_map/ppermute | solution.py:182
  115.2 5.0 %collective-permute-start.5 = (f32[128,1,1152]{2,1,0:T(1,128)S(1)}, f32[128,1,1152]{2,1,0:T(1,128)S(1)}, u32[]{:S(2)}, u32[]{:S(2)}) collective-permute-start(f32[128,1,1152]{2,1,0:T(1,128)S(1)} %all_to_all.16.mine), channel_id=1, source_target_pairs={{0,4},{4,0},{1,5},{5,1},{2,6},{6,2},{3,7},{7,3},{8,12},{12,8},{9,1... | collective-permute-start | bytes 1769480 | tf_op jit(solution)/shard_map/ppermute | solution.py:182
  121.9 1.0 copy-start
  122.9 0.6 copy-start.1
Sparse Core Ops, SparseCore 0:
  11.3 116.6 all-gather.2
where the time goes:
time: 153 us; the launch traced here: 152 us
  blocking collectives  56.6 us (37%)
  waiting for transfers between devices  29.1 us (19%)
  Pallas kernels  26.9 us (18%)
  starting transfers between devices  23.4 us (15%)
  between operations  14.1 us (9%)
  local copies, waits for them, and re-layouts  1.6 us (1%)
    all_to_all x1, blocking collectives, per_device(): mine = lax.all_to_all(out, (*CHIPS, 'tp'), 0, 0, tiled=True)  32.7 us
    all_to_all x1, blocking collectives, per_device(): arrived = lax.all_to_all(pair, CHIPS, 0, 0, tiled=True)  23.8 us
    pallas_call x1, Pallas kernels, per_device(): pl.pallas_call(finish_kernel, grid=(64 // GROUP,), in_specs=[whole(8, 128...  17.1 us
    all_to_all x1, waiting for transfers between devices, per_device(): mine = lax.all_to_all(send, CHIPS, 0, 0, tiled=True)  13.3 us
    all_to_all x1, starting transfers between devices, per_device(): mine = lax.all_to_all(send, CHIPS, 0, 0, tiled=True)  11.9 us
    ppermute x3, waiting for transfers between devices, per_device(): lax.ppermute(cot, 'tp', [(i, (i + k) % 4) for i in range(4)])  8.34 us
    ppermute x3, starting transfers between devices, swapped(): return lax.ppermute(values, 'fs_2', [(0, 1), (1, 0)])  7.66 us
    pallas_call x1, Pallas kernels, per_device(): pl.pallas_call(project_kernel, in_specs=[SMEM] + [pl.BlockSpec(memory_spa...  4.95 us
  transfers between devices with their start and end apart: 8, of which 5 were waited for; matrix products, arithmetic and copies ran while one was open for 0% of the time, Pallas kernels for 5%

commit v1 on v0

--- a/solution.py
+++ b/solution.py
@@ -23,10 +23,10 @@
 REACH = 85.0
 SHRINK = 2.0**-10
 
-MOMENTS_AT = 192
-TOPS_AT = 224
-BLOCK_ROWS = 232
-GROUP = 4
+MOMENTS_AT = 128
+TOPS_AT = 160
+BLOCK_ROWS = 168
+GROUP = 8
 
 
 VMEM = pl.BlockSpec(memory_space=pltpu.VMEM)
@@ -55,8 +55,6 @@
         top = top.astype(bf16).astype(f32)
         block[64 * side : 64 * side + 64, :] = jnp.exp(values * (REACH / top)).astype(bf16)
         tops.append(top)
-    block[128:192, :256] = qb[...]
-    block[128:192, 256:] = ob[...]
     for side, (first, second) in enumerate(((q1, q2), (o1, o2))):
         first_high, first_low = high_and_low(first[...])
         second_high, second_low = high_and_low(second[...])
@@ -137,7 +135,12 @@
         second_new[...] = beta_two * second[...] + (1.0 - beta_two) * scaled * scaled
 
 
-def finish_kernel(factor, low, qb, ob, qm, om, moments, block, tops, qw, ow, qs, os, qc, oc, direction):
+def finish_kernel(
+    at, factor, low, qb, ob, qm, om, moments, block, tops, *rest
+):
+    quarters, (qw, ow, qs, os, qc, oc, natural, direction) = rest[:8], rest[8:]
+    core, tp = at[0], at[1]
+
     @pl.when(pl.program_id(0) == 0)
     def _():
         scale = factor[0:1, 0:1]
@@ -152,17 +155,26 @@
                 scaled = lows[:, 512 * side : 512 * side + 512]
                 first = beta_one * first + (1.0 - beta_one) * scaled
                 second = beta_two * second + (1.0 - beta_two) * scaled * scaled
-                direction[pl.ds(16 * i, 16), 512 * side : 512 * side + 512] = (first / jnp.sqrt(second)).astype(bf16)
+                natural[pl.ds(16 * i, 16), 512 * side : 512 * side + 512] = (first / jnp.sqrt(second)).astype(bf16)
             return carry
 
         lax.fori_loop(0, 16, rows, 0)
+        for k in range(4):
+            start = pl.multiple_of((tp + 4 - k) % 4 * 64, 64)
+            direction[64 * k : 64 * k + 64, :] = natural[pl.ds(start, 64), :]
         for side, basis, master, weight, step in ((0, qb, qm, qw, qs), (1, ob, om, ow, os)):
-            moved = jnp.dot(basis[...], direction[:, 512 * side : 512 * side + 512], preferred_element_type=f32)
+            moved = jnp.dot(basis[...], natural[:, 512 * side : 512 * side + 512], preferred_element_type=f32)
             step[...] = moved
             weight[...] = master[...] - rate * moved
 
+    bases = []
+    for k in range(4):
+        own, other = quarters[2 * k][...], quarters[2 * k + 1][...]
+        first = jnp.where(core == 0, own, other)
+        second = jnp.where(core == 0, other, own)
+        bases.append(jnp.concatenate([first, second], axis=1).reshape(GROUP * 64, 128))
     for side, copy in ((0, qc), (1, oc)):
-        basis = block[:, 128:192, 256 * side : 256 * side + 256].reshape(GROUP * 64, 256)
+        basis = jnp.concatenate([b[:, 64 * side : 64 * side + 64] for b in bases], axis=1)
         moved = jnp.dot(basis, direction[:, 512 * side : 512 * side + 512], preferred_element_type=f32)
         codes = block[:, 64 * side : 64 * side + 64, :].astype(f32)
         unit = tops[:, side : side + 1, :].astype(f32) * (1.0 / REACH)
@@ -216,6 +228,10 @@
     cots = [cots[i] for i in (0, 2, 1, 3)]
     mine = lax.all_to_all(send, CHIPS, 0, 0, tiled=True)
     theirs = swapped(mine)
+    quarters = [mine, theirs]
+    for k in range(1, 4):
+        quarter = lax.ppermute(mine, "tp", [(i, (i + k) % 4) for i in range(4)])
+        quarters += [quarter, swapped(quarter)]
     keep, give = pl.pallas_call(
         project_kernel,
         in_specs=[SMEM] + [pl.BlockSpec(memory_space=pl.ANY)] * 2 + [VMEM] * 6,
@@ -255,6 +271,7 @@
         finish_kernel,
         grid=(64 // GROUP,),
         in_specs=[
+            SMEM,
             whole(8, 128),
             whole(RANK, 1024),
             whole(64, 256),
@@ -262,15 +279,20 @@
             local,
             local,
             pl.BlockSpec((64, 32, 512), lambda i: (0, MOMENTS_AT // 32, 0)),
-            pl.BlockSpec((GROUP, 192, 512), lambda i: (i, 0, 0)),
+            pl.BlockSpec((GROUP, 128, 512), lambda i: (i, 0, 0)),
             pl.BlockSpec((GROUP, 8, 512), lambda i: (i, TOPS_AT // 8, 0)),
+            *[pl.BlockSpec((GROUP // 2, 64, 128), lambda i: (i, 0, 0))] * 8,
         ],
         out_specs=[local] * 4 + [pl.BlockSpec((GROUP * 64, 512), lambda i: (i, 0))] * 2,
         out_shape=[shape((64, 512), f32)] * 4 + [shape((D, 512), bf16)] * 2,
-        scratch_shapes=[pltpu.VMEM((RANK, 1024), bf16)],
-        compiler_params=pltpu.CompilerParams(dimension_semantics=("arbitrary",)),
+        scratch_shapes=[pltpu.VMEM((RANK, 1024), bf16)] * 2,
+        compiler_params=pltpu.CompilerParams(dimension_semantics=("arbitrary",), vmem_limit_bytes=40 * 2**20),
         name="finish",
-    )(factor, low, query_basis, output_basis, query_master, output_master, gathered, gathered, gathered)
+    )(
+        at,
+        *near(factor, low),
+        *far(query_basis, output_basis, query_master, output_master, gathered, gathered, gathered, *quarters),
+    )
     return (
         query_weight,
         output_weight,

time: 153 us -> 150 us (0.980)
  blocking collectives: 56.6 us -> 23.9 us
  waiting for transfers between devices: 29.1 us -> 49.6 us
  starting transfers between devices: 23.4 us -> 34.3 us
  Pallas kernels: 26.9 us -> 24 us
  local copies, waits for them, and re-layouts: 1.6 us -> 3.44 us
    all_to_all x1 -> x0, blocking collectives: 32.7 us -> none  [per_device(): mine = lax.all_to_all(out, (*CHIPS, 'tp'), 0, 0, tiled=True)]
    all_to_all x0 -> x1, waiting for transfers between devices: none -> 24 us  [per_device(): mine = lax.all_to_all(out, (*CHIPS, 'tp'), 0, 0, tiled=True)]
    all_to_all x0 -> x1, starting transfers between devices: none -> 6.18 us  [per_device(): mine = lax.all_to_all(out, (*CHIPS, 'tp'), 0, 0, tiled=True)]
    all_gather x1, waiting for transfers between devices: 4.48 us -> 0.01 us  [per_device(): gathered = lax.all_gather(block, FS, axis=0, tiled=False)]
    pallas_call x1, Pallas kernels: 17.1 us -> 13.7 us  [per_device(): pl.pallas_call(finish_kernel, grid=(64 // GROUP,), in_specs=[SMEM, whole(...]
    ppermute x0 -> x3, starting transfers between devices: none -> 2.91 us  [per_device(): quarter = lax.ppermute(mine, 'tp', [(i, (i + k) % 4) for i in range(4)])]
    ppermute x0 -> x3, waiting for transfers between devices: none -> 2.83 us  [per_device(): quarter = lax.ppermute(mine, 'tp', [(i, (i + k) % 4) for i in range(4)])]
    unnamed x4 -> x16, local copies, waits for them, and re-layouts: 1.6 us -> 3.44 us
  transfers between devices with their start and end apart: 8 -> 15, of which waited for: 5 -> 5; matrix products, arithmetic and copies ran while one was open for 0% -> 0% of each run, Pallas kernels for 5% -> 5%
where the time goes in v1:
time: 150 us
  waiting for transfers between devices  49.6 us (33%)
  starting transfers between devices  34.3 us (23%)
  Pallas kernels  24 us (16%)
  blocking collectives  23.9 us (16%)
  between operations  14.1 us (9%)
  local copies, waits for them, and re-layouts  3.44 us (2%)
    all_to_all x1, waiting for transfers between devices, per_device(): mine = lax.all_to_all(out, (*CHIPS, 'tp'), 0, 0, tiled=True)  24 us
    all_to_all x1, blocking collectives, per_device(): arrived = lax.all_to_all(pair, CHIPS, 0, 0, tiled=True)  23.9 us
    pallas_call x1, Pallas kernels, per_device(): pl.pallas_call(finish_kernel, grid=(64 // GROUP,), in_specs=[SMEM, whole(...  13.7 us
    all_to_all x1, waiting for transfers between devices, per_device(): mine = lax.all_to_all(send, CHIPS, 0, 0, tiled=True)  13.1 us
    all_to_all x1, starting transfers between devices, per_device(): mine = lax.all_to_all(send, CHIPS, 0, 0, tiled=True)  11.9 us
    ppermute x6, starting transfers between devices, swapped(): return lax.ppermute(values, 'fs_2', [(0, 1), (1, 0)])  9.48 us
    ppermute x3, waiting for transfers between devices, per_device(): lax.ppermute(cot, 'tp', [(i, (i + k) % 4) for i in range(4)])  8.51 us
    all_to_all x1, starting transfers between devices, per_device(): mine = lax.all_to_all(out, (*CHIPS, 'tp'), 0, 0, tiled=True)  6.18 us
  transfers between devices with their start and end apart: 15, of which 5 were waited for; matrix products, arithmetic and copies ran while one was open for 0% of the time, Pallas kernels for 5%

profile of v1, /device:TPU:1, one launch (start us, length us, event | category | flops | bytes accessed | tf_op | source)
XLA Modules:
  0.0 149.6 jit_solution(8188880465851164191)
XLA Ops:
  7.3 2.4 %pack.1 = (bf16[168,512]{1,0:T(8,128)(2,1)}, bf16[32,64,128]{2,1,0:T(8,128)(2,1)}, bf16[256,1024]{1,0:T(8,128)(2,1)S(1)}) custom-call(s32[3]{0:T(128)S(1)} %pad_add_fusion.at, bf16[64,256]{1,0:T(8,128)(2,1)} %qb.3, bf16[64,256]{1,0:T(8,128)(2,1)} %ob.3, f32[64,512]{1,0:T(8,128)} %qm.3, f32[64,512]{1,0:T(8,128)} %om.3, f32[4,512]{1,0:T(4,128)} %q1.3, ...), custom_call_target="tpu_custom_call" | custom-call | tf_op jit(solution)/shard_map/pack/pallas_call | solution.py:214
  9.7 11.9 %all-to-all-start = ((bf16[32,64,128]{2,1,0:T(8,128)(2,1)}), bf16[32,64,128]{2,1,0:T(8,128)(2,1)S(1)}, u32[]{:S(2)}, u32[]{:S(2)}) async-start(bf16[32,64,128]{2,1,0:T(8,128)(2,1)} %get-tuple-element.27), calls=%async_computation | async-start | bytes 1048576 | tf_op jit(solution)/shard_map/all_to_all | solution.py:229
  21.6 2.8 %collective-permute-start.3 = (bf16[256,1024]{1,0:T(8,128)(2,1)S(1)}, bf16[256,1024]{1,0:T(8,128)(2,1)S(1)}, u32[]{:S(2)}, u32[]{:S(2)}) collective-permute-start(bf16[256,1024]{1,0:T(8,128)(2,1)S(1)} %get-tuple-element.28.c0), channel_id=1, source_target_pairs={{0,3},{1,0},{2,1},{3,2},{4,7},{5,4},{6,5},{7,6},{8,11},{9,8},{10,9... | collective-permute-start | bytes 1572872 | tf_op jit(solution)/shard_map/ppermute | solution.py:227
  24.8 0.7 collective-permute-start.1
  25.5 13.1 %all-to-all-done.mine.rest_0_ = bf16[32,64,128]{2,1,0:T(8,128)(2,1)S(1)} async-done(((bf16[32,64,128]{2,1,0:T(8,128)(2,1)}), bf16[32,64,128]{2,1,0:T(8,128)(2,1)S(1)}, u32[]{:S(2)}, u32[]{:S(2)}) %all-to-all-start) | async-done | bytes 524320 | tf_op jit(solution)/shard_map/all_to_all | solution.py:229
  38.5 4.0 %collective-permute-start = (bf16[32,64,128]{2,1,0:T(8,128)(2,1)S(1)}, bf16[32,64,128]{2,1,0:T(8,128)(2,1)S(1)}, u32[]{:S(2)}, u32[]{:S(2)}) collective-permute-start(bf16[32,64,128]{2,1,0:T(8,128)(2,1)S(1)} %all-to-all-done.mine.rest_0_), channel_id=1, source_target_pairs={{0,4},{4,0},{1,5},{5,1},{2,6},{6,2},{3,7},{7,3},{8,12},{12,8},{9,1... | collective-permute-start | bytes 1572872 | tf_op jit(solution)/shard_map/ppermute | solution.py:194
  42.5 8.5 %collective-permute-done.1.c1 = bf16[256,1024]{1,0:T(8,128)(2,1)S(1)} collective-permute-done((bf16[256,1024]{1,0:T(8,128)(2,1)S(1)}, bf16[256,1024]{1,0:T(8,128)(2,1)S(1)}, u32[]{:S(2)}, u32[]{:S(2)}) %collective-permute-start.1) | collective-permute-done | bytes 524320 | tf_op jit(solution)/shard_map/ppermute | solution.py:227
  51.0 0.8 copy-done.2
  51.8 1.0 copy-done.3
  52.9 4.7 %project.1 = (f32[32,32,128]{2,1,0:T(8,128)S(1)}, f32[32,32,128]{2,1,0:T(8,128)S(1)}) custom-call(s32[3]{0:T(128)S(1)} %pad_add_fusion.at, bf16[256,4096]{1,0:T(8,128)(2,1)} %saved.1, bf16[256,4096]{1,0:T(8,128)(2,1)} %layer.1, bf16[32,64,128]{2,1,0:T(8,128)(2,1)S(1)} %all-to-all-done.mine.rest_0_, ...), custom_call_target="tpu_custom_call" | custom-call | tf_op jit(solution)/shard_map/project/pallas_call | solution.py:235
  57.6 0.6 collective-permute-start.4
  58.2 1.2 collective-permute-done.4
  59.4 23.9 %all_to_all.15 = f16[32,32,128]{2,1,0:T(8,128)(2,1)S(1)} all-to-all(f16[32,32,128]{2,1,0:T(8,128)(2,1)S(1)} %add_convert_fusion), channel_id=1, replica_groups=mesh['fs_0'=8,'fs_1'=4,'fs_2'=2,'tp'=4] {'fs_0','fs_1'}, dimensions={0} | all-to-all | bytes 524288 | tf_op jit(solution)/shard_map/all_to_all | solution.py:245
  83.4 1.5 %spread.1 = f32[128,1,1152]{2,1,0:T(1,128)} custom-call(s32[3]{0:T(128)S(1)} %pad_add_fusion.at, f32[32,128]{1,0:T(8,128)S(1)} %convert_reduce_fusion.row), custom_call_target="tpu_custom_call" | custom-call | tf_op jit(solution)/shard_map/spread/pallas_call | solution.py:247
  84.9 6.2 %all-to-all-start.2 = ((f32[128,1,1152]{2,1,0:T(1,128)}), f32[128,1,1152]{2,1,0:T(1,128)S(1)}, u32[]{:S(2)}, u32[]{:S(2)}) async-start(f32[128,1,1152]{2,1,0:T(1,128)} %spread.1), calls=%async_computation.2 | async-start | bytes 1179648 | tf_op jit(solution)/shard_map/all_to_all | solution.py:255
  91.1 1.8 %collective-permute-start.10 = (bf16[32,64,128]{2,1,0:T(8,128)(2,1)S(1)}, bf16[32,64,128]{2,1,0:T(8,128)(2,1)S(1)}, u32[]{:S(2)}, u32[]{:S(2)}) collective-permute-start(bf16[32,64,128]{2,1,0:T(8,128)(2,1)S(1)} %all-to-all-done.mine.rest_0_), channel_id=1, source_target_pairs={{0,3},{1,0},{2,1},{3,2},{4,7},{5,4},{6,5},{7,6},{8,11},{9,8},{10,9... | collective-permute-start | bytes 1572872 | tf_op jit(solution)/shard_map/ppermute | solution.py:233
  94.0 24.0 %all-to-all-done.2.mine = f32[128,1,1152]{2,1,0:T(1,128)S(1)} async-done(((f32[128,1,1152]{2,1,0:T(1,128)}), f32[128,1,1152]{2,1,0:T(1,128)S(1)}, u32[]{:S(2)}, u32[]{:S(2)}) %all-to-all-start.2) | async-done | bytes 589856 | tf_op jit(solution)/shard_map/all_to_all | solution.py:255
  118.0 2.6 %collective-permute-start.5 = (f32[128,1,1152]{2,1,0:T(1,128)S(1)}, f32[128,1,1152]{2,1,0:T(1,128)S(1)}, u32[]{:S(2)}, u32[]{:S(2)}) collective-permute-start(f32[128,1,1152]{2,1,0:T(1,128)S(1)} %all-to-all-done.2.mine), channel_id=1, source_target_pairs={{0,4},{4,0},{1,5},{5,1},{2,6},{6,2},{3,7},{7,3},{8,12},{12,8},{9,1... | collective-permute-start | bytes 1769480 | tf_op jit(solution)/shard_map/ppermute | solution.py:194
  120.6 1.8 %collective-permute-start.11 = (bf16[32,64,128]{2,1,0:T(8,128)(2,1)S(1)}, bf16[32,64,128]{2,1,0:T(8,128)(2,1)S(1)}, u32[]{:S(2)}, u32[]{:S(2)}) collective-permute-start(bf16[32,64,128]{2,1,0:T(8,128)(2,1)S(1)} %collective-permute-done.10.rest_6_), channel_id=1, source_target_pairs={{0,4},{4,0},{1,5},{5,1},{2,6},{6,2},{3,7},{7,3},{8,12},{12,8},{9,1... | collective-permute-start | bytes 1572872 | tf_op jit(solution)/shard_map/ppermute | solution.py:194
  122.4 2.8 %collective-permute-done.6.rest_2_ = bf16[32,64,128]{2,1,0:T(8,128)(2,1)} collective-permute-done((bf16[32,64,128]{2,1,0:T(8,128)(2,1)S(1)}, bf16[32,64,128]{2,1,0:T(8,128)(2,1)}, u32[]{:S(2)}, u32[]{:S(2)}) %collective-permute-start.6) | collective-permute-done | bytes 524320 | tf_op jit(solution)/shard_map/ppermute | solution.py:233
  125.8 1.7 %update.1 = (f32[256,1024]{1,0:T(8,128)S(1)}, f32[8,128]{1,0:T(8,128)S(1)}, f32[4,512]{1,0:T(4,128)}, f32[4,512]{1,0:T(4,128)}, f32[4,512]{1,0:T(4,128)}, /*index=5*/f32[4,512]{1,0:T(4,128)}) custom-call(s32[3]{0:T(128)S(1)} %pad_add_fusion.at, f32[128,1,1152]{2,1,0:T(1,128)S(1)} %all-to-all-done.2.mine, f32[128,1,1152]{2,1,0:T(1,128)S(1)} %collective-permute-done.5.theirs, ...), custom_call_target="tpu_custom_call" | custom-call | tf_op jit(solution)/shard_map/update/pallas_call | solution.py:257
  127.5 0.8 copy-done.6
  128.3 0.8 copy-done.7
  129.1 13.7 %finish.1 = (f32[64,512]{1,0:T(8,128)}, f32[64,512]{1,0:T(8,128)}, f32[64,512]{1,0:T(8,128)}, f32[64,512]{1,0:T(8,128)}, bf16[4096,512]{1,0:T(8,128)(2,1)}, /*index=5*/bf16[4096,512]{1,0:T(8,128)(2,1)}) custom-call(s32[3]{0:T(128)S(1)} %pad_add_fusion.at, f32[8,128]{1,0:T(8,128)S(1)} %get-tuple-element.31.factor, f32[256,1024]{1,0:T(8,128)S(1)} %get-tuple-element.32.low, ...), custom_call_target="tpu_custom_call" | custom-call | tf_op jit(solution)/shard_map/finish/pallas_call | solution.py:270
  (33 shorter events, 2.5 us)
Async XLA Ops:
  7.2 121.9 %all-gather.3.cloned.1.call-start = ((), (), s32[]{:S(2)}) async-start(), calls=%async_computation.3 | async-start | bytes 11182080 | tf_op jit(solution)/shard_map/all_gather | solution.py:226
  9.7 28.8 %all-to-all-start = ((bf16[32,64,128]{2,1,0:T(8,128)(2,1)}), bf16[32,64,128]{2,1,0:T(8,128)(2,1)S(1)}, u32[]{:S(2)}, u32[]{:S(2)}) async-start(bf16[32,64,128]{2,1,0:T(8,128)(2,1)} %get-tuple-element.27), calls=%async_computation | async-start | bytes 1048576 | tf_op jit(solution)/shard_map/all_to_all | solution.py:229
  21.6 20.9 %collective-permute-start.3 = (bf16[256,1024]{1,0:T(8,128)(2,1)S(1)}, bf16[256,1024]{1,0:T(8,128)(2,1)S(1)}, u32[]{:S(2)}, u32[]{:S(2)}) collective-permute-start(bf16[256,1024]{1,0:T(8,128)(2,1)S(1)} %get-tuple-element.28.c0), channel_id=1, source_target_pairs={{0,3},{1,0},{2,1},{3,2},{4,7},{5,4},{6,5},{7,6},{8,11},{9,8},{10,9... | collective-permute-start | bytes 1572872 | tf_op jit(solution)/shard_map/ppermute | solution.py:227
  24.4 18.1 %collective-permute-start.2 = (bf16[256,1024]{1,0:T(8,128)(2,1)S(1)}, bf16[256,1024]{1,0:T(8,128)(2,1)S(1)}, u32[]{:S(2)}, u32[]{:S(2)}) collective-permute-start(bf16[256,1024]{1,0:T(8,128)(2,1)S(1)} %get-tuple-element.28.c0), channel_id=1, source_target_pairs={{0,2},{1,3},{2,0},{3,1},{4,6},{5,7},{6,4},{7,5},{8,10},{9,11},{10,... | collective-permute-start | bytes 1572872 | tf_op jit(solution)/shard_map/ppermute | solution.py:227
  24.8 26.2 %collective-permute-start.1 = (bf16[256,1024]{1,0:T(8,128)(2,1)S(1)}, bf16[256,1024]{1,0:T(8,128)(2,1)S(1)}, u32[]{:S(2)}, u32[]{:S(2)}) collective-permute-start(bf16[256,1024]{1,0:T(8,128)(2,1)S(1)} %get-tuple-element.28.c0), channel_id=1, source_target_pairs={{0,1},{1,2},{2,3},{3,0},{4,5},{5,6},{6,7},{7,4},{8,9},{9,10},{10,1... | collective-permute-start | bytes 1572872 | tf_op jit(solution)/shard_map/ppermute | solution.py:227
  38.5 54.9 %copy-start = (bf16[32,64,128]{2,1,0:T(8,128)(2,1)}, bf16[32,64,128]{2,1,0:T(8,128)(2,1)S(1)}, u32[]{:S(2)}) copy-start(bf16[32,64,128]{2,1,0:T(8,128)(2,1)S(1)} %all-to-all-done.mine.rest_0_) | copy-start | bytes 1572868
  38.5 13.3 %collective-permute-start = (bf16[32,64,128]{2,1,0:T(8,128)(2,1)S(1)}, bf16[32,64,128]{2,1,0:T(8,128)(2,1)S(1)}, u32[]{:S(2)}, u32[]{:S(2)}) collective-permute-start(bf16[32,64,128]{2,1,0:T(8,128)(2,1)S(1)} %all-to-all-done.mine.rest_0_), channel_id=1, source_target_pairs={{0,4},{4,0},{1,5},{5,1},{2,6},{6,2},{3,7},{7,3},{8,12},{12,8},{9,1... | collective-permute-start | bytes 1572872 | tf_op jit(solution)/shard_map/ppermute | solution.py:194
  51.0 0.8 copy-start.2
  51.8 1.0 copy-start.3
  52.9 6.6 %copy-start.1 = (bf16[32,64,128]{2,1,0:T(8,128)(2,1)}, bf16[32,64,128]{2,1,0:T(8,128)(2,1)S(1)}, u32[]{:S(2)}) copy-start(bf16[32,64,128]{2,1,0:T(8,128)(2,1)S(1)} %collective-permute-done.theirs.rest_1_) | copy-start | bytes 1572868
  57.6 1.7 %collective-permute-start.4 = (f16[32,32,128]{2,1,0:T(8,128)(2,1)S(1)}, f16[32,32,128]{2,1,0:T(8,128)(2,1)S(1)}, u32[]{:S(2)}, u32[]{:S(2)}) collective-permute-start(f16[32,32,128]{2,1,0:T(8,128)(2,1)S(1)} %convert_element_type.12), channel_id=1, source_target_pairs={{0,4},{4,0},{1,5},{5,1},{2,6},{6,2},{3,7},{7,3},{8,12},{12,8},{9,1... | collective-permute-start | bytes 786440 | tf_op jit(solution)/shard_map/ppermute | solution.py:194
  84.9 33.1 %all-to-all-start.2 = ((f32[128,1,1152]{2,1,0:T(1,128)}), f32[128,1,1152]{2,1,0:T(1,128)S(1)}, u32[]{:S(2)}, u32[]{:S(2)}) async-start(f32[128,1,1152]{2,1,0:T(1,128)} %spread.1), calls=%async_computation.2 | async-start | bytes 1179648 | tf_op jit(solution)/shard_map/all_to_all | solution.py:255
  91.1 29.5 %collective-permute-start.10 = (bf16[32,64,128]{2,1,0:T(8,128)(2,1)S(1)}, bf16[32,64,128]{2,1,0:T(8,128)(2,1)S(1)}, u32[]{:S(2)}, u32[]{:S(2)}) collective-permute-start(bf16[32,64,128]{2,1,0:T(8,128)(2,1)S(1)} %all-to-all-done.mine.rest_0_), channel_id=1, source_target_pairs={{0,3},{1,0},{2,1},{3,2},{4,7},{5,4},{6,5},{7,6},{8,11},{9,8},{10,9... | collective-permute-start | bytes 1572872 | tf_op jit(solution)/shard_map/ppermute | solution.py:233
  92.9 29.5 %collective-permute-start.8 = (bf16[32,64,128]{2,1,0:T(8,128)(2,1)S(1)}, bf16[32,64,128]{2,1,0:T(8,128)(2,1)S(1)}, u32[]{:S(2)}, u32[]{:S(2)}) collective-permute-start(bf16[32,64,128]{2,1,0:T(8,128)(2,1)S(1)} %all-to-all-done.mine.rest_0_), channel_id=1, source_target_pairs={{0,2},{1,3},{2,0},{3,1},{4,6},{5,7},{6,4},{7,5},{8,10},{9,11},{10,... | collective-permute-start | bytes 1572872 | tf_op jit(solution)/shard_map/ppermute | solution.py:233
  93.4 31.8 %collective-permute-start.6 = (bf16[32,64,128]{2,1,0:T(8,128)(2,1)S(1)}, bf16[32,64,128]{2,1,0:T(8,128)(2,1)}, u32[]{:S(2)}, u32[]{:S(2)}) collective-permute-start(bf16[32,64,128]{2,1,0:T(8,128)(2,1)S(1)} %all-to-all-done.mine.rest_0_), channel_id=1, source_target_pairs={{0,1},{1,2},{2,3},{3,0},{4,5},{5,6},{6,7},{7,4},{8,9},{9,10},{10,1... | collective-permute-start | bytes 1572872 | tf_op jit(solution)/shard_map/ppermute | solution.py:233
  118.0 7.8 %collective-permute-start.5 = (f32[128,1,1152]{2,1,0:T(1,128)S(1)}, f32[128,1,1152]{2,1,0:T(1,128)S(1)}, u32[]{:S(2)}, u32[]{:S(2)}) collective-permute-start(f32[128,1,1152]{2,1,0:T(1,128)S(1)} %all-to-all-done.2.mine), channel_id=1, source_target_pairs={{0,4},{4,0},{1,5},{5,1},{2,6},{6,2},{3,7},{7,3},{8,12},{12,8},{9,1... | collective-permute-start | bytes 1769480 | tf_op jit(solution)/shard_map/ppermute | solution.py:194
  120.6 8.5 %copy-start.4 = (bf16[32,64,128]{2,1,0:T(8,128)(2,1)}, bf16[32,64,128]{2,1,0:T(8,128)(2,1)S(1)}, u32[]{:S(2)}) copy-start(bf16[32,64,128]{2,1,0:T(8,128)(2,1)S(1)} %collective-permute-done.10.rest_6_) | copy-start | bytes 1572868
  120.6 6.9 %collective-permute-start.11 = (bf16[32,64,128]{2,1,0:T(8,128)(2,1)S(1)}, bf16[32,64,128]{2,1,0:T(8,128)(2,1)S(1)}, u32[]{:S(2)}, u32[]{:S(2)}) collective-permute-start(bf16[32,64,128]{2,1,0:T(8,128)(2,1)S(1)} %collective-permute-done.10.rest_6_), channel_id=1, source_target_pairs={{0,4},{4,0},{1,5},{5,1},{2,6},{6,2},{3,7},{7,3},{8,12},{12,8},{9,1... | collective-permute-start | bytes 1572872 | tf_op jit(solution)/shard_map/ppermute | solution.py:194
  122.4 6.7 %copy-start.5 = (bf16[32,64,128]{2,1,0:T(8,128)(2,1)}, bf16[32,64,128]{2,1,0:T(8,128)(2,1)S(1)}, u32[]{:S(2)}) copy-start(bf16[32,64,128]{2,1,0:T(8,128)(2,1)S(1)} %collective-permute-done.8.rest_4_) | copy-start | bytes 1572868
  122.4 5.1 %collective-permute-start.9 = (bf16[32,64,128]{2,1,0:T(8,128)(2,1)S(1)}, bf16[32,64,128]{2,1,0:T(8,128)(2,1)S(1)}, u32[]{:S(2)}, u32[]{:S(2)}) collective-permute-start(bf16[32,64,128]{2,1,0:T(8,128)(2,1)S(1)} %collective-permute-done.8.rest_4_), channel_id=1, source_target_pairs={{0,4},{4,0},{1,5},{5,1},{2,6},{6,2},{3,7},{7,3},{8,12},{12,8},{9,1... | collective-permute-start | bytes 1572872 | tf_op jit(solution)/shard_map/ppermute | solution.py:194
  125.3 3.8 %collective-permute-start.7 = (bf16[32,64,128]{2,1,0:T(8,128)(2,1)}, bf16[32,64,128]{2,1,0:T(8,128)(2,1)}, u32[]{:S(2)}, u32[]{:S(2)}) collective-permute-start(bf16[32,64,128]{2,1,0:T(8,128)(2,1)} %collective-permute-done.6.rest_2_), channel_id=1, source_target_pairs={{0,4},{4,0},{1,5},{5,1},{2,6},{6,2},{3,7},{7,3},{8,12},{12,8},{9,1... | collective-permute-start | bytes 1572872 | tf_op jit(solution)/shard_map/ppermute | solution.py:194
  127.5 0.8 copy-start.6
  128.3 0.8 copy-start.7
Sparse Core Ops, SparseCore 0:
  11.3 105.2 all-gather.2

commit v2 on v1

--- a/solution.py
+++ b/solution.py
@@ -26,7 +26,7 @@
 MOMENTS_AT = 128
 TOPS_AT = 160
 BLOCK_ROWS = 168
-GROUP = 8
+GROUP = 16
 
 
 VMEM = pl.BlockSpec(memory_space=pltpu.VMEM)
@@ -169,7 +169,8 @@
 
     bases = []
     for k in range(4):
-        own, other = quarters[2 * k][...], quarters[2 * k + 1][...]
+        chips = pl.ds(pl.program_id(0) * (GROUP // 2), GROUP // 2)
+        own, other = quarters[k][...], quarters[4][...] if k == 0 else quarters[4 + k][chips]
         first = jnp.where(core == 0, own, other)
         second = jnp.where(core == 0, other, own)
         bases.append(jnp.concatenate([first, second], axis=1).reshape(GROUP * 64, 128))
@@ -192,6 +193,44 @@
 
 def swapped(values):
     return lax.ppermute(values, "fs_2", [(0, 1), (1, 0)])
+
+
+def finished(at, factor, low, query_basis, output_basis, query_master, output_master, gathered, quarters):
+    shape = jax.ShapeDtypeStruct
+
+    def whole(*dims):
+        return pl.BlockSpec(dims, lambda i: (0,) * len(dims))
+
+    local = whole(64, 512)
+    return pl.pallas_call(
+        finish_kernel,
+        grid=(64 // GROUP,),
+        in_specs=[
+            SMEM,
+            whole(8, 128),
+            whole(RANK, 1024),
+            whole(64, 256),
+            whole(64, 256),
+            local,
+            local,
+            pl.BlockSpec((64, 32, 512), lambda i: (0, MOMENTS_AT // 32, 0)),
+            pl.BlockSpec((GROUP, 128, 512), lambda i: (i, 0, 0)),
+            pl.BlockSpec((GROUP, 8, 512), lambda i: (i, TOPS_AT // 8, 0)),
+            *[pl.BlockSpec((GROUP // 2, 64, 128), lambda i: (i, 0, 0))] * 5,
+            *[VMEM] * 3,
+        ],
+        out_specs=[local] * 4 + [pl.BlockSpec((GROUP * 64, 512), lambda i: (i, 0))] * 2,
+        out_shape=[shape((64, 512), f32)] * 4 + [shape((D, 512), bf16)] * 2,
+        scratch_shapes=[pltpu.VMEM((RANK, 1024), bf16)] * 2,
+        compiler_params=pltpu.CompilerParams(dimension_semantics=("arbitrary",), vmem_limit_bytes=40 * 2**20),
+        name="finish",
+    )(
+        at,
+        *near(factor, low),
+        *far(query_basis, output_basis, query_master, output_master, gathered, gathered, gathered),
+        *far(*quarters[:5]),
+        *near(*quarters[5:]),
+    )
 
 
 def per_device(
@@ -228,10 +267,12 @@
     cots = [cots[i] for i in (0, 2, 1, 3)]
     mine = lax.all_to_all(send, CHIPS, 0, 0, tiled=True)
     theirs = swapped(mine)
-    quarters = [mine, theirs]
+    owns, others = [mine], [theirs]
     for k in range(1, 4):
         quarter = lax.ppermute(mine, "tp", [(i, (i + k) % 4) for i in range(4)])
-        quarters += [quarter, swapped(quarter)]
+        owns.append(quarter)
+        others.append(swapped(quarter))
+    quarters = owns + others
     keep, give = pl.pallas_call(
         project_kernel,
         in_specs=[SMEM] + [pl.BlockSpec(memory_space=pl.ANY)] * 2 + [VMEM] * 6,
@@ -263,35 +304,8 @@
         name="update",
     )(at, *near(mine, theirs), *far(*moments))
 
-    def whole(*dims):
-        return pl.BlockSpec(dims, lambda i: (0,) * len(dims))
-
-    local = whole(64, 512)
-    query_weight, output_weight, query_step, output_step, query_copy, output_copy = pl.pallas_call(
-        finish_kernel,
-        grid=(64 // GROUP,),
-        in_specs=[
-            SMEM,
-            whole(8, 128),
-            whole(RANK, 1024),
-            whole(64, 256),
-            whole(64, 256),
-            local,
-            local,
-            pl.BlockSpec((64, 32, 512), lambda i: (0, MOMENTS_AT // 32, 0)),
-            pl.BlockSpec((GROUP, 128, 512), lambda i: (i, 0, 0)),
-            pl.BlockSpec((GROUP, 8, 512), lambda i: (i, TOPS_AT // 8, 0)),
-            *[pl.BlockSpec((GROUP // 2, 64, 128), lambda i: (i, 0, 0))] * 8,
-        ],
-        out_specs=[local] * 4 + [pl.BlockSpec((GROUP * 64, 512), lambda i: (i, 0))] * 2,
-        out_shape=[shape((64, 512), f32)] * 4 + [shape((D, 512), bf16)] * 2,
-        scratch_shapes=[pltpu.VMEM((RANK, 1024), bf16)] * 2,
-        compiler_params=pltpu.CompilerParams(dimension_semantics=("arbitrary",), vmem_limit_bytes=40 * 2**20),
-        name="finish",
-    )(
-        at,
-        *near(factor, low),
-        *far(query_basis, output_basis, query_master, output_master, gathered, gathered, gathered, *quarters),
+    query_weight, output_weight, query_step, output_step, query_copy, output_copy = finished(
+        at, factor, low, query_basis, output_basis, query_master, output_master, gathered, quarters
     )
     return (
         query_weight,

time: 150 us -> 147 us (0.980)
  Pallas kernels: 24 us -> 22.2 us
  local copies, waits for them, and re-layouts: 3.44 us -> 1.84 us
    pallas_call x1, Pallas kernels: 13.7 us -> 11.9 us  [finished(): pl.pallas_call(finish_kernel, grid=(64 // GROUP,), in_specs=[SMEM, whole(...]
    unnamed x16 -> x8, local copies, waits for them, and re-layouts: 3.44 us -> 1.84 us
where the time goes in v2:
time: 147 us; the launch traced here: 146 us
  waiting for transfers between devices  49.7 us (34%)
  starting transfers between devices  34.2 us (23%)
  blocking collectives  23.9 us (16%)
  Pallas kernels  22.2 us (15%)
  between operations  14.1 us (10%)
  local copies, waits for them, and re-layouts  1.84 us (1%)
    all_to_all x1, waiting for transfers between devices, per_device(): mine = lax.all_to_all(out, (*CHIPS, 'tp'), 0, 0, tiled=True)  24 us
    all_to_all x1, blocking collectives, per_device(): arrived = lax.all_to_all(pair, CHIPS, 0, 0, tiled=True)  23.9 us
    all_to_all x1, waiting for transfers between devices, per_device(): mine = lax.all_to_all(send, CHIPS, 0, 0, tiled=True)  13.1 us
    pallas_call x1, Pallas kernels, finished(): pl.pallas_call(finish_kernel, grid=(64 // GROUP,), in_specs=[SMEM, whole(...  11.9 us
    all_to_all x1, starting transfers between devices, per_device(): mine = lax.all_to_all(send, CHIPS, 0, 0, tiled=True)  11.9 us
    ppermute x6, starting transfers between devices, swapped(): return lax.ppermute(values, 'fs_2', [(0, 1), (1, 0)])  9.39 us
    ppermute x3, waiting for transfers between devices, per_device(): lax.ppermute(cot, 'tp', [(i, (i + k) % 4) for i in range(4)])  8.51 us
    all_to_all x1, starting transfers between devices, per_device(): mine = lax.all_to_all(out, (*CHIPS, 'tp'), 0, 0, tiled=True)  6.18 us
  transfers between devices with their start and end apart: 15, of which 5 were waited for; matrix products, arithmetic and copies ran while one was open for 0% of the time, Pallas kernels for 5%

profile of v2, /device:TPU:1, one launch (start us, length us, event | category | flops | bytes accessed | tf_op | source)
XLA Modules:
  0.0 146.3 jit_solution(8206055137435728965)
XLA Ops:
  7.3 2.4 %pack.1 = (bf16[168,512]{1,0:T(8,128)(2,1)}, bf16[32,64,128]{2,1,0:T(8,128)(2,1)}, bf16[256,1024]{1,0:T(8,128)(2,1)S(1)}) custom-call(s32[3]{0:T(128)S(1)} %pad_add_fusion.at, bf16[64,256]{1,0:T(8,128)(2,1)} %qb.3, bf16[64,256]{1,0:T(8,128)(2,1)} %ob.3, f32[64,512]{1,0:T(8,128)} %qm.3, f32[64,512]{1,0:T(8,128)} %om.3, f32[4,512]{1,0:T(4,128)} %q1.3, ...), custom_call_target="tpu_custom_call" | custom-call | tf_op jit(solution)/shard_map/pack/pallas_call | solution.py:253
  9.7 11.9 %all-to-all-start = ((bf16[32,64,128]{2,1,0:T(8,128)(2,1)}), bf16[32,64,128]{2,1,0:T(8,128)(2,1)S(1)}, u32[]{:S(2)}, u32[]{:S(2)}) async-start(bf16[32,64,128]{2,1,0:T(8,128)(2,1)} %get-tuple-element.27), calls=%async_computation | async-start | bytes 1048576 | tf_op jit(solution)/shard_map/all_to_all | solution.py:268
  21.6 2.8 %collective-permute-start.3 = (bf16[256,1024]{1,0:T(8,128)(2,1)S(1)}, bf16[256,1024]{1,0:T(8,128)(2,1)S(1)}, u32[]{:S(2)}, u32[]{:S(2)}) collective-permute-start(bf16[256,1024]{1,0:T(8,128)(2,1)S(1)} %get-tuple-element.28.c0), channel_id=1, source_target_pairs={{0,3},{1,0},{2,1},{3,2},{4,7},{5,4},{6,5},{7,6},{8,11},{9,8},{10,9... | collective-permute-start | bytes 1572872 | tf_op jit(solution)/shard_map/ppermute | solution.py:266
  24.8 0.7 collective-permute-start.1
  25.5 13.1 %all-to-all-done.mine.rest_0_ = bf16[32,64,128]{2,1,0:T(8,128)(2,1)S(1)} async-done(((bf16[32,64,128]{2,1,0:T(8,128)(2,1)}), bf16[32,64,128]{2,1,0:T(8,128)(2,1)S(1)}, u32[]{:S(2)}, u32[]{:S(2)}) %all-to-all-start) | async-done | bytes 524320 | tf_op jit(solution)/shard_map/all_to_all | solution.py:268
  38.5 4.0 %collective-permute-start = (bf16[32,64,128]{2,1,0:T(8,128)(2,1)S(1)}, bf16[32,64,128]{2,1,0:T(8,128)(2,1)S(1)}, u32[]{:S(2)}, u32[]{:S(2)}) collective-permute-start(bf16[32,64,128]{2,1,0:T(8,128)(2,1)S(1)} %all-to-all-done.mine.rest_0_), channel_id=1, source_target_pairs={{0,4},{4,0},{1,5},{5,1},{2,6},{6,2},{3,7},{7,3},{8,12},{12,8},{9,1... | collective-permute-start | bytes 1572872 | tf_op jit(solution)/shard_map/ppermute | solution.py:195
  42.5 8.5 %collective-permute-done.1.c1 = bf16[256,1024]{1,0:T(8,128)(2,1)S(1)} collective-permute-done((bf16[256,1024]{1,0:T(8,128)(2,1)S(1)}, bf16[256,1024]{1,0:T(8,128)(2,1)S(1)}, u32[]{:S(2)}, u32[]{:S(2)}) %collective-permute-start.1) | collective-permute-done | bytes 524320 | tf_op jit(solution)/shard_map/ppermute | solution.py:266
  51.0 0.8 copy-done.2
  51.8 1.0 copy-done.3
  52.9 4.7 %project.1 = (f32[32,32,128]{2,1,0:T(8,128)S(1)}, f32[32,32,128]{2,1,0:T(8,128)S(1)}) custom-call(s32[3]{0:T(128)S(1)} %pad_add_fusion.at, bf16[256,4096]{1,0:T(8,128)(2,1)} %saved.1, bf16[256,4096]{1,0:T(8,128)(2,1)} %layer.1, bf16[32,64,128]{2,1,0:T(8,128)(2,1)S(1)} %all-to-all-done.mine.rest_0_, ...), custom_call_target="tpu_custom_call" | custom-call | tf_op jit(solution)/shard_map/project/pallas_call | solution.py:276
  57.6 0.6 collective-permute-start.4
  58.2 1.2 collective-permute-done.4
  59.4 23.9 %all_to_all.15 = f16[32,32,128]{2,1,0:T(8,128)(2,1)S(1)} all-to-all(f16[32,32,128]{2,1,0:T(8,128)(2,1)S(1)} %add_convert_fusion), channel_id=1, replica_groups=mesh['fs_0'=8,'fs_1'=4,'fs_2'=2,'tp'=4] {'fs_0','fs_1'}, dimensions={0} | all-to-all | bytes 524288 | tf_op jit(solution)/shard_map/all_to_all | solution.py:286
  83.4 1.5 %spread.1 = f32[128,1,1152]{2,1,0:T(1,128)} custom-call(s32[3]{0:T(128)S(1)} %pad_add_fusion.at, f32[32,128]{1,0:T(8,128)S(1)} %convert_reduce_fusion.row), custom_call_target="tpu_custom_call" | custom-call | tf_op jit(solution)/shard_map/spread/pallas_call | solution.py:288
  84.9 6.2 %all-to-all-start.2 = ((f32[128,1,1152]{2,1,0:T(1,128)}), f32[128,1,1152]{2,1,0:T(1,128)S(1)}, u32[]{:S(2)}, u32[]{:S(2)}) async-start(f32[128,1,1152]{2,1,0:T(1,128)} %spread.1), calls=%async_computation.2 | async-start | bytes 1179648 | tf_op jit(solution)/shard_map/all_to_all | solution.py:296
  91.1 1.8 %collective-permute-start.8 = (bf16[32,64,128]{2,1,0:T(8,128)(2,1)S(1)}, bf16[32,64,128]{2,1,0:T(8,128)(2,1)}, u32[]{:S(2)}, u32[]{:S(2)}) collective-permute-start(bf16[32,64,128]{2,1,0:T(8,128)(2,1)S(1)} %all-to-all-done.mine.rest_0_), channel_id=1, source_target_pairs={{0,3},{1,0},{2,1},{3,2},{4,7},{5,4},{6,5},{7,6},{8,11},{9,8},{10,9... | collective-permute-start | bytes 1572872 | tf_op jit(solution)/shard_map/ppermute | solution.py:272
  92.9 0.6 collective-permute-start.7
  93.4 0.6 collective-permute-start.6
  94.0 24.0 %all-to-all-done.2.mine = f32[128,1,1152]{2,1,0:T(1,128)S(1)} async-done(((f32[128,1,1152]{2,1,0:T(1,128)}), f32[128,1,1152]{2,1,0:T(1,128)S(1)}, u32[]{:S(2)}, u32[]{:S(2)}) %all-to-all-start.2) | async-done | bytes 589856 | tf_op jit(solution)/shard_map/all_to_all | solution.py:296
  118.0 2.6 %collective-permute-start.5 = (f32[128,1,1152]{2,1,0:T(1,128)S(1)}, f32[128,1,1152]{2,1,0:T(1,128)S(1)}, u32[]{:S(2)}, u32[]{:S(2)}) collective-permute-start(f32[128,1,1152]{2,1,0:T(1,128)S(1)} %all-to-all-done.2.mine), channel_id=1, source_target_pairs={{0,4},{4,0},{1,5},{5,1},{2,6},{6,2},{3,7},{7,3},{8,12},{12,8},{9,1... | collective-permute-start | bytes 1769480 | tf_op jit(solution)/shard_map/ppermute | solution.py:195
  120.6 1.8 %collective-permute-start.11 = (bf16[32,64,128]{2,1,0:T(8,128)(2,1)}, bf16[32,64,128]{2,1,0:T(8,128)(2,1)S(1)}, u32[]{:S(2)}, u32[]{:S(2)}) collective-permute-start(bf16[32,64,128]{2,1,0:T(8,128)(2,1)} %collective-permute-done.8.rest_3_), channel_id=1, source_target_pairs={{0,4},{4,0},{1,5},{5,1},{2,6},{6,2},{3,7},{7,3},{8,12},{12,8},{9,1... | collective-permute-start | bytes 1572872 | tf_op jit(solution)/shard_map/ppermute | solution.py:195
  122.4 2.9 %collective-permute-done.6.rest_1_ = bf16[32,64,128]{2,1,0:T(8,128)(2,1)} collective-permute-done((bf16[32,64,128]{2,1,0:T(8,128)(2,1)S(1)}, bf16[32,64,128]{2,1,0:T(8,128)(2,1)}, u32[]{:S(2)}, u32[]{:S(2)}) %collective-permute-start.6) | collective-permute-done | bytes 524320 | tf_op jit(solution)/shard_map/ppermute | solution.py:272
  125.8 1.7 %update.1 = (f32[256,1024]{1,0:T(8,128)S(1)}, f32[8,128]{1,0:T(8,128)S(1)}, f32[4,512]{1,0:T(4,128)}, f32[4,512]{1,0:T(4,128)}, f32[4,512]{1,0:T(4,128)}, /*index=5*/f32[4,512]{1,0:T(4,128)}) custom-call(s32[3]{0:T(128)S(1)} %pad_add_fusion.at, f32[128,1,1152]{2,1,0:T(1,128)S(1)} %all-to-all-done.2.mine, f32[128,1,1152]{2,1,0:T(1,128)S(1)} %collective-permute-done.5.theirs, ...), custom_call_target="tpu_custom_call" | custom-call | tf_op jit(solution)/shard_map/update/pallas_call | solution.py:298
  127.5 11.9 %finish.1 = (f32[64,512]{1,0:T(8,128)}, f32[64,512]{1,0:T(8,128)}, f32[64,512]{1,0:T(8,128)}, f32[64,512]{1,0:T(8,128)}, bf16[4096,512]{1,0:T(8,128)(2,1)}, /*index=5*/bf16[4096,512]{1,0:T(8,128)(2,1)}) custom-call(s32[3]{0:T(128)S(1)} %pad_add_fusion.at, f32[8,128]{1,0:T(8,128)S(1)} %get-tuple-element.31.factor, f32[256,1024]{1,0:T(8,128)S(1)} %get-tuple-element.32.low, ...), custom_call_target="tpu_custom_call" | custom-call | tf_op jit(solution)/shard_map/finish/pallas_call | solution.py:205
  (25 shorter events, 1.2 us)
Async XLA Ops:
  7.2 120.3 %all-gather.3.cloned.1.call-start = ((), (), s32[]{:S(2)}) async-start(), calls=%async_computation.3 | async-start | bytes 11182080 | tf_op jit(solution)/shard_map/all_gather | solution.py:265
  9.7 28.8 %all-to-all-start = ((bf16[32,64,128]{2,1,0:T(8,128)(2,1)}), bf16[32,64,128]{2,1,0:T(8,128)(2,1)S(1)}, u32[]{:S(2)}, u32[]{:S(2)}) async-start(bf16[32,64,128]{2,1,0:T(8,128)(2,1)} %get-tuple-element.27), calls=%async_computation | async-start | bytes 1048576 | tf_op jit(solution)/shard_map/all_to_all | solution.py:268
  21.6 20.9 %collective-permute-start.3 = (bf16[256,1024]{1,0:T(8,128)(2,1)S(1)}, bf16[256,1024]{1,0:T(8,128)(2,1)S(1)}, u32[]{:S(2)}, u32[]{:S(2)}) collective-permute-start(bf16[256,1024]{1,0:T(8,128)(2,1)S(1)} %get-tuple-element.28.c0), channel_id=1, source_target_pairs={{0,3},{1,0},{2,1},{3,2},{4,7},{5,4},{6,5},{7,6},{8,11},{9,8},{10,9... | collective-permute-start | bytes 1572872 | tf_op jit(solution)/shard_map/ppermute | solution.py:266
  24.4 18.1 %collective-permute-start.2 = (bf16[256,1024]{1,0:T(8,128)(2,1)S(1)}, bf16[256,1024]{1,0:T(8,128)(2,1)S(1)}, u32[]{:S(2)}, u32[]{:S(2)}) collective-permute-start(bf16[256,1024]{1,0:T(8,128)(2,1)S(1)} %get-tuple-element.28.c0), channel_id=1, source_target_pairs={{0,2},{1,3},{2,0},{3,1},{4,6},{5,7},{6,4},{7,5},{8,10},{9,11},{10,... | collective-permute-start | bytes 1572872 | tf_op jit(solution)/shard_map/ppermute | solution.py:266
  24.8 26.2 %collective-permute-start.1 = (bf16[256,1024]{1,0:T(8,128)(2,1)S(1)}, bf16[256,1024]{1,0:T(8,128)(2,1)S(1)}, u32[]{:S(2)}, u32[]{:S(2)}) collective-permute-start(bf16[256,1024]{1,0:T(8,128)(2,1)S(1)} %get-tuple-element.28.c0), channel_id=1, source_target_pairs={{0,1},{1,2},{2,3},{3,0},{4,5},{5,6},{6,7},{7,4},{8,9},{9,10},{10,1... | collective-permute-start | bytes 1572872 | tf_op jit(solution)/shard_map/ppermute | solution.py:266
  38.5 54.9 %copy-start = (bf16[32,64,128]{2,1,0:T(8,128)(2,1)}, bf16[32,64,128]{2,1,0:T(8,128)(2,1)S(1)}, u32[]{:S(2)}) copy-start(bf16[32,64,128]{2,1,0:T(8,128)(2,1)S(1)} %all-to-all-done.mine.rest_0_) | copy-start | bytes 1572868
  38.5 13.3 %collective-permute-start = (bf16[32,64,128]{2,1,0:T(8,128)(2,1)S(1)}, bf16[32,64,128]{2,1,0:T(8,128)(2,1)S(1)}, u32[]{:S(2)}, u32[]{:S(2)}) collective-permute-start(bf16[32,64,128]{2,1,0:T(8,128)(2,1)S(1)} %all-to-all-done.mine.rest_0_), channel_id=1, source_target_pairs={{0,4},{4,0},{1,5},{5,1},{2,6},{6,2},{3,7},{7,3},{8,12},{12,8},{9,1... | collective-permute-start | bytes 1572872 | tf_op jit(solution)/shard_map/ppermute | solution.py:195
  51.0 0.8 copy-start.2
  51.8 1.0 copy-start.3
  52.9 6.6 %copy-start.1 = (bf16[32,64,128]{2,1,0:T(8,128)(2,1)}, bf16[32,64,128]{2,1,0:T(8,128)(2,1)S(1)}, u32[]{:S(2)}) copy-start(bf16[32,64,128]{2,1,0:T(8,128)(2,1)S(1)} %collective-permute-done.theirs.rest_4_) | copy-start | bytes 1572868
  57.6 1.7 %collective-permute-start.4 = (f16[32,32,128]{2,1,0:T(8,128)(2,1)S(1)}, f16[32,32,128]{2,1,0:T(8,128)(2,1)S(1)}, u32[]{:S(2)}, u32[]{:S(2)}) collective-permute-start(f16[32,32,128]{2,1,0:T(8,128)(2,1)S(1)} %convert_element_type.12), channel_id=1, source_target_pairs={{0,4},{4,0},{1,5},{5,1},{2,6},{6,2},{3,7},{7,3},{8,12},{12,8},{9,1... | collective-permute-start | bytes 786440 | tf_op jit(solution)/shard_map/ppermute | solution.py:195
  84.9 33.1 %all-to-all-start.2 = ((f32[128,1,1152]{2,1,0:T(1,128)}), f32[128,1,1152]{2,1,0:T(1,128)S(1)}, u32[]{:S(2)}, u32[]{:S(2)}) async-start(f32[128,1,1152]{2,1,0:T(1,128)} %spread.1), calls=%async_computation.2 | async-start | bytes 1179648 | tf_op jit(solution)/shard_map/all_to_all | solution.py:296
  91.1 29.5 %collective-permute-start.8 = (bf16[32,64,128]{2,1,0:T(8,128)(2,1)S(1)}, bf16[32,64,128]{2,1,0:T(8,128)(2,1)}, u32[]{:S(2)}, u32[]{:S(2)}) collective-permute-start(bf16[32,64,128]{2,1,0:T(8,128)(2,1)S(1)} %all-to-all-done.mine.rest_0_), channel_id=1, source_target_pairs={{0,3},{1,0},{2,1},{3,2},{4,7},{5,4},{6,5},{7,6},{8,11},{9,8},{10,9... | collective-permute-start | bytes 1572872 | tf_op jit(solution)/shard_map/ppermute | solution.py:272
  92.9 29.5 %collective-permute-start.7 = (bf16[32,64,128]{2,1,0:T(8,128)(2,1)S(1)}, bf16[32,64,128]{2,1,0:T(8,128)(2,1)}, u32[]{:S(2)}, u32[]{:S(2)}) collective-permute-start(bf16[32,64,128]{2,1,0:T(8,128)(2,1)S(1)} %all-to-all-done.mine.rest_0_), channel_id=1, source_target_pairs={{0,2},{1,3},{2,0},{3,1},{4,6},{5,7},{6,4},{7,5},{8,10},{9,11},{10,... | collective-permute-start | bytes 1572872 | tf_op jit(solution)/shard_map/ppermute | solution.py:272
  93.4 31.8 %collective-permute-start.6 = (bf16[32,64,128]{2,1,0:T(8,128)(2,1)S(1)}, bf16[32,64,128]{2,1,0:T(8,128)(2,1)}, u32[]{:S(2)}, u32[]{:S(2)}) collective-permute-start(bf16[32,64,128]{2,1,0:T(8,128)(2,1)S(1)} %all-to-all-done.mine.rest_0_), channel_id=1, source_target_pairs={{0,1},{1,2},{2,3},{3,0},{4,5},{5,6},{6,7},{7,4},{8,9},{9,10},{10,1... | collective-permute-start | bytes 1572872 | tf_op jit(solution)/shard_map/ppermute | solution.py:272
  118.0 7.8 %collective-permute-start.5 = (f32[128,1,1152]{2,1,0:T(1,128)S(1)}, f32[128,1,1152]{2,1,0:T(1,128)S(1)}, u32[]{:S(2)}, u32[]{:S(2)}) collective-permute-start(f32[128,1,1152]{2,1,0:T(1,128)S(1)} %all-to-all-done.2.mine), channel_id=1, source_target_pairs={{0,4},{4,0},{1,5},{5,1},{2,6},{6,2},{3,7},{7,3},{8,12},{12,8},{9,1... | collective-permute-start | bytes 1769480 | tf_op jit(solution)/shard_map/ppermute | solution.py:195
  120.6 6.9 %collective-permute-start.11 = (bf16[32,64,128]{2,1,0:T(8,128)(2,1)}, bf16[32,64,128]{2,1,0:T(8,128)(2,1)S(1)}, u32[]{:S(2)}, u32[]{:S(2)}) collective-permute-start(bf16[32,64,128]{2,1,0:T(8,128)(2,1)} %collective-permute-done.8.rest_3_), channel_id=1, source_target_pairs={{0,4},{4,0},{1,5},{5,1},{2,6},{6,2},{3,7},{7,3},{8,12},{12,8},{9,1... | collective-permute-start | bytes 1572872 | tf_op jit(solution)/shard_map/ppermute | solution.py:195
  122.3 5.1 %collective-permute-start.10 = (bf16[32,64,128]{2,1,0:T(8,128)(2,1)}, bf16[32,64,128]{2,1,0:T(8,128)(2,1)S(1)}, u32[]{:S(2)}, u32[]{:S(2)}) collective-permute-start(bf16[32,64,128]{2,1,0:T(8,128)(2,1)} %collective-permute-done.7.rest_2_), channel_id=1, source_target_pairs={{0,4},{4,0},{1,5},{5,1},{2,6},{6,2},{3,7},{7,3},{8,12},{12,8},{9,1... | collective-permute-start | bytes 1572872 | tf_op jit(solution)/shard_map/ppermute | solution.py:195
  125.3 2.2 %collective-permute-start.9 = (bf16[32,64,128]{2,1,0:T(8,128)(2,1)}, bf16[32,64,128]{2,1,0:T(8,128)(2,1)S(1)}, u32[]{:S(2)}, u32[]{:S(2)}) collective-permute-start(bf16[32,64,128]{2,1,0:T(8,128)(2,1)} %collective-permute-done.6.rest_1_), channel_id=1, source_target_pairs={{0,4},{4,0},{1,5},{5,1},{2,6},{6,2},{3,7},{7,3},{8,12},{12,8},{9,1... | collective-permute-start | bytes 1572872 | tf_op jit(solution)/shard_map/ppermute | solution.py:195
Sparse Core Ops, SparseCore 0:
  11.3 105.2 all-gather.2

commit v3 on v2

--- a/solution.py
+++ b/solution.py
@@ -24,8 +24,8 @@
 SHRINK = 2.0**-10
 
 MOMENTS_AT = 128
-TOPS_AT = 160
-BLOCK_ROWS = 168
+TOPS_AT = 144
+BLOCK_ROWS = 152
 GROUP = 16
 
 
@@ -36,6 +36,12 @@
 def high_and_low(values):
     high = values.astype(bf16).astype(f32)
     return high, values - high
+
+
+def coded(values):
+    top = jnp.max(jnp.abs(values), axis=(0, 1), keepdims=True) * 1.01 + 1e-30
+    top = top.astype(bf16).astype(f32)
+    return jnp.exp(values * (REACH / top)), top
 
 
 def pack_kernel(at, qb, ob, qm, om, q1, q2, o1, o2, qc, oc, block, send, cot):
@@ -48,22 +54,20 @@
             part = jnp.where(tp == t, full[:, 64 * t : 64 * t + 64], part)
         picked.append(part)
     send[...] = jnp.broadcast_to(jnp.concatenate(picked, axis=1).astype(bf16)[None], send.shape)
-    tops = []
+    row = lax.broadcasted_iota(jnp.int32, (8, 512), 0)
+    tops = jnp.zeros((8, 512), f32)
     for side, master in ((0, qm), (1, om)):
-        values = master[...]
-        top = jnp.max(jnp.abs(values), axis=(0, 1), keepdims=True) * 1.01 + 1e-30
-        top = top.astype(bf16).astype(f32)
-        block[64 * side : 64 * side + 64, :] = jnp.exp(values * (REACH / top)).astype(bf16)
-        tops.append(top)
-    for side, (first, second) in enumerate(((q1, q2), (o1, o2))):
-        first_high, first_low = high_and_low(first[...])
-        second_high, second_low = high_and_low(second[...])
-        at_row = MOMENTS_AT + 16 * side
-        block[at_row : at_row + 16, :] = jnp.concatenate(
-            [first_high, second_high, first_low, second_low], axis=0
-        ).astype(bf16)
-    row = lax.broadcasted_iota(jnp.int32, (8, 512), 0)
-    block[TOPS_AT:, :] = jnp.where(row == 0, tops[0], tops[1]).astype(bf16)
+        codes, top = coded(master[...])
+        block[64 * side : 64 * side + 64, :] = codes.astype(bf16)
+        tops = jnp.where(row == side, top, tops)
+    held = []
+    for side, first, second in ((0, q1, q2), (1, o1, o2)):
+        for at_row, values in ((2 + side, first), (4 + side, second)):
+            codes, top = coded(values[...])
+            held.append(codes)
+            tops = jnp.where(row == at_row, top, tops)
+    block[MOMENTS_AT : MOMENTS_AT + 16, :] = jnp.concatenate(held, axis=0).astype(bf16)
+    block[TOPS_AT:, :] = tops.astype(bf16)
     cot[:, :512] = qc[...]
     cot[:, 512:] = oc[...]
 
@@ -145,13 +149,19 @@
     def _():
         scale = factor[0:1, 0:1]
 
+        is_first = lax.broadcasted_iota(jnp.int32, (8, 512), 0) < 4
+
         def rows(i, carry):
-            held = moments[pl.ds(4 * i, 4)].astype(f32)
+            codes = moments[pl.ds(4 * i, 4)].astype(f32)
+            units = tops[pl.ds(4 * i, 4)].astype(f32) * (1.0 / REACH)
             lows = low[pl.ds(16 * i, 16), :] * scale
             for side in range(2):
-                sums = [held[j, 16 * side : 16 * side + 8] + held[j, 16 * side + 8 : 16 * side + 16] for j in range(4)]
-                first = jnp.concatenate([s[:4] for s in sums], axis=0)
-                second = jnp.concatenate([s[4:] for s in sums], axis=0)
+                held = []
+                for j in range(4):
+                    unit = jnp.where(is_first, units[j, 2 + side : 3 + side], units[j, 4 + side : 5 + side])
+                    held.append(jnp.log(codes[j, 8 * side : 8 * side + 8]) * unit)
+                first = jnp.concatenate([h[:4] for h in held], axis=0)
+                second = jnp.concatenate([h[4:] for h in held], axis=0)
                 scaled = lows[:, 512 * side : 512 * side + 512]
                 first = beta_one * first + (1.0 - beta_one) * scaled
                 second = beta_two * second + (1.0 - beta_two) * scaled * scaled
@@ -178,7 +188,8 @@
         basis = jnp.concatenate([b[:, 64 * side : 64 * side + 64] for b in bases], axis=1)
         moved = jnp.dot(basis, direction[:, 512 * side : 512 * side + 512], preferred_element_type=f32)
         codes = block[:, 64 * side : 64 * side + 64, :].astype(f32)
-        unit = tops[:, side : side + 1, :].astype(f32) * (1.0 / REACH)
+        blocks = pl.ds(pl.program_id(0) * GROUP, GROUP)
+        unit = tops[blocks, side : side + 1, :].astype(f32) * (1.0 / REACH)
         master = (jnp.log(codes) * unit).reshape(GROUP * 64, 512)
         copy[...] = (master - rate * moved).astype(bf16)
 
@@ -213,9 +224,9 @@
             whole(64, 256),
             local,
             local,
-            pl.BlockSpec((64, 32, 512), lambda i: (0, MOMENTS_AT // 32, 0)),
+            pl.BlockSpec((64, 16, 512), lambda i: (0, MOMENTS_AT // 16, 0)),
             pl.BlockSpec((GROUP, 128, 512), lambda i: (i, 0, 0)),
-            pl.BlockSpec((GROUP, 8, 512), lambda i: (i, TOPS_AT // 8, 0)),
+            pl.BlockSpec((64, 8, 512), lambda i: (0, TOPS_AT // 8, 0)),
             *[pl.BlockSpec((GROUP // 2, 64, 128), lambda i: (i, 0, 0))] * 5,
             *[VMEM] * 3,
         ],

time: 147 us -> 147 us (level)
  waiting for transfers between devices: 49.7 us -> 47.6 us
  starting transfers between devices: 34.2 us -> 36.2 us
    all_to_all x1, waiting for transfers between devices: 24 us -> 21.9 us  [per_device(): mine = lax.all_to_all(out, (*CHIPS, 'tp'), 0, 0, tiled=True)]
    ppermute x6, starting transfers between devices: 9.39 us -> 11.3 us  [swapped(): return lax.ppermute(values, 'fs_2', [(0, 1), (1, 0)])]
where the time goes in v3:
time: 147 us; the launch traced here: 146 us
  waiting for transfers between devices  47.6 us (32%)
  starting transfers between devices  36.2 us (25%)
  blocking collectives  24 us (16%)
  Pallas kernels  22.2 us (15%)
  between operations  14.1 us (10%)
  local copies, waits for them, and re-layouts  1.84 us (1%)
    all_to_all x1, blocking collectives, per_device(): arrived = lax.all_to_all(pair, CHIPS, 0, 0, tiled=True)  24 us
    all_to_all x1, waiting for transfers between devices, per_device(): mine = lax.all_to_all(out, (*CHIPS, 'tp'), 0, 0, tiled=True)  21.9 us
    all_to_all x1, waiting for transfers between devices, per_device(): mine = lax.all_to_all(send, CHIPS, 0, 0, tiled=True)  13.1 us
    pallas_call x1, Pallas kernels, finished(): pl.pallas_call(finish_kernel, grid=(64 // GROUP,), in_specs=[SMEM, whole(...  11.9 us
    all_to_all x1, starting transfers between devices, per_device(): mine = lax.all_to_all(send, CHIPS, 0, 0, tiled=True)  11.9 us
    ppermute x6, starting transfers between devices, swapped(): return lax.ppermute(values, 'fs_2', [(0, 1), (1, 0)])  11.3 us
    ppermute x3, waiting for transfers between devices, per_device(): lax.ppermute(cot, 'tp', [(i, (i + k) % 4) for i in range(4)])  8.62 us
    all_to_all x1, starting transfers between devices, per_device(): mine = lax.all_to_all(out, (*CHIPS, 'tp'), 0, 0, tiled=True)  6.18 us
  transfers between devices with their start and end apart: 15, of which 5 were waited for; matrix products, arithmetic and copies ran while one was open for 0% of the time, Pallas kernels for 5%

profile of v3, /device:TPU:1, one launch (start us, length us, event | category | flops | bytes accessed | tf_op | source)
XLA Modules:
  0.0 146.3 jit_solution(18106313657144495224)
XLA Ops:
  7.3 2.4 %pack.1 = (bf16[152,512]{1,0:T(8,128)(2,1)}, bf16[32,64,128]{2,1,0:T(8,128)(2,1)}, bf16[256,1024]{1,0:T(8,128)(2,1)S(1)}) custom-call(s32[3]{0:T(128)S(1)} %pad_add_fusion.at, bf16[64,256]{1,0:T(8,128)(2,1)} %qb.3, bf16[64,256]{1,0:T(8,128)(2,1)} %ob.3, f32[64,512]{1,0:T(8,128)} %qm.3, f32[64,512]{1,0:T(8,128)} %om.3, f32[4,512]{1,0:T(4,128)} %q1.3, ...), custom_call_target="tpu_custom_call" | custom-call | tf_op jit(solution)/shard_map/pack/pallas_call | solution.py:264
  9.8 11.9 %all-to-all-start = ((bf16[32,64,128]{2,1,0:T(8,128)(2,1)}), bf16[32,64,128]{2,1,0:T(8,128)(2,1)S(1)}, u32[]{:S(2)}, u32[]{:S(2)}) async-start(bf16[32,64,128]{2,1,0:T(8,128)(2,1)} %get-tuple-element.27), calls=%async_computation | async-start | bytes 1048576 | tf_op jit(solution)/shard_map/all_to_all | solution.py:279
  21.6 2.8 %collective-permute-start.3 = (bf16[256,1024]{1,0:T(8,128)(2,1)S(1)}, bf16[256,1024]{1,0:T(8,128)(2,1)S(1)}, u32[]{:S(2)}, u32[]{:S(2)}) collective-permute-start(bf16[256,1024]{1,0:T(8,128)(2,1)S(1)} %get-tuple-element.28.c0), channel_id=1, source_target_pairs={{0,3},{1,0},{2,1},{3,2},{4,7},{5,4},{6,5},{7,6},{8,11},{9,8},{10,9... | collective-permute-start | bytes 1572872 | tf_op jit(solution)/shard_map/ppermute | solution.py:277
  24.8 0.7 collective-permute-start.1
  25.5 13.1 %all-to-all-done.mine.rest_0_ = bf16[32,64,128]{2,1,0:T(8,128)(2,1)S(1)} async-done(((bf16[32,64,128]{2,1,0:T(8,128)(2,1)}), bf16[32,64,128]{2,1,0:T(8,128)(2,1)S(1)}, u32[]{:S(2)}, u32[]{:S(2)}) %all-to-all-start) | async-done | bytes 524320 | tf_op jit(solution)/shard_map/all_to_all | solution.py:279
  38.6 3.9 %collective-permute-start = (bf16[32,64,128]{2,1,0:T(8,128)(2,1)S(1)}, bf16[32,64,128]{2,1,0:T(8,128)(2,1)S(1)}, u32[]{:S(2)}, u32[]{:S(2)}) collective-permute-start(bf16[32,64,128]{2,1,0:T(8,128)(2,1)S(1)} %all-to-all-done.mine.rest_0_), channel_id=1, source_target_pairs={{0,4},{4,0},{1,5},{5,1},{2,6},{6,2},{3,7},{7,3},{8,12},{12,8},{9,1... | collective-permute-start | bytes 1572872 | tf_op jit(solution)/shard_map/ppermute | solution.py:206
  42.4 8.6 %collective-permute-done.1.c1 = bf16[256,1024]{1,0:T(8,128)(2,1)S(1)} collective-permute-done((bf16[256,1024]{1,0:T(8,128)(2,1)S(1)}, bf16[256,1024]{1,0:T(8,128)(2,1)S(1)}, u32[]{:S(2)}, u32[]{:S(2)}) %collective-permute-start.1) | collective-permute-done | bytes 524320 | tf_op jit(solution)/shard_map/ppermute | solution.py:277
  51.0 0.8 copy-done.2
  51.8 1.0 copy-done.3
  52.9 4.7 %project.1 = (f32[32,32,128]{2,1,0:T(8,128)S(1)}, f32[32,32,128]{2,1,0:T(8,128)S(1)}) custom-call(s32[3]{0:T(128)S(1)} %pad_add_fusion.at, bf16[256,4096]{1,0:T(8,128)(2,1)} %saved.1, bf16[256,4096]{1,0:T(8,128)(2,1)} %layer.1, bf16[32,64,128]{2,1,0:T(8,128)(2,1)S(1)} %all-to-all-done.mine.rest_0_, ...), custom_call_target="tpu_custom_call" | custom-call | tf_op jit(solution)/shard_map/project/pallas_call | solution.py:287
  57.6 0.6 collective-permute-start.4
  58.2 1.2 collective-permute-done.4
  59.4 24.0 %all_to_all.15 = f16[32,32,128]{2,1,0:T(8,128)(2,1)S(1)} all-to-all(f16[32,32,128]{2,1,0:T(8,128)(2,1)S(1)} %add_convert_fusion), channel_id=1, replica_groups=mesh['fs_0'=8,'fs_1'=4,'fs_2'=2,'tp'=4] {'fs_0','fs_1'}, dimensions={0} | all-to-all | bytes 524288 | tf_op jit(solution)/shard_map/all_to_all | solution.py:297
  83.5 1.5 %spread.1 = f32[128,1,1152]{2,1,0:T(1,128)} custom-call(s32[3]{0:T(128)S(1)} %pad_add_fusion.at, f32[32,128]{1,0:T(8,128)S(1)} %convert_reduce_fusion.row), custom_call_target="tpu_custom_call" | custom-call | tf_op jit(solution)/shard_map/spread/pallas_call | solution.py:299
  85.0 6.2 %all-to-all-start.2 = ((f32[128,1,1152]{2,1,0:T(1,128)}), f32[128,1,1152]{2,1,0:T(1,128)S(1)}, u32[]{:S(2)}, u32[]{:S(2)}) async-start(f32[128,1,1152]{2,1,0:T(1,128)} %spread.1), calls=%async_computation.2 | async-start | bytes 1179648 | tf_op jit(solution)/shard_map/all_to_all | solution.py:307
  91.2 1.8 %collective-permute-start.8 = (bf16[32,64,128]{2,1,0:T(8,128)(2,1)S(1)}, bf16[32,64,128]{2,1,0:T(8,128)(2,1)}, u32[]{:S(2)}, u32[]{:S(2)}) collective-permute-start(bf16[32,64,128]{2,1,0:T(8,128)(2,1)S(1)} %all-to-all-done.mine.rest_0_), channel_id=1, source_target_pairs={{0,3},{1,0},{2,1},{3,2},{4,7},{5,4},{6,5},{7,6},{8,11},{9,8},{10,9... | collective-permute-start | bytes 1572872 | tf_op jit(solution)/shard_map/ppermute | solution.py:283
  92.9 0.6 collective-permute-start.7
  93.5 0.6 collective-permute-start.6
  94.1 21.9 %all-to-all-done.2.mine = f32[128,1,1152]{2,1,0:T(1,128)S(1)} async-done(((f32[128,1,1152]{2,1,0:T(1,128)}), f32[128,1,1152]{2,1,0:T(1,128)S(1)}, u32[]{:S(2)}, u32[]{:S(2)}) %all-to-all-start.2) | async-done | bytes 589856 | tf_op jit(solution)/shard_map/all_to_all | solution.py:307
  115.9 2.4 %collective-permute-start.5 = (f32[128,1,1152]{2,1,0:T(1,128)S(1)}, f32[128,1,1152]{2,1,0:T(1,128)S(1)}, u32[]{:S(2)}, u32[]{:S(2)}) collective-permute-start(f32[128,1,1152]{2,1,0:T(1,128)S(1)} %all-to-all-done.2.mine), channel_id=1, source_target_pairs={{0,4},{4,0},{1,5},{5,1},{2,6},{6,2},{3,7},{7,3},{8,12},{12,8},{9,1... | collective-permute-start | bytes 1769480 | tf_op jit(solution)/shard_map/ppermute | solution.py:206
  118.4 4.0 %collective-permute-start.11 = (bf16[32,64,128]{2,1,0:T(8,128)(2,1)}, bf16[32,64,128]{2,1,0:T(8,128)(2,1)S(1)}, u32[]{:S(2)}, u32[]{:S(2)}) collective-permute-start(bf16[32,64,128]{2,1,0:T(8,128)(2,1)} %collective-permute-done.8.rest_3_), channel_id=1, source_target_pairs={{0,4},{4,0},{1,5},{5,1},{2,6},{6,2},{3,7},{7,3},{8,12},{12,8},{9,1... | collective-permute-start | bytes 1572872 | tf_op jit(solution)/shard_map/ppermute | solution.py:206
  122.4 2.9 %collective-permute-done.6.rest_1_ = bf16[32,64,128]{2,1,0:T(8,128)(2,1)} collective-permute-done((bf16[32,64,128]{2,1,0:T(8,128)(2,1)S(1)}, bf16[32,64,128]{2,1,0:T(8,128)(2,1)}, u32[]{:S(2)}, u32[]{:S(2)}) %collective-permute-start.6) | collective-permute-done | bytes 524320 | tf_op jit(solution)/shard_map/ppermute | solution.py:283
  125.7 1.7 %update.1 = (f32[256,1024]{1,0:T(8,128)S(1)}, f32[8,128]{1,0:T(8,128)S(1)}, f32[4,512]{1,0:T(4,128)}, f32[4,512]{1,0:T(4,128)}, f32[4,512]{1,0:T(4,128)}, /*index=5*/f32[4,512]{1,0:T(4,128)}) custom-call(s32[3]{0:T(128)S(1)} %pad_add_fusion.at, f32[128,1,1152]{2,1,0:T(1,128)S(1)} %all-to-all-done.2.mine, f32[128,1,1152]{2,1,0:T(1,128)S(1)} %collective-permute-done.5.theirs, ...), custom_call_target="tpu_custom_call" | custom-call | tf_op jit(solution)/shard_map/update/pallas_call | solution.py:309
  127.5 11.9 %finish.1 = (f32[64,512]{1,0:T(8,128)}, f32[64,512]{1,0:T(8,128)}, f32[64,512]{1,0:T(8,128)}, f32[64,512]{1,0:T(8,128)}, bf16[4096,512]{1,0:T(8,128)(2,1)}, /*index=5*/bf16[4096,512]{1,0:T(8,128)(2,1)}) custom-call(s32[3]{0:T(128)S(1)} %pad_add_fusion.at, f32[8,128]{1,0:T(8,128)S(1)} %get-tuple-element.31.factor, f32[256,1024]{1,0:T(8,128)S(1)} %get-tuple-element.32.low, ...), custom_call_target="tpu_custom_call" | custom-call | tf_op jit(solution)/shard_map/finish/pallas_call | solution.py:216
  (25 shorter events, 1.2 us)
Async XLA Ops:
  7.2 120.3 %all-gather.3.cloned.1.call-start = ((), (), s32[]{:S(2)}) async-start(), calls=%async_computation.3 | async-start | bytes 10117120 | tf_op jit(solution)/shard_map/all_gather | solution.py:276
  9.8 28.8 %all-to-all-start = ((bf16[32,64,128]{2,1,0:T(8,128)(2,1)}), bf16[32,64,128]{2,1,0:T(8,128)(2,1)S(1)}, u32[]{:S(2)}, u32[]{:S(2)}) async-start(bf16[32,64,128]{2,1,0:T(8,128)(2,1)} %get-tuple-element.27), calls=%async_computation | async-start | bytes 1048576 | tf_op jit(solution)/shard_map/all_to_all | solution.py:279
  21.6 20.8 %collective-permute-start.3 = (bf16[256,1024]{1,0:T(8,128)(2,1)S(1)}, bf16[256,1024]{1,0:T(8,128)(2,1)S(1)}, u32[]{:S(2)}, u32[]{:S(2)}) collective-permute-start(bf16[256,1024]{1,0:T(8,128)(2,1)S(1)} %get-tuple-element.28.c0), channel_id=1, source_target_pairs={{0,3},{1,0},{2,1},{3,2},{4,7},{5,4},{6,5},{7,6},{8,11},{9,8},{10,9... | collective-permute-start | bytes 1572872 | tf_op jit(solution)/shard_map/ppermute | solution.py:277
  24.4 18.0 %collective-permute-start.2 = (bf16[256,1024]{1,0:T(8,128)(2,1)S(1)}, bf16[256,1024]{1,0:T(8,128)(2,1)S(1)}, u32[]{:S(2)}, u32[]{:S(2)}) collective-permute-start(bf16[256,1024]{1,0:T(8,128)(2,1)S(1)} %get-tuple-element.28.c0), channel_id=1, source_target_pairs={{0,2},{1,3},{2,0},{3,1},{4,6},{5,7},{6,4},{7,5},{8,10},{9,11},{10,... | collective-permute-start | bytes 1572872 | tf_op jit(solution)/shard_map/ppermute | solution.py:277
  24.8 26.2 %collective-permute-start.1 = (bf16[256,1024]{1,0:T(8,128)(2,1)S(1)}, bf16[256,1024]{1,0:T(8,128)(2,1)S(1)}, u32[]{:S(2)}, u32[]{:S(2)}) collective-permute-start(bf16[256,1024]{1,0:T(8,128)(2,1)S(1)} %get-tuple-element.28.c0), channel_id=1, source_target_pairs={{0,1},{1,2},{2,3},{3,0},{4,5},{5,6},{6,7},{7,4},{8,9},{9,10},{10,1... | collective-permute-start | bytes 1572872 | tf_op jit(solution)/shard_map/ppermute | solution.py:277
  38.6 55.0 %copy-start = (bf16[32,64,128]{2,1,0:T(8,128)(2,1)}, bf16[32,64,128]{2,1,0:T(8,128)(2,1)S(1)}, u32[]{:S(2)}) copy-start(bf16[32,64,128]{2,1,0:T(8,128)(2,1)S(1)} %all-to-all-done.mine.rest_0_) | copy-start | bytes 1572868
  38.6 13.3 %collective-permute-start = (bf16[32,64,128]{2,1,0:T(8,128)(2,1)S(1)}, bf16[32,64,128]{2,1,0:T(8,128)(2,1)S(1)}, u32[]{:S(2)}, u32[]{:S(2)}) collective-permute-start(bf16[32,64,128]{2,1,0:T(8,128)(2,1)S(1)} %all-to-all-done.mine.rest_0_), channel_id=1, source_target_pairs={{0,4},{4,0},{1,5},{5,1},{2,6},{6,2},{3,7},{7,3},{8,12},{12,8},{9,1... | collective-permute-start | bytes 1572872 | tf_op jit(solution)/shard_map/ppermute | solution.py:206
  51.0 0.8 copy-start.2
  51.8 1.0 copy-start.3
  52.9 6.6 %copy-start.1 = (bf16[32,64,128]{2,1,0:T(8,128)(2,1)}, bf16[32,64,128]{2,1,0:T(8,128)(2,1)S(1)}, u32[]{:S(2)}) copy-start(bf16[32,64,128]{2,1,0:T(8,128)(2,1)S(1)} %collective-permute-done.theirs.rest_4_) | copy-start | bytes 1572868
  57.6 1.7 %collective-permute-start.4 = (f16[32,32,128]{2,1,0:T(8,128)(2,1)S(1)}, f16[32,32,128]{2,1,0:T(8,128)(2,1)S(1)}, u32[]{:S(2)}, u32[]{:S(2)}) collective-permute-start(f16[32,32,128]{2,1,0:T(8,128)(2,1)S(1)} %convert_element_type.12), channel_id=1, source_target_pairs={{0,4},{4,0},{1,5},{5,1},{2,6},{6,2},{3,7},{7,3},{8,12},{12,8},{9,1... | collective-permute-start | bytes 786440 | tf_op jit(solution)/shard_map/ppermute | solution.py:206
  85.0 31.0 %all-to-all-start.2 = ((f32[128,1,1152]{2,1,0:T(1,128)}), f32[128,1,1152]{2,1,0:T(1,128)S(1)}, u32[]{:S(2)}, u32[]{:S(2)}) async-start(f32[128,1,1152]{2,1,0:T(1,128)} %spread.1), calls=%async_computation.2 | async-start | bytes 1179648 | tf_op jit(solution)/shard_map/all_to_all | solution.py:307
  91.2 27.2 %collective-permute-start.8 = (bf16[32,64,128]{2,1,0:T(8,128)(2,1)S(1)}, bf16[32,64,128]{2,1,0:T(8,128)(2,1)}, u32[]{:S(2)}, u32[]{:S(2)}) collective-permute-start(bf16[32,64,128]{2,1,0:T(8,128)(2,1)S(1)} %all-to-all-done.mine.rest_0_), channel_id=1, source_target_pairs={{0,3},{1,0},{2,1},{3,2},{4,7},{5,4},{6,5},{7,6},{8,11},{9,8},{10,9... | collective-permute-start | bytes 1572872 | tf_op jit(solution)/shard_map/ppermute | solution.py:283
  92.9 29.4 %collective-permute-start.7 = (bf16[32,64,128]{2,1,0:T(8,128)(2,1)S(1)}, bf16[32,64,128]{2,1,0:T(8,128)(2,1)}, u32[]{:S(2)}, u32[]{:S(2)}) collective-permute-start(bf16[32,64,128]{2,1,0:T(8,128)(2,1)S(1)} %all-to-all-done.mine.rest_0_), channel_id=1, source_target_pairs={{0,2},{1,3},{2,0},{3,1},{4,6},{5,7},{6,4},{7,5},{8,10},{9,11},{10,... | collective-permute-start | bytes 1572872 | tf_op jit(solution)/shard_map/ppermute | solution.py:283
  93.5 31.7 %collective-permute-start.6 = (bf16[32,64,128]{2,1,0:T(8,128)(2,1)S(1)}, bf16[32,64,128]{2,1,0:T(8,128)(2,1)}, u32[]{:S(2)}, u32[]{:S(2)}) collective-permute-start(bf16[32,64,128]{2,1,0:T(8,128)(2,1)S(1)} %all-to-all-done.mine.rest_0_), channel_id=1, source_target_pairs={{0,1},{1,2},{2,3},{3,0},{4,5},{5,6},{6,7},{7,4},{8,9},{9,10},{10,1... | collective-permute-start | bytes 1572872 | tf_op jit(solution)/shard_map/ppermute | solution.py:283
  115.9 9.8 %collective-permute-start.5 = (f32[128,1,1152]{2,1,0:T(1,128)S(1)}, f32[128,1,1152]{2,1,0:T(1,128)S(1)}, u32[]{:S(2)}, u32[]{:S(2)}) collective-permute-start(f32[128,1,1152]{2,1,0:T(1,128)S(1)} %all-to-all-done.2.mine), channel_id=1, source_target_pairs={{0,4},{4,0},{1,5},{5,1},{2,6},{6,2},{3,7},{7,3},{8,12},{12,8},{9,1... | collective-permute-start | bytes 1769480 | tf_op jit(solution)/shard_map/ppermute | solution.py:206
  118.4 9.1 %collective-permute-start.11 = (bf16[32,64,128]{2,1,0:T(8,128)(2,1)}, bf16[32,64,128]{2,1,0:T(8,128)(2,1)S(1)}, u32[]{:S(2)}, u32[]{:S(2)}) collective-permute-start(bf16[32,64,128]{2,1,0:T(8,128)(2,1)} %collective-permute-done.8.rest_3_), channel_id=1, source_target_pairs={{0,4},{4,0},{1,5},{5,1},{2,6},{6,2},{3,7},{7,3},{8,12},{12,8},{9,1... | collective-permute-start | bytes 1572872 | tf_op jit(solution)/shard_map/ppermute | solution.py:206
  122.4 5.1 %collective-permute-start.10 = (bf16[32,64,128]{2,1,0:T(8,128)(2,1)}, bf16[32,64,128]{2,1,0:T(8,128)(2,1)S(1)}, u32[]{:S(2)}, u32[]{:S(2)}) collective-permute-start(bf16[32,64,128]{2,1,0:T(8,128)(2,1)} %collective-permute-done.7.rest_2_), channel_id=1, source_target_pairs={{0,4},{4,0},{1,5},{5,1},{2,6},{6,2},{3,7},{7,3},{8,12},{12,8},{9,1... | collective-permute-start | bytes 1572872 | tf_op jit(solution)/shard_map/ppermute | solution.py:206
  125.2 2.3 %collective-permute-start.9 = (bf16[32,64,128]{2,1,0:T(8,128)(2,1)}, bf16[32,64,128]{2,1,0:T(8,128)(2,1)S(1)}, u32[]{:S(2)}, u32[]{:S(2)}) collective-permute-start(bf16[32,64,128]{2,1,0:T(8,128)(2,1)} %collective-permute-done.6.rest_1_), channel_id=1, source_target_pairs={{0,4},{4,0},{1,5},{5,1},{2,6},{6,2},{3,7},{7,3},{8,12},{12,8},{9,1... | collective-permute-start | bytes 1572872 | tf_op jit(solution)/shard_map/ppermute | solution.py:206
Sparse Core Ops, SparseCore 0:
  11.3 102.0 all-gather.2

commit v4 on v3

--- a/solution.py
+++ b/solution.py
@@ -44,7 +44,9 @@
     return jnp.exp(values * (REACH / top)), top
 
 
-def pack_kernel(at, qb, ob, qm, om, q1, q2, o1, o2, qc, oc, block, send, cot):
+def pack_kernel(at, qb, ob, qm, om, q1, q2, o1, o2, qc, oc, saved, block, send, cot, saved_near, sem):
+    staged = pltpu.make_async_copy(saved, saved_near, sem)
+    staged.start()
     tp = at[1]
     picked = []
     for basis in (qb, ob):
@@ -70,22 +72,20 @@
     block[TOPS_AT:, :] = tops.astype(bf16)
     cot[:, :512] = qc[...]
     cot[:, 512:] = oc[...]
-
-
-def project_kernel(at, saved, layer, mine, theirs, c0, c1, c2, c3, keep, give, saved_near, layer_near, sems):
-    copies = [
-        pltpu.make_async_copy(saved, saved_near, sems.at[0]),
-        pltpu.make_async_copy(layer, layer_near, sems.at[1]),
-    ]
-    for copy in copies:
-        copy.start()
+    staged.wait()
+
+
+def project_kernel(at, saved, layer, mine, theirs, c0, c1, c2, c3, keep, give, layer_near, sem):
+    staged = pltpu.make_async_copy(layer, layer_near, sem)
+    staged.start()
     core = at[0]
     own, other = mine[...], theirs[...]
     first = jnp.where(core == 0, own, other)
     second = jnp.where(core == 0, other, own)
     basis = jnp.concatenate([first, second], axis=1).reshape(D, 128)
-    for side, source in ((0, saved_near), (1, layer_near)):
-        copies[side].wait()
+    for side, source in ((0, saved), (1, layer_near)):
+        if side == 1:
+            staged.wait()
         coords = jnp.dot(source[...], basis, preferred_element_type=f32)[:, 64 * side : 64 * side + 64]
         high, low = high_and_low(coords.T)
         left = jnp.concatenate([high, low], axis=0).astype(bf16)
@@ -140,10 +140,23 @@
 
 
 def finish_kernel(
-    at, factor, low, qb, ob, qm, om, moments, block, tops, *rest
+    at, factor, low, qb, ob, qm, om, moments, gathered, tops, *rest
 ):
-    quarters, (qw, ow, qs, os, qc, oc, natural, direction) = rest[:8], rest[8:]
+    quarters, (qw, ow, qs, os, qc, oc, natural, direction, held_codes, sems) = rest[:8], rest[8:]
     core, tp = at[0], at[1]
+    step, steps = pl.program_id(0), 64 // GROUP
+
+    def fetch(i):
+        source = gathered.at[pl.ds(i * GROUP, GROUP), pl.ds(0, 128), :]
+        return pltpu.make_async_copy(source, held_codes.at[i % 2], sems.at[i % 2])
+
+    @pl.when(step == 0)
+    def _():
+        fetch(0).start()
+
+    @pl.when(step + 1 < steps)
+    def _():
+        fetch(step + 1).start()
 
     @pl.when(pl.program_id(0) == 0)
     def _():
@@ -168,7 +181,7 @@
                 natural[pl.ds(16 * i, 16), 512 * side : 512 * side + 512] = (first / jnp.sqrt(second)).astype(bf16)
             return carry
 
-        lax.fori_loop(0, 16, rows, 0)
+        lax.fori_loop(0, 16, rows, 0, unroll=4)
         for k in range(4):
             start = pl.multiple_of((tp + 4 - k) % 4 * 64, 64)
             direction[64 * k : 64 * k + 64, :] = natural[pl.ds(start, 64), :]
@@ -177,6 +190,8 @@
             step[...] = moved
             weight[...] = master[...] - rate * moved
 
+    fetch(step).wait()
+    block = held_codes.at[step % 2]
     bases = []
     for k in range(4):
         chips = pl.ds(pl.program_id(0) * (GROUP // 2), GROUP // 2)
@@ -225,14 +240,15 @@
             local,
             local,
             pl.BlockSpec((64, 16, 512), lambda i: (0, MOMENTS_AT // 16, 0)),
-            pl.BlockSpec((GROUP, 128, 512), lambda i: (i, 0, 0)),
+            pl.BlockSpec(memory_space=pl.ANY),
             pl.BlockSpec((64, 8, 512), lambda i: (0, TOPS_AT // 8, 0)),
             *[pl.BlockSpec((GROUP // 2, 64, 128), lambda i: (i, 0, 0))] * 5,
             *[VMEM] * 3,
         ],
         out_specs=[local] * 4 + [pl.BlockSpec((GROUP * 64, 512), lambda i: (i, 0))] * 2,
         out_shape=[shape((64, 512), f32)] * 4 + [shape((D, 512), bf16)] * 2,
-        scratch_shapes=[pltpu.VMEM((RANK, 1024), bf16)] * 2,
+        scratch_shapes=[pltpu.VMEM((RANK, 1024), bf16)] * 2
+        + [pltpu.VMEM((2, GROUP, 128, 512), bf16), pltpu.SemaphoreType.DMA((2,))],
         compiler_params=pltpu.CompilerParams(dimension_semantics=("arbitrary",), vmem_limit_bytes=40 * 2**20),
         name="finish",
     )(
@@ -261,17 +277,23 @@
     shape = jax.ShapeDtypeStruct
     at = jnp.stack([lax.axis_index("fs_2"), lax.axis_index("tp"), lax.axis_index(FS)]).astype(jnp.int32)
     moments = (query_first, query_second, output_first, output_second)
-    block, send, cot = pl.pallas_call(
+    block, send, cot, saved_near = pl.pallas_call(
         pack_kernel,
-        in_specs=[SMEM] + [VMEM] * 10,
-        out_specs=[VMEM] * 3,
-        out_shape=[shape((BLOCK_ROWS, 512), bf16), shape((32, 64, 128), bf16), shape((256, 1024), bf16)],
+        in_specs=[SMEM] + [VMEM] * 10 + [pl.BlockSpec(memory_space=pl.ANY)],
+        out_specs=[VMEM] * 4,
+        out_shape=[
+            shape((BLOCK_ROWS, 512), bf16),
+            shape((32, 64, 128), bf16),
+            shape((256, 1024), bf16),
+            pltpu.VMEM((256, D), bf16),
+        ],
+        scratch_shapes=[pltpu.SemaphoreType.DMA],
         compiler_params=pltpu.CompilerParams(vmem_limit_bytes=24 * 2**20),
         name="pack",
     )(
         at,
         *far(query_basis, output_basis, query_master, output_master, *moments),
-        *far(query_cotangent, mixed_heads),
+        *far(query_cotangent, mixed_heads, saved_input),
     )
     gathered = lax.all_gather(block, FS, axis=0, tiled=False)
     cots = [cot] + [lax.ppermute(cot, "tp", [(i, (i + k) % 4) for i in range(4)]) for k in (2, 1, 3)]
@@ -286,13 +308,13 @@
     quarters = owns + others
     keep, give = pl.pallas_call(
         project_kernel,
-        in_specs=[SMEM] + [pl.BlockSpec(memory_space=pl.ANY)] * 2 + [VMEM] * 6,
+        in_specs=[SMEM, VMEM, pl.BlockSpec(memory_space=pl.ANY)] + [VMEM] * 6,
         out_specs=[VMEM] * 2,
-        scratch_shapes=[pltpu.VMEM((256, D), bf16)] * 2 + [pltpu.SemaphoreType.DMA((2,))],
+        scratch_shapes=[pltpu.VMEM((256, D), bf16), pltpu.SemaphoreType.DMA],
         out_shape=[pltpu.VMEM((32, 32, 128), f32)] * 2,
         compiler_params=pltpu.CompilerParams(vmem_limit_bytes=20 * 2**20),
         name="project",
-    )(at, *far(saved_input, layer_cotangent), *near(mine, theirs, *cots))
+    )(at, *near(saved_near), *far(layer_cotangent), *near(mine, theirs, *cots))
     pair = (keep + swapped(give.astype(f16)).astype(f32)).astype(f16)
     arrived = lax.all_to_all(pair, CHIPS, 0, 0, tiled=True)
     row = jnp.sum(arrived.astype(f32), axis=0)

time: 147 us -> 149 us (1.014)
  local copies, waits for them, and re-layouts: 1.84 us -> 4.94 us
  starting transfers between devices: 36.2 us -> 38.1 us
  waiting for transfers between devices: 47.6 us -> 45.9 us
    unnamed x8 -> x12, local copies, waits for them, and re-layouts: 1.84 us -> 4.94 us
    all_to_all x1, waiting for transfers between devices: 21.9 us -> 19.9 us  [per_device(): mine = lax.all_to_all(out, (*CHIPS, 'tp'), 0, 0, tiled=True)]
    ppermute x6, starting transfers between devices: 11.3 us -> 13.1 us  [swapped(): return lax.ppermute(values, 'fs_2', [(0, 1), (1, 0)])]
  transfers between devices with their start and end apart: 15 -> 15, of which waited for: 5 -> 5; matrix products, arithmetic and copies ran while one was open for 0% -> 0% of each run, Pallas kernels for 5% -> 4%
where the time goes in v4:
time: 149 us
  waiting for transfers between devices  45.9 us (31%)
  starting transfers between devices  38.1 us (26%)
  blocking collectives  23.8 us (16%)
  Pallas kernels  21.7 us (15%)
  between operations  14.2 us (10%)
  local copies, waits for them, and re-layouts  4.94 us (3%)
    all_to_all x1, blocking collectives, per_device(): arrived = lax.all_to_all(pair, CHIPS, 0, 0, tiled=True)  23.8 us
    all_to_all x1, waiting for transfers between devices, per_device(): mine = lax.all_to_all(out, (*CHIPS, 'tp'), 0, 0, tiled=True)  19.9 us
    all_to_all x1, waiting for transfers between devices, per_device(): mine = lax.all_to_all(send, CHIPS, 0, 0, tiled=True)  13.4 us
    ppermute x6, starting transfers between devices, swapped(): return lax.ppermute(values, 'fs_2', [(0, 1), (1, 0)])  13.1 us
    all_to_all x1, starting transfers between devices, per_device(): mine = lax.all_to_all(send, CHIPS, 0, 0, tiled=True)  11.9 us
    pallas_call x1, Pallas kernels, finished(): pl.pallas_call(finish_kernel, grid=(64 // GROUP,), in_specs=[SMEM, whole(...  11.3 us
    ppermute x3, waiting for transfers between devices, per_device(): lax.ppermute(cot, 'tp', [(i, (i + k) % 4) for i in range(4)])  8.41 us
    all_to_all x1, starting transfers between devices, per_device(): mine = lax.all_to_all(out, (*CHIPS, 'tp'), 0, 0, tiled=True)  6.23 us
  transfers between devices with their start and end apart: 15, of which 5 were waited for; matrix products, arithmetic and copies ran while one was open for 0% of the time, Pallas kernels for 4%

profile of v4, /device:TPU:1, one launch (start us, length us, event | category | flops | bytes accessed | tf_op | source)
XLA Modules:
  0.0 148.9 jit_solution(18438847472502204384)
XLA Ops:
  7.3 3.7 %pack.1 = (bf16[152,512]{1,0:T(8,128)(2,1)}, bf16[32,64,128]{2,1,0:T(8,128)(2,1)}, bf16[256,1024]{1,0:T(8,128)(2,1)S(1)}, bf16[256,4096]{1,0:T(8,128)(2,1)S(1)}) custom-call(s32[3]{0:T(128)S(1)} %pad_add_fusion.at, bf16[64,256]{1,0:T(8,128)(2,1)} %qb.3, bf16[64,256]{1,0:T(8,128)(2,1)} %ob.3, f32[64,512]{1,0:T(8,128)} %qm.3, f32[64,512]{1,0:T(8,128)} %om.3, ...), custom_call_target="tpu_custom_call" | custom-call | tf_op jit(solution)/shard_map/pack/pallas_call | solution.py:280
  11.0 1.3 copy-done.2
  12.4 11.9 %all-to-all-start = ((bf16[32,64,128]{2,1,0:T(8,128)(2,1)}), bf16[32,64,128]{2,1,0:T(8,128)(2,1)S(1)}, u32[]{:S(2)}, u32[]{:S(2)}) async-start(bf16[32,64,128]{2,1,0:T(8,128)(2,1)} %get-tuple-element.29), calls=%async_computation | async-start | bytes 1048576 | tf_op jit(solution)/shard_map/all_to_all | solution.py:301
  24.3 2.8 %collective-permute-start.3 = (bf16[256,1024]{1,0:T(8,128)(2,1)S(1)}, bf16[256,1024]{1,0:T(8,128)(2,1)S(1)}, u32[]{:S(2)}, u32[]{:S(2)}) collective-permute-start(bf16[256,1024]{1,0:T(8,128)(2,1)S(1)} %get-tuple-element.30.c0), channel_id=1, source_target_pairs={{0,3},{1,0},{2,1},{3,2},{4,7},{5,4},{6,5},{7,6},{8,11},{9,8},{10,9... | collective-permute-start | bytes 1572872 | tf_op jit(solution)/shard_map/ppermute | solution.py:299
  27.4 0.7 collective-permute-start.1
  28.1 13.4 %all-to-all-done.mine.rest_0_ = bf16[32,64,128]{2,1,0:T(8,128)(2,1)S(1)} async-done(((bf16[32,64,128]{2,1,0:T(8,128)(2,1)}), bf16[32,64,128]{2,1,0:T(8,128)(2,1)S(1)}, u32[]{:S(2)}, u32[]{:S(2)}) %all-to-all-start) | async-done | bytes 524320 | tf_op jit(solution)/shard_map/all_to_all | solution.py:301
  41.5 3.8 %collective-permute-start = (bf16[32,64,128]{2,1,0:T(8,128)(2,1)S(1)}, bf16[32,64,128]{2,1,0:T(8,128)(2,1)S(1)}, u32[]{:S(2)}, u32[]{:S(2)}) collective-permute-start(bf16[32,64,128]{2,1,0:T(8,128)(2,1)S(1)} %all-to-all-done.mine.rest_0_), channel_id=1, source_target_pairs={{0,4},{4,0},{1,5},{5,1},{2,6},{6,2},{3,7},{7,3},{8,12},{12,8},{9,1... | collective-permute-start | bytes 1572872 | tf_op jit(solution)/shard_map/ppermute | solution.py:221
  45.3 8.4 %collective-permute-done.1.c1 = bf16[256,1024]{1,0:T(8,128)(2,1)S(1)} collective-permute-done((bf16[256,1024]{1,0:T(8,128)(2,1)S(1)}, bf16[256,1024]{1,0:T(8,128)(2,1)S(1)}, u32[]{:S(2)}, u32[]{:S(2)}) %collective-permute-start.1) | collective-permute-done | bytes 524320 | tf_op jit(solution)/shard_map/ppermute | solution.py:299
  53.7 0.8 copy-done.4
  54.5 1.8 %copy-done.3 = bf16[256,4096]{1,0:T(8,128)(2,1)S(1)} copy-done((bf16[256,4096]{1,0:T(8,128)(2,1)S(1)}, bf16[256,4096]{1,0:T(8,128)(2,1)}, u32[]{:S(2)}) %copy-start.3) | copy-done | bytes 2097176
  56.3 1.0 copy-done.5
  57.3 3.4 %project.1 = (f32[32,32,128]{2,1,0:T(8,128)S(1)}, f32[32,32,128]{2,1,0:T(8,128)S(1)}) custom-call(s32[3]{0:T(128)S(1)} %pad_add_fusion.at, bf16[256,4096]{1,0:T(8,128)(2,1)S(1)} %copy-done.3, bf16[256,4096]{1,0:T(8,128)(2,1)} %layer.1, bf16[32,64,128]{2,1,0:T(8,128)(2,1)S(1)} %all-to-all-done.mine.rest_0_, ...), custom_call_target="tpu_custom_call" | custom-call | tf_op jit(solution)/shard_map/project/pallas_call | solution.py:309
  61.3 1.2 collective-permute-done.4
  62.6 23.8 %all_to_all.15 = f16[32,32,128]{2,1,0:T(8,128)(2,1)S(1)} all-to-all(f16[32,32,128]{2,1,0:T(8,128)(2,1)S(1)} %add_convert_fusion), channel_id=1, replica_groups=mesh['fs_0'=8,'fs_1'=4,'fs_2'=2,'tp'=4] {'fs_0','fs_1'}, dimensions={0} | all-to-all | bytes 524288 | tf_op jit(solution)/shard_map/all_to_all | solution.py:319
  86.5 1.5 %spread.1 = f32[128,1,1152]{2,1,0:T(1,128)} custom-call(s32[3]{0:T(128)S(1)} %pad_add_fusion.at, f32[32,128]{1,0:T(8,128)S(1)} %convert_reduce_fusion.row), custom_call_target="tpu_custom_call" | custom-call | tf_op jit(solution)/shard_map/spread/pallas_call | solution.py:321
  88.0 6.2 %all-to-all-start.2 = ((f32[128,1,1152]{2,1,0:T(1,128)}), f32[128,1,1152]{2,1,0:T(1,128)S(1)}, u32[]{:S(2)}, u32[]{:S(2)}) async-start(f32[128,1,1152]{2,1,0:T(1,128)} %spread.1), calls=%async_computation.2 | async-start | bytes 1179648 | tf_op jit(solution)/shard_map/all_to_all | solution.py:329
  94.3 1.9 %collective-permute-start.8 = (bf16[32,64,128]{2,1,0:T(8,128)(2,1)S(1)}, bf16[32,64,128]{2,1,0:T(8,128)(2,1)}, u32[]{:S(2)}, u32[]{:S(2)}) collective-permute-start(bf16[32,64,128]{2,1,0:T(8,128)(2,1)S(1)} %all-to-all-done.mine.rest_0_), channel_id=1, source_target_pairs={{0,3},{1,0},{2,1},{3,2},{4,7},{5,4},{6,5},{7,6},{8,11},{9,8},{10,9... | collective-permute-start | bytes 1572872 | tf_op jit(solution)/shard_map/ppermute | solution.py:305
  96.7 0.6 collective-permute-start.6
  97.3 19.9 %all-to-all-done.2.mine = f32[128,1,1152]{2,1,0:T(1,128)S(1)} async-done(((f32[128,1,1152]{2,1,0:T(1,128)}), f32[128,1,1152]{2,1,0:T(1,128)S(1)}, u32[]{:S(2)}, u32[]{:S(2)}) %all-to-all-start.2) | async-done | bytes 589856 | tf_op jit(solution)/shard_map/all_to_all | solution.py:329
  117.2 2.2 %collective-permute-start.5 = (f32[128,1,1152]{2,1,0:T(1,128)S(1)}, f32[128,1,1152]{2,1,0:T(1,128)S(1)}, u32[]{:S(2)}, u32[]{:S(2)}) collective-permute-start(f32[128,1,1152]{2,1,0:T(1,128)S(1)} %all-to-all-done.2.mine), channel_id=1, source_target_pairs={{0,4},{4,0},{1,5},{5,1},{2,6},{6,2},{3,7},{7,3},{8,12},{12,8},{9,1... | collective-permute-start | bytes 1769480 | tf_op jit(solution)/shard_map/ppermute | solution.py:221
  119.4 6.1 %collective-permute-start.11 = (bf16[32,64,128]{2,1,0:T(8,128)(2,1)}, bf16[32,64,128]{2,1,0:T(8,128)(2,1)S(1)}, u32[]{:S(2)}, u32[]{:S(2)}) collective-permute-start(bf16[32,64,128]{2,1,0:T(8,128)(2,1)} %collective-permute-done.8.rest_3_), channel_id=1, source_target_pairs={{0,4},{4,0},{1,5},{5,1},{2,6},{6,2},{3,7},{7,3},{8,12},{12,8},{9,1... | collective-permute-start | bytes 1572872 | tf_op jit(solution)/shard_map/ppermute | solution.py:221
  125.6 2.9 %collective-permute-done.6.rest_1_ = bf16[32,64,128]{2,1,0:T(8,128)(2,1)} collective-permute-done((bf16[32,64,128]{2,1,0:T(8,128)(2,1)S(1)}, bf16[32,64,128]{2,1,0:T(8,128)(2,1)}, u32[]{:S(2)}, u32[]{:S(2)}) %collective-permute-start.6) | collective-permute-done | bytes 524320 | tf_op jit(solution)/shard_map/ppermute | solution.py:305
  128.9 1.7 %update.1 = (f32[256,1024]{1,0:T(8,128)S(1)}, f32[8,128]{1,0:T(8,128)S(1)}, f32[4,512]{1,0:T(4,128)}, f32[4,512]{1,0:T(4,128)}, f32[4,512]{1,0:T(4,128)}, /*index=5*/f32[4,512]{1,0:T(4,128)}) custom-call(s32[3]{0:T(128)S(1)} %pad_add_fusion.at, f32[128,1,1152]{2,1,0:T(1,128)S(1)} %all-to-all-done.2.mine, f32[128,1,1152]{2,1,0:T(1,128)S(1)} %collective-permute-done.5.theirs, ...), custom_call_target="tpu_custom_call" | custom-call | tf_op jit(solution)/shard_map/update/pallas_call | solution.py:331
  130.7 11.3 %finish.1 = (f32[64,512]{1,0:T(8,128)}, f32[64,512]{1,0:T(8,128)}, f32[64,512]{1,0:T(8,128)}, f32[64,512]{1,0:T(8,128)}, bf16[4096,512]{1,0:T(8,128)(2,1)}, /*index=5*/bf16[4096,512]{1,0:T(8,128)(2,1)}) custom-call(s32[3]{0:T(128)S(1)} %pad_add_fusion.at, f32[8,128]{1,0:T(8,128)S(1)} %get-tuple-element.33.factor, f32[256,1024]{1,0:T(8,128)S(1)} %get-tuple-element.34.low, ...), custom_call_target="tpu_custom_call" | custom-call | tf_op jit(solution)/shard_map/finish/pallas_call | solution.py:231
  (29 shorter events, 2.3 us)
Async XLA Ops:
  7.2 123.5 %all-gather.3.cloned.1.call-start = ((), (), s32[]{:S(2)}) async-start(), calls=%async_computation.3 | async-start | bytes 10117120 | tf_op jit(solution)/shard_map/all_gather | solution.py:298
  11.0 1.3 copy-start.2
  12.4 29.2 %all-to-all-start = ((bf16[32,64,128]{2,1,0:T(8,128)(2,1)}), bf16[32,64,128]{2,1,0:T(8,128)(2,1)S(1)}, u32[]{:S(2)}, u32[]{:S(2)}) async-start(bf16[32,64,128]{2,1,0:T(8,128)(2,1)} %get-tuple-element.29), calls=%async_computation | async-start | bytes 1048576 | tf_op jit(solution)/shard_map/all_to_all | solution.py:301
  24.3 21.1 %collective-permute-start.3 = (bf16[256,1024]{1,0:T(8,128)(2,1)S(1)}, bf16[256,1024]{1,0:T(8,128)(2,1)S(1)}, u32[]{:S(2)}, u32[]{:S(2)}) collective-permute-start(bf16[256,1024]{1,0:T(8,128)(2,1)S(1)} %get-tuple-element.30.c0), channel_id=1, source_target_pairs={{0,3},{1,0},{2,1},{3,2},{4,7},{5,4},{6,5},{7,6},{8,11},{9,8},{10,9... | collective-permute-start | bytes 1572872 | tf_op jit(solution)/shard_map/ppermute | solution.py:299
  27.1 18.2 %collective-permute-start.2 = (bf16[256,1024]{1,0:T(8,128)(2,1)S(1)}, bf16[256,1024]{1,0:T(8,128)(2,1)S(1)}, u32[]{:S(2)}, u32[]{:S(2)}) collective-permute-start(bf16[256,1024]{1,0:T(8,128)(2,1)S(1)} %get-tuple-element.30.c0), channel_id=1, source_target_pairs={{0,2},{1,3},{2,0},{3,1},{4,6},{5,7},{6,4},{7,5},{8,10},{9,11},{10,... | collective-permute-start | bytes 1572872 | tf_op jit(solution)/shard_map/ppermute | solution.py:299
  27.4 26.3 %collective-permute-start.1 = (bf16[256,1024]{1,0:T(8,128)(2,1)S(1)}, bf16[256,1024]{1,0:T(8,128)(2,1)S(1)}, u32[]{:S(2)}, u32[]{:S(2)}) collective-permute-start(bf16[256,1024]{1,0:T(8,128)(2,1)S(1)} %get-tuple-element.30.c0), channel_id=1, source_target_pairs={{0,1},{1,2},{2,3},{3,0},{4,5},{5,6},{6,7},{7,4},{8,9},{9,10},{10,1... | collective-permute-start | bytes 1572872 | tf_op jit(solution)/shard_map/ppermute | solution.py:299
  41.5 55.2 %copy-start = (bf16[32,64,128]{2,1,0:T(8,128)(2,1)}, bf16[32,64,128]{2,1,0:T(8,128)(2,1)S(1)}, u32[]{:S(2)}) copy-start(bf16[32,64,128]{2,1,0:T(8,128)(2,1)S(1)} %all-to-all-done.mine.rest_0_) | copy-start | bytes 1572868
  41.5 13.0 %collective-permute-start = (bf16[32,64,128]{2,1,0:T(8,128)(2,1)S(1)}, bf16[32,64,128]{2,1,0:T(8,128)(2,1)S(1)}, u32[]{:S(2)}, u32[]{:S(2)}) collective-permute-start(bf16[32,64,128]{2,1,0:T(8,128)(2,1)S(1)} %all-to-all-done.mine.rest_0_), channel_id=1, source_target_pairs={{0,4},{4,0},{1,5},{5,1},{2,6},{6,2},{3,7},{7,3},{8,12},{12,8},{9,1... | collective-permute-start | bytes 1572872 | tf_op jit(solution)/shard_map/ppermute | solution.py:221
  53.7 0.8 copy-start.4
  54.5 8.1 %copy-start.1 = (bf16[32,64,128]{2,1,0:T(8,128)(2,1)}, bf16[32,64,128]{2,1,0:T(8,128)(2,1)S(1)}, u32[]{:S(2)}) copy-start(bf16[32,64,128]{2,1,0:T(8,128)(2,1)S(1)} %collective-permute-done.theirs.rest_4_) | copy-start | bytes 1572868
  54.5 1.8 %copy-start.3 = (bf16[256,4096]{1,0:T(8,128)(2,1)S(1)}, bf16[256,4096]{1,0:T(8,128)(2,1)}, u32[]{:S(2)}) copy-start(bf16[256,4096]{1,0:T(8,128)(2,1)} %copy-done.2) | copy-start | bytes 6291460
  56.3 1.0 copy-start.5
  60.8 1.7 %collective-permute-start.4 = (f16[32,32,128]{2,1,0:T(8,128)(2,1)S(1)}, f16[32,32,128]{2,1,0:T(8,128)(2,1)S(1)}, u32[]{:S(2)}, u32[]{:S(2)}) collective-permute-start(f16[32,32,128]{2,1,0:T(8,128)(2,1)S(1)} %convert_element_type.12), channel_id=1, source_target_pairs={{0,4},{4,0},{1,5},{5,1},{2,6},{6,2},{3,7},{7,3},{8,12},{12,8},{9,1... | collective-permute-start | bytes 786440 | tf_op jit(solution)/shard_map/ppermute | solution.py:221
  88.0 29.2 %all-to-all-start.2 = ((f32[128,1,1152]{2,1,0:T(1,128)}), f32[128,1,1152]{2,1,0:T(1,128)S(1)}, u32[]{:S(2)}, u32[]{:S(2)}) async-start(f32[128,1,1152]{2,1,0:T(1,128)} %spread.1), calls=%async_computation.2 | async-start | bytes 1179648 | tf_op jit(solution)/shard_map/all_to_all | solution.py:329
  94.3 25.2 %collective-permute-start.8 = (bf16[32,64,128]{2,1,0:T(8,128)(2,1)S(1)}, bf16[32,64,128]{2,1,0:T(8,128)(2,1)}, u32[]{:S(2)}, u32[]{:S(2)}) collective-permute-start(bf16[32,64,128]{2,1,0:T(8,128)(2,1)S(1)} %all-to-all-done.mine.rest_0_), channel_id=1, source_target_pairs={{0,3},{1,0},{2,1},{3,2},{4,7},{5,4},{6,5},{7,6},{8,11},{9,8},{10,9... | collective-permute-start | bytes 1572872 | tf_op jit(solution)/shard_map/ppermute | solution.py:305
  96.1 29.4 %collective-permute-start.7 = (bf16[32,64,128]{2,1,0:T(8,128)(2,1)S(1)}, bf16[32,64,128]{2,1,0:T(8,128)(2,1)}, u32[]{:S(2)}, u32[]{:S(2)}) collective-permute-start(bf16[32,64,128]{2,1,0:T(8,128)(2,1)S(1)} %all-to-all-done.mine.rest_0_), channel_id=1, source_target_pairs={{0,2},{1,3},{2,0},{3,1},{4,6},{5,7},{6,4},{7,5},{8,10},{9,11},{10,... | collective-permute-start | bytes 1572872 | tf_op jit(solution)/shard_map/ppermute | solution.py:305
  96.7 31.7 %collective-permute-start.6 = (bf16[32,64,128]{2,1,0:T(8,128)(2,1)S(1)}, bf16[32,64,128]{2,1,0:T(8,128)(2,1)}, u32[]{:S(2)}, u32[]{:S(2)}) collective-permute-start(bf16[32,64,128]{2,1,0:T(8,128)(2,1)S(1)} %all-to-all-done.mine.rest_0_), channel_id=1, source_target_pairs={{0,1},{1,2},{2,3},{3,0},{4,5},{5,6},{6,7},{7,4},{8,9},{9,10},{10,1... | collective-permute-start | bytes 1572872 | tf_op jit(solution)/shard_map/ppermute | solution.py:305
  117.2 11.7 %collective-permute-start.5 = (f32[128,1,1152]{2,1,0:T(1,128)S(1)}, f32[128,1,1152]{2,1,0:T(1,128)S(1)}, u32[]{:S(2)}, u32[]{:S(2)}) collective-permute-start(f32[128,1,1152]{2,1,0:T(1,128)S(1)} %all-to-all-done.2.mine), channel_id=1, source_target_pairs={{0,4},{4,0},{1,5},{5,1},{2,6},{6,2},{3,7},{7,3},{8,12},{12,8},{9,1... | collective-permute-start | bytes 1769480 | tf_op jit(solution)/shard_map/ppermute | solution.py:221
  119.4 11.2 %collective-permute-start.11 = (bf16[32,64,128]{2,1,0:T(8,128)(2,1)}, bf16[32,64,128]{2,1,0:T(8,128)(2,1)S(1)}, u32[]{:S(2)}, u32[]{:S(2)}) collective-permute-start(bf16[32,64,128]{2,1,0:T(8,128)(2,1)} %collective-permute-done.8.rest_3_), channel_id=1, source_target_pairs={{0,4},{4,0},{1,5},{5,1},{2,6},{6,2},{3,7},{7,3},{8,12},{12,8},{9,1... | collective-permute-start | bytes 1572872 | tf_op jit(solution)/shard_map/ppermute | solution.py:221
  125.5 5.1 %collective-permute-start.10 = (bf16[32,64,128]{2,1,0:T(8,128)(2,1)}, bf16[32,64,128]{2,1,0:T(8,128)(2,1)S(1)}, u32[]{:S(2)}, u32[]{:S(2)}) collective-permute-start(bf16[32,64,128]{2,1,0:T(8,128)(2,1)} %collective-permute-done.7.rest_2_), channel_id=1, source_target_pairs={{0,4},{4,0},{1,5},{5,1},{2,6},{6,2},{3,7},{7,3},{8,12},{12,8},{9,1... | collective-permute-start | bytes 1572872 | tf_op jit(solution)/shard_map/ppermute | solution.py:221
  128.4 2.2 %collective-permute-start.9 = (bf16[32,64,128]{2,1,0:T(8,128)(2,1)}, bf16[32,64,128]{2,1,0:T(8,128)(2,1)S(1)}, u32[]{:S(2)}, u32[]{:S(2)}) collective-permute-start(bf16[32,64,128]{2,1,0:T(8,128)(2,1)} %collective-permute-done.6.rest_1_), channel_id=1, source_target_pairs={{0,4},{4,0},{1,5},{5,1},{2,6},{6,2},{3,7},{7,3},{8,12},{12,8},{9,1... | collective-permute-start | bytes 1572872 | tf_op jit(solution)/shard_map/ppermute | solution.py:221
Sparse Core Ops, SparseCore 0:
  12.5 102.2 all-gather.2

commit v5 on v3

--- a/solution.py
+++ b/solution.py
@@ -140,10 +140,23 @@
 
 
 def finish_kernel(
-    at, factor, low, qb, ob, qm, om, moments, block, tops, *rest
+    at, factor, low, qb, ob, qm, om, moments, gathered, tops, *rest
 ):
-    quarters, (qw, ow, qs, os, qc, oc, natural, direction) = rest[:8], rest[8:]
+    quarters, (qw, ow, qs, os, qc, oc, natural, direction, held_codes, sems) = rest[:8], rest[8:]
     core, tp = at[0], at[1]
+    step, steps = pl.program_id(0), 64 // GROUP
+
+    def fetch(i):
+        source = gathered.at[pl.ds(i * GROUP, GROUP), pl.ds(0, 128), :]
+        return pltpu.make_async_copy(source, held_codes.at[i % 2], sems.at[i % 2])
+
+    @pl.when(step == 0)
+    def _():
+        fetch(0).start()
+
+    @pl.when(step + 1 < steps)
+    def _():
+        fetch(step + 1).start()
 
     @pl.when(pl.program_id(0) == 0)
     def _():
@@ -168,7 +181,7 @@
                 natural[pl.ds(16 * i, 16), 512 * side : 512 * side + 512] = (first / jnp.sqrt(second)).astype(bf16)
             return carry
 
-        lax.fori_loop(0, 16, rows, 0)
+        lax.fori_loop(0, 16, rows, 0, unroll=4)
         for k in range(4):
             start = pl.multiple_of((tp + 4 - k) % 4 * 64, 64)
             direction[64 * k : 64 * k + 64, :] = natural[pl.ds(start, 64), :]
@@ -177,6 +190,8 @@
             step[...] = moved
             weight[...] = master[...] - rate * moved
 
+    fetch(step).wait()
+    block = held_codes.at[step % 2]
     bases = []
     for k in range(4):
         chips = pl.ds(pl.program_id(0) * (GROUP // 2), GROUP // 2)
@@ -225,14 +240,15 @@
             local,
             local,
             pl.BlockSpec((64, 16, 512), lambda i: (0, MOMENTS_AT // 16, 0)),
-            pl.BlockSpec((GROUP, 128, 512), lambda i: (i, 0, 0)),
+            pl.BlockSpec(memory_space=pl.ANY),
             pl.BlockSpec((64, 8, 512), lambda i: (0, TOPS_AT // 8, 0)),
             *[pl.BlockSpec((GROUP // 2, 64, 128), lambda i: (i, 0, 0))] * 5,
             *[VMEM] * 3,
         ],
         out_specs=[local] * 4 + [pl.BlockSpec((GROUP * 64, 512), lambda i: (i, 0))] * 2,
         out_shape=[shape((64, 512), f32)] * 4 + [shape((D, 512), bf16)] * 2,
-        scratch_shapes=[pltpu.VMEM((RANK, 1024), bf16)] * 2,
+        scratch_shapes=[pltpu.VMEM((RANK, 1024), bf16)] * 2
+        + [pltpu.VMEM((2, GROUP, 128, 512), bf16), pltpu.SemaphoreType.DMA((2,))],
         compiler_params=pltpu.CompilerParams(dimension_semantics=("arbitrary",), vmem_limit_bytes=40 * 2**20),
         name="finish",
     )(

time: 147 us -> 146 us (level)
  no operation moved by 1% of the time
where the time goes in v5:
time: 146 us
  waiting for transfers between devices  47.6 us (33%)
  starting transfers between devices  36.2 us (25%)
  blocking collectives  24 us (16%)
  Pallas kernels  21.6 us (15%)
  between operations  14.1 us (10%)
  local copies, waits for them, and re-layouts  1.84 us (1%)
    all_to_all x1, blocking collectives, per_device(): arrived = lax.all_to_all(pair, CHIPS, 0, 0, tiled=True)  24 us
    all_to_all x1, waiting for transfers between devices, per_device(): mine = lax.all_to_all(out, (*CHIPS, 'tp'), 0, 0, tiled=True)  21.9 us
    all_to_all x1, waiting for transfers between devices, per_device(): mine = lax.all_to_all(send, CHIPS, 0, 0, tiled=True)  13.1 us
    all_to_all x1, starting transfers between devices, per_device(): mine = lax.all_to_all(send, CHIPS, 0, 0, tiled=True)  11.9 us
    ppermute x6, starting transfers between devices, swapped(): return lax.ppermute(values, 'fs_2', [(0, 1), (1, 0)])  11.3 us
    pallas_call x1, Pallas kernels, finished(): pl.pallas_call(finish_kernel, grid=(64 // GROUP,), in_specs=[SMEM, whole(...  11.3 us
    ppermute x3, waiting for transfers between devices, per_device(): lax.ppermute(cot, 'tp', [(i, (i + k) % 4) for i in range(4)])  8.62 us
    all_to_all x1, starting transfers between devices, per_device(): mine = lax.all_to_all(out, (*CHIPS, 'tp'), 0, 0, tiled=True)  6.18 us
  transfers between devices with their start and end apart: 15, of which 5 were waited for; matrix products, arithmetic and copies ran while one was open for 0% of the time, Pallas kernels for 5%

profile of v5, /device:TPU:1, one launch (start us, length us, event | category | flops | bytes accessed | tf_op | source)
XLA Modules:
  0.0 145.7 jit_solution(16735740235046184173)
XLA Ops:
  7.3 2.4 %pack.1 = (bf16[152,512]{1,0:T(8,128)(2,1)}, bf16[32,64,128]{2,1,0:T(8,128)(2,1)}, bf16[256,1024]{1,0:T(8,128)(2,1)S(1)}) custom-call(s32[3]{0:T(128)S(1)} %pad_add_fusion.at, bf16[64,256]{1,0:T(8,128)(2,1)} %qb.3, bf16[64,256]{1,0:T(8,128)(2,1)} %ob.3, f32[64,512]{1,0:T(8,128)} %qm.3, f32[64,512]{1,0:T(8,128)} %om.3, f32[4,512]{1,0:T(4,128)} %q1.3, ...), custom_call_target="tpu_custom_call" | custom-call | tf_op jit(solution)/shard_map/pack/pallas_call | solution.py:280
  9.8 11.9 %all-to-all-start = ((bf16[32,64,128]{2,1,0:T(8,128)(2,1)}), bf16[32,64,128]{2,1,0:T(8,128)(2,1)S(1)}, u32[]{:S(2)}, u32[]{:S(2)}) async-start(bf16[32,64,128]{2,1,0:T(8,128)(2,1)} %get-tuple-element.27), calls=%async_computation | async-start | bytes 1048576 | tf_op jit(solution)/shard_map/all_to_all | solution.py:295
  21.6 2.8 %collective-permute-start.3 = (bf16[256,1024]{1,0:T(8,128)(2,1)S(1)}, bf16[256,1024]{1,0:T(8,128)(2,1)S(1)}, u32[]{:S(2)}, u32[]{:S(2)}) collective-permute-start(bf16[256,1024]{1,0:T(8,128)(2,1)S(1)} %get-tuple-element.28.c0), channel_id=1, source_target_pairs={{0,3},{1,0},{2,1},{3,2},{4,7},{5,4},{6,5},{7,6},{8,11},{9,8},{10,9... | collective-permute-start | bytes 1572872 | tf_op jit(solution)/shard_map/ppermute | solution.py:293
  24.8 0.7 collective-permute-start.1
  25.5 13.1 %all-to-all-done.mine.rest_0_ = bf16[32,64,128]{2,1,0:T(8,128)(2,1)S(1)} async-done(((bf16[32,64,128]{2,1,0:T(8,128)(2,1)}), bf16[32,64,128]{2,1,0:T(8,128)(2,1)S(1)}, u32[]{:S(2)}, u32[]{:S(2)}) %all-to-all-start) | async-done | bytes 524320 | tf_op jit(solution)/shard_map/all_to_all | solution.py:295
  38.6 3.9 %collective-permute-start = (bf16[32,64,128]{2,1,0:T(8,128)(2,1)S(1)}, bf16[32,64,128]{2,1,0:T(8,128)(2,1)S(1)}, u32[]{:S(2)}, u32[]{:S(2)}) collective-permute-start(bf16[32,64,128]{2,1,0:T(8,128)(2,1)S(1)} %all-to-all-done.mine.rest_0_), channel_id=1, source_target_pairs={{0,4},{4,0},{1,5},{5,1},{2,6},{6,2},{3,7},{7,3},{8,12},{12,8},{9,1... | collective-permute-start | bytes 1572872 | tf_op jit(solution)/shard_map/ppermute | solution.py:221
  42.4 8.6 %collective-permute-done.1.c1 = bf16[256,1024]{1,0:T(8,128)(2,1)S(1)} collective-permute-done((bf16[256,1024]{1,0:T(8,128)(2,1)S(1)}, bf16[256,1024]{1,0:T(8,128)(2,1)S(1)}, u32[]{:S(2)}, u32[]{:S(2)}) %collective-permute-start.1) | collective-permute-done | bytes 524320 | tf_op jit(solution)/shard_map/ppermute | solution.py:293
  51.0 0.8 copy-done.2
  51.8 1.0 copy-done.3
  52.9 4.7 %project.1 = (f32[32,32,128]{2,1,0:T(8,128)S(1)}, f32[32,32,128]{2,1,0:T(8,128)S(1)}) custom-call(s32[3]{0:T(128)S(1)} %pad_add_fusion.at, bf16[256,4096]{1,0:T(8,128)(2,1)} %saved.1, bf16[256,4096]{1,0:T(8,128)(2,1)} %layer.1, bf16[32,64,128]{2,1,0:T(8,128)(2,1)S(1)} %all-to-all-done.mine.rest_0_, ...), custom_call_target="tpu_custom_call" | custom-call | tf_op jit(solution)/shard_map/project/pallas_call | solution.py:303
  57.6 0.6 collective-permute-start.4
  58.2 1.2 collective-permute-done.4
  59.4 24.0 %all_to_all.15 = f16[32,32,128]{2,1,0:T(8,128)(2,1)S(1)} all-to-all(f16[32,32,128]{2,1,0:T(8,128)(2,1)S(1)} %add_convert_fusion), channel_id=1, replica_groups=mesh['fs_0'=8,'fs_1'=4,'fs_2'=2,'tp'=4] {'fs_0','fs_1'}, dimensions={0} | all-to-all | bytes 524288 | tf_op jit(solution)/shard_map/all_to_all | solution.py:313
  83.5 1.5 %spread.1 = f32[128,1,1152]{2,1,0:T(1,128)} custom-call(s32[3]{0:T(128)S(1)} %pad_add_fusion.at, f32[32,128]{1,0:T(8,128)S(1)} %convert_reduce_fusion.row), custom_call_target="tpu_custom_call" | custom-call | tf_op jit(solution)/shard_map/spread/pallas_call | solution.py:315
  85.0 6.2 %all-to-all-start.2 = ((f32[128,1,1152]{2,1,0:T(1,128)}), f32[128,1,1152]{2,1,0:T(1,128)S(1)}, u32[]{:S(2)}, u32[]{:S(2)}) async-start(f32[128,1,1152]{2,1,0:T(1,128)} %spread.1), calls=%async_computation.2 | async-start | bytes 1179648 | tf_op jit(solution)/shard_map/all_to_all | solution.py:323
  91.2 1.8 %collective-permute-start.8 = (bf16[32,64,128]{2,1,0:T(8,128)(2,1)S(1)}, bf16[32,64,128]{2,1,0:T(8,128)(2,1)}, u32[]{:S(2)}, u32[]{:S(2)}) collective-permute-start(bf16[32,64,128]{2,1,0:T(8,128)(2,1)S(1)} %all-to-all-done.mine.rest_0_), channel_id=1, source_target_pairs={{0,3},{1,0},{2,1},{3,2},{4,7},{5,4},{6,5},{7,6},{8,11},{9,8},{10,9... | collective-permute-start | bytes 1572872 | tf_op jit(solution)/shard_map/ppermute | solution.py:299
  92.9 0.6 collective-permute-start.7
  93.5 0.6 collective-permute-start.6
  94.1 21.9 %all-to-all-done.2.mine = f32[128,1,1152]{2,1,0:T(1,128)S(1)} async-done(((f32[128,1,1152]{2,1,0:T(1,128)}), f32[128,1,1152]{2,1,0:T(1,128)S(1)}, u32[]{:S(2)}, u32[]{:S(2)}) %all-to-all-start.2) | async-done | bytes 589856 | tf_op jit(solution)/shard_map/all_to_all | solution.py:323
  115.9 2.4 %collective-permute-start.5 = (f32[128,1,1152]{2,1,0:T(1,128)S(1)}, f32[128,1,1152]{2,1,0:T(1,128)S(1)}, u32[]{:S(2)}, u32[]{:S(2)}) collective-permute-start(f32[128,1,1152]{2,1,0:T(1,128)S(1)} %all-to-all-done.2.mine), channel_id=1, source_target_pairs={{0,4},{4,0},{1,5},{5,1},{2,6},{6,2},{3,7},{7,3},{8,12},{12,8},{9,1... | collective-permute-start | bytes 1769480 | tf_op jit(solution)/shard_map/ppermute | solution.py:221
  118.4 4.0 %collective-permute-start.11 = (bf16[32,64,128]{2,1,0:T(8,128)(2,1)}, bf16[32,64,128]{2,1,0:T(8,128)(2,1)S(1)}, u32[]{:S(2)}, u32[]{:S(2)}) collective-permute-start(bf16[32,64,128]{2,1,0:T(8,128)(2,1)} %collective-permute-done.8.rest_3_), channel_id=1, source_target_pairs={{0,4},{4,0},{1,5},{5,1},{2,6},{6,2},{3,7},{7,3},{8,12},{12,8},{9,1... | collective-permute-start | bytes 1572872 | tf_op jit(solution)/shard_map/ppermute | solution.py:221
  122.4 2.9 %collective-permute-done.6.rest_1_ = bf16[32,64,128]{2,1,0:T(8,128)(2,1)} collective-permute-done((bf16[32,64,128]{2,1,0:T(8,128)(2,1)S(1)}, bf16[32,64,128]{2,1,0:T(8,128)(2,1)}, u32[]{:S(2)}, u32[]{:S(2)}) %collective-permute-start.6) | collective-permute-done | bytes 524320 | tf_op jit(solution)/shard_map/ppermute | solution.py:299
  125.7 1.7 %update.1 = (f32[256,1024]{1,0:T(8,128)S(1)}, f32[8,128]{1,0:T(8,128)S(1)}, f32[4,512]{1,0:T(4,128)}, f32[4,512]{1,0:T(4,128)}, f32[4,512]{1,0:T(4,128)}, /*index=5*/f32[4,512]{1,0:T(4,128)}) custom-call(s32[3]{0:T(128)S(1)} %pad_add_fusion.at, f32[128,1,1152]{2,1,0:T(1,128)S(1)} %all-to-all-done.2.mine, f32[128,1,1152]{2,1,0:T(1,128)S(1)} %collective-permute-done.5.theirs, ...), custom_call_target="tpu_custom_call" | custom-call | tf_op jit(solution)/shard_map/update/pallas_call | solution.py:325
  127.5 11.3 %finish.1 = (f32[64,512]{1,0:T(8,128)}, f32[64,512]{1,0:T(8,128)}, f32[64,512]{1,0:T(8,128)}, f32[64,512]{1,0:T(8,128)}, bf16[4096,512]{1,0:T(8,128)(2,1)}, /*index=5*/bf16[4096,512]{1,0:T(8,128)(2,1)}) custom-call(s32[3]{0:T(128)S(1)} %pad_add_fusion.at, f32[8,128]{1,0:T(8,128)S(1)} %get-tuple-element.31.factor, f32[256,1024]{1,0:T(8,128)S(1)} %get-tuple-element.32.low, ...), custom_call_target="tpu_custom_call" | custom-call | tf_op jit(solution)/shard_map/finish/pallas_call | solution.py:231
  (25 shorter events, 1.2 us)
Async XLA Ops:
  7.2 120.3 %all-gather.3.cloned.1.call-start = ((), (), s32[]{:S(2)}) async-start(), calls=%async_computation.3 | async-start | bytes 10117120 | tf_op jit(solution)/shard_map/all_gather | solution.py:292
  9.8 28.8 %all-to-all-start = ((bf16[32,64,128]{2,1,0:T(8,128)(2,1)}), bf16[32,64,128]{2,1,0:T(8,128)(2,1)S(1)}, u32[]{:S(2)}, u32[]{:S(2)}) async-start(bf16[32,64,128]{2,1,0:T(8,128)(2,1)} %get-tuple-element.27), calls=%async_computation | async-start | bytes 1048576 | tf_op jit(solution)/shard_map/all_to_all | solution.py:295
  21.6 20.8 %collective-permute-start.3 = (bf16[256,1024]{1,0:T(8,128)(2,1)S(1)}, bf16[256,1024]{1,0:T(8,128)(2,1)S(1)}, u32[]{:S(2)}, u32[]{:S(2)}) collective-permute-start(bf16[256,1024]{1,0:T(8,128)(2,1)S(1)} %get-tuple-element.28.c0), channel_id=1, source_target_pairs={{0,3},{1,0},{2,1},{3,2},{4,7},{5,4},{6,5},{7,6},{8,11},{9,8},{10,9... | collective-permute-start | bytes 1572872 | tf_op jit(solution)/shard_map/ppermute | solution.py:293
  24.4 18.0 %collective-permute-start.2 = (bf16[256,1024]{1,0:T(8,128)(2,1)S(1)}, bf16[256,1024]{1,0:T(8,128)(2,1)S(1)}, u32[]{:S(2)}, u32[]{:S(2)}) collective-permute-start(bf16[256,1024]{1,0:T(8,128)(2,1)S(1)} %get-tuple-element.28.c0), channel_id=1, source_target_pairs={{0,2},{1,3},{2,0},{3,1},{4,6},{5,7},{6,4},{7,5},{8,10},{9,11},{10,... | collective-permute-start | bytes 1572872 | tf_op jit(solution)/shard_map/ppermute | solution.py:293
  24.8 26.2 %collective-permute-start.1 = (bf16[256,1024]{1,0:T(8,128)(2,1)S(1)}, bf16[256,1024]{1,0:T(8,128)(2,1)S(1)}, u32[]{:S(2)}, u32[]{:S(2)}) collective-permute-start(bf16[256,1024]{1,0:T(8,128)(2,1)S(1)} %get-tuple-element.28.c0), channel_id=1, source_target_pairs={{0,1},{1,2},{2,3},{3,0},{4,5},{5,6},{6,7},{7,4},{8,9},{9,10},{10,1... | collective-permute-start | bytes 1572872 | tf_op jit(solution)/shard_map/ppermute | solution.py:293
  38.6 55.0 %copy-start = (bf16[32,64,128]{2,1,0:T(8,128)(2,1)}, bf16[32,64,128]{2,1,0:T(8,128)(2,1)S(1)}, u32[]{:S(2)}) copy-start(bf16[32,64,128]{2,1,0:T(8,128)(2,1)S(1)} %all-to-all-done.mine.rest_0_) | copy-start | bytes 1572868
  38.6 13.3 %collective-permute-start = (bf16[32,64,128]{2,1,0:T(8,128)(2,1)S(1)}, bf16[32,64,128]{2,1,0:T(8,128)(2,1)S(1)}, u32[]{:S(2)}, u32[]{:S(2)}) collective-permute-start(bf16[32,64,128]{2,1,0:T(8,128)(2,1)S(1)} %all-to-all-done.mine.rest_0_), channel_id=1, source_target_pairs={{0,4},{4,0},{1,5},{5,1},{2,6},{6,2},{3,7},{7,3},{8,12},{12,8},{9,1... | collective-permute-start | bytes 1572872 | tf_op jit(solution)/shard_map/ppermute | solution.py:221
  51.0 0.8 copy-start.2
  51.8 1.0 copy-start.3
  52.9 6.6 %copy-start.1 = (bf16[32,64,128]{2,1,0:T(8,128)(2,1)}, bf16[32,64,128]{2,1,0:T(8,128)(2,1)S(1)}, u32[]{:S(2)}) copy-start(bf16[32,64,128]{2,1,0:T(8,128)(2,1)S(1)} %collective-permute-done.theirs.rest_4_) | copy-start | bytes 1572868
  57.6 1.7 %collective-permute-start.4 = (f16[32,32,128]{2,1,0:T(8,128)(2,1)S(1)}, f16[32,32,128]{2,1,0:T(8,128)(2,1)S(1)}, u32[]{:S(2)}, u32[]{:S(2)}) collective-permute-start(f16[32,32,128]{2,1,0:T(8,128)(2,1)S(1)} %convert_element_type.12), channel_id=1, source_target_pairs={{0,4},{4,0},{1,5},{5,1},{2,6},{6,2},{3,7},{7,3},{8,12},{12,8},{9,1... | collective-permute-start | bytes 786440 | tf_op jit(solution)/shard_map/ppermute | solution.py:221
  85.0 31.0 %all-to-all-start.2 = ((f32[128,1,1152]{2,1,0:T(1,128)}), f32[128,1,1152]{2,1,0:T(1,128)S(1)}, u32[]{:S(2)}, u32[]{:S(2)}) async-start(f32[128,1,1152]{2,1,0:T(1,128)} %spread.1), calls=%async_computation.2 | async-start | bytes 1179648 | tf_op jit(solution)/shard_map/all_to_all | solution.py:323
  91.2 27.2 %collective-permute-start.8 = (bf16[32,64,128]{2,1,0:T(8,128)(2,1)S(1)}, bf16[32,64,128]{2,1,0:T(8,128)(2,1)}, u32[]{:S(2)}, u32[]{:S(2)}) collective-permute-start(bf16[32,64,128]{2,1,0:T(8,128)(2,1)S(1)} %all-to-all-done.mine.rest_0_), channel_id=1, source_target_pairs={{0,3},{1,0},{2,1},{3,2},{4,7},{5,4},{6,5},{7,6},{8,11},{9,8},{10,9... | collective-permute-start | bytes 1572872 | tf_op jit(solution)/shard_map/ppermute | solution.py:299
  92.9 29.4 %collective-permute-start.7 = (bf16[32,64,128]{2,1,0:T(8,128)(2,1)S(1)}, bf16[32,64,128]{2,1,0:T(8,128)(2,1)}, u32[]{:S(2)}, u32[]{:S(2)}) collective-permute-start(bf16[32,64,128]{2,1,0:T(8,128)(2,1)S(1)} %all-to-all-done.mine.rest_0_), channel_id=1, source_target_pairs={{0,2},{1,3},{2,0},{3,1},{4,6},{5,7},{6,4},{7,5},{8,10},{9,11},{10,... | collective-permute-start | bytes 1572872 | tf_op jit(solution)/shard_map/ppermute | solution.py:299
  93.5 31.7 %collective-permute-start.6 = (bf16[32,64,128]{2,1,0:T(8,128)(2,1)S(1)}, bf16[32,64,128]{2,1,0:T(8,128)(2,1)}, u32[]{:S(2)}, u32[]{:S(2)}) collective-permute-start(bf16[32,64,128]{2,1,0:T(8,128)(2,1)S(1)} %all-to-all-done.mine.rest_0_), channel_id=1, source_target_pairs={{0,1},{1,2},{2,3},{3,0},{4,5},{5,6},{6,7},{7,4},{8,9},{9,10},{10,1... | collective-permute-start | bytes 1572872 | tf_op jit(solution)/shard_map/ppermute | solution.py:299
  115.9 9.8 %collective-permute-start.5 = (f32[128,1,1152]{2,1,0:T(1,128)S(1)}, f32[128,1,1152]{2,1,0:T(1,128)S(1)}, u32[]{:S(2)}, u32[]{:S(2)}) collective-permute-start(f32[128,1,1152]{2,1,0:T(1,128)S(1)} %all-to-all-done.2.mine), channel_id=1, source_target_pairs={{0,4},{4,0},{1,5},{5,1},{2,6},{6,2},{3,7},{7,3},{8,12},{12,8},{9,1... | collective-permute-start | bytes 1769480 | tf_op jit(solution)/shard_map/ppermute | solution.py:221
  118.4 9.1 %collective-permute-start.11 = (bf16[32,64,128]{2,1,0:T(8,128)(2,1)}, bf16[32,64,128]{2,1,0:T(8,128)(2,1)S(1)}, u32[]{:S(2)}, u32[]{:S(2)}) collective-permute-start(bf16[32,64,128]{2,1,0:T(8,128)(2,1)} %collective-permute-done.8.rest_3_), channel_id=1, source_target_pairs={{0,4},{4,0},{1,5},{5,1},{2,6},{6,2},{3,7},{7,3},{8,12},{12,8},{9,1... | collective-permute-start | bytes 1572872 | tf_op jit(solution)/shard_map/ppermute | solution.py:221
  122.4 5.1 %collective-permute-start.10 = (bf16[32,64,128]{2,1,0:T(8,128)(2,1)}, bf16[32,64,128]{2,1,0:T(8,128)(2,1)S(1)}, u32[]{:S(2)}, u32[]{:S(2)}) collective-permute-start(bf16[32,64,128]{2,1,0:T(8,128)(2,1)} %collective-permute-done.7.rest_2_), channel_id=1, source_target_pairs={{0,4},{4,0},{1,5},{5,1},{2,6},{6,2},{3,7},{7,3},{8,12},{12,8},{9,1... | collective-permute-start | bytes 1572872 | tf_op jit(solution)/shard_map/ppermute | solution.py:221
  125.2 2.3 %collective-permute-start.9 = (bf16[32,64,128]{2,1,0:T(8,128)(2,1)}, bf16[32,64,128]{2,1,0:T(8,128)(2,1)S(1)}, u32[]{:S(2)}, u32[]{:S(2)}) collective-permute-start(bf16[32,64,128]{2,1,0:T(8,128)(2,1)} %collective-permute-done.6.rest_1_), channel_id=1, source_target_pairs={{0,4},{4,0},{1,5},{5,1},{2,6},{6,2},{3,7},{7,3},{8,12},{12,8},{9,1... | collective-permute-start | bytes 1572872 | tf_op jit(solution)/shard_map/ppermute | solution.py:221
Sparse Core Ops, SparseCore 0:
  11.3 102.0 all-gather.2

commit v6 on v5

--- a/solution.py
+++ b/solution.py
@@ -195,7 +195,7 @@
     bases = []
     for k in range(4):
         chips = pl.ds(pl.program_id(0) * (GROUP // 2), GROUP // 2)
-        own, other = quarters[k][...], quarters[4][...] if k == 0 else quarters[4 + k][chips]
+        own, other = quarters[k][...], quarters[4 + k][chips]
         first = jnp.where(core == 0, own, other)
         second = jnp.where(core == 0, other, own)
         bases.append(jnp.concatenate([first, second], axis=1).reshape(GROUP * 64, 128))
@@ -242,8 +242,8 @@
             pl.BlockSpec((64, 16, 512), lambda i: (0, MOMENTS_AT // 16, 0)),
             pl.BlockSpec(memory_space=pl.ANY),
             pl.BlockSpec((64, 8, 512), lambda i: (0, TOPS_AT // 8, 0)),
-            *[pl.BlockSpec((GROUP // 2, 64, 128), lambda i: (i, 0, 0))] * 5,
-            *[VMEM] * 3,
+            *[pl.BlockSpec((GROUP // 2, 64, 128), lambda i: (i, 0, 0))] * 4,
+            *[VMEM] * 4,
         ],
         out_specs=[local] * 4 + [pl.BlockSpec((GROUP * 64, 512), lambda i: (i, 0))] * 2,
         out_shape=[shape((64, 512), f32)] * 4 + [shape((D, 512), bf16)] * 2,
@@ -255,8 +255,8 @@
         at,
         *near(factor, low),
         *far(query_basis, output_basis, query_master, output_master, gathered, gathered, gathered),
-        *far(*quarters[:5]),
-        *near(*quarters[5:]),
+        *far(*quarters[:4]),
+        *near(*quarters[4:]),
     )
 
 

time: 146 us -> 148 us (1.014)
  local copies, waits for them, and re-layouts: 1.84 us -> 3.67 us
    unnamed x8 -> x10, local copies, waits for them, and re-layouts: 1.84 us -> 3.67 us
where the time goes in v6:
time: 148 us; the launch traced here: 147 us
  waiting for transfers between devices  47.6 us (32%)
  starting transfers between devices  36.2 us (24%)
  blocking collectives  24 us (16%)
  Pallas kernels  21.5 us (15%)
  between operations  14.1 us (10%)
  local copies, waits for them, and re-layouts  3.67 us (2%)
    all_to_all x1, blocking collectives, per_device(): arrived = lax.all_to_all(pair, CHIPS, 0, 0, tiled=True)  24 us
    all_to_all x1, waiting for transfers between devices, per_device(): mine = lax.all_to_all(out, (*CHIPS, 'tp'), 0, 0, tiled=True)  21.9 us
    all_to_all x1, waiting for transfers between devices, per_device(): mine = lax.all_to_all(send, CHIPS, 0, 0, tiled=True)  13.1 us
    all_to_all x1, starting transfers between devices, per_device(): mine = lax.all_to_all(send, CHIPS, 0, 0, tiled=True)  11.9 us
    ppermute x6, starting transfers between devices, swapped(): return lax.ppermute(values, 'fs_2', [(0, 1), (1, 0)])  11.4 us
    pallas_call x1, Pallas kernels, finished(): pl.pallas_call(finish_kernel, grid=(64 // GROUP,), in_specs=[SMEM, whole(...  11.2 us
    ppermute x3, waiting for transfers between devices, per_device(): lax.ppermute(cot, 'tp', [(i, (i + k) % 4) for i in range(4)])  8.62 us
    all_to_all x1, starting transfers between devices, per_device(): mine = lax.all_to_all(out, (*CHIPS, 'tp'), 0, 0, tiled=True)  6.18 us
  transfers between devices with their start and end apart: 15, of which 5 were waited for; matrix products, arithmetic and copies ran while one was open for 0% of the time, Pallas kernels for 5%

profile of v6, /device:TPU:1, one launch (start us, length us, event | category | flops | bytes accessed | tf_op | source)
XLA Modules:
  0.0 147.4 jit_solution(824323054306706965)
XLA Ops:
  7.3 2.4 %pack.1 = (bf16[152,512]{1,0:T(8,128)(2,1)}, bf16[32,64,128]{2,1,0:T(8,128)(2,1)}, bf16[256,1024]{1,0:T(8,128)(2,1)S(1)}) custom-call(s32[3]{0:T(128)S(1)} %pad_add_fusion.at, bf16[64,256]{1,0:T(8,128)(2,1)} %qb.3, bf16[64,256]{1,0:T(8,128)(2,1)} %ob.3, f32[64,512]{1,0:T(8,128)} %qm.3, f32[64,512]{1,0:T(8,128)} %om.3, f32[4,512]{1,0:T(4,128)} %q1.3, ...), custom_call_target="tpu_custom_call" | custom-call | tf_op jit(solution)/shard_map/pack/pallas_call | solution.py:280
  9.8 11.9 %all-to-all-start = ((bf16[32,64,128]{2,1,0:T(8,128)(2,1)}), bf16[32,64,128]{2,1,0:T(8,128)(2,1)S(1)}, u32[]{:S(2)}, u32[]{:S(2)}) async-start(bf16[32,64,128]{2,1,0:T(8,128)(2,1)} %get-tuple-element.27), calls=%async_computation | async-start | bytes 1048576 | tf_op jit(solution)/shard_map/all_to_all | solution.py:295
  21.6 2.8 %collective-permute-start.3 = (bf16[256,1024]{1,0:T(8,128)(2,1)S(1)}, bf16[256,1024]{1,0:T(8,128)(2,1)S(1)}, u32[]{:S(2)}, u32[]{:S(2)}) collective-permute-start(bf16[256,1024]{1,0:T(8,128)(2,1)S(1)} %get-tuple-element.28.c0), channel_id=1, source_target_pairs={{0,3},{1,0},{2,1},{3,2},{4,7},{5,4},{6,5},{7,6},{8,11},{9,8},{10,9... | collective-permute-start | bytes 1572872 | tf_op jit(solution)/shard_map/ppermute | solution.py:293
  24.8 0.7 collective-permute-start.1
  25.5 13.1 %all-to-all-done.mine.rest_0_ = bf16[32,64,128]{2,1,0:T(8,128)(2,1)S(1)} async-done(((bf16[32,64,128]{2,1,0:T(8,128)(2,1)}), bf16[32,64,128]{2,1,0:T(8,128)(2,1)S(1)}, u32[]{:S(2)}, u32[]{:S(2)}) %all-to-all-start) | async-done | bytes 524320 | tf_op jit(solution)/shard_map/all_to_all | solution.py:295
  38.6 3.9 %collective-permute-start = (bf16[32,64,128]{2,1,0:T(8,128)(2,1)S(1)}, bf16[32,64,128]{2,1,0:T(8,128)(2,1)S(1)}, u32[]{:S(2)}, u32[]{:S(2)}) collective-permute-start(bf16[32,64,128]{2,1,0:T(8,128)(2,1)S(1)} %all-to-all-done.mine.rest_0_), channel_id=1, source_target_pairs={{0,4},{4,0},{1,5},{5,1},{2,6},{6,2},{3,7},{7,3},{8,12},{12,8},{9,1... | collective-permute-start | bytes 1572872 | tf_op jit(solution)/shard_map/ppermute | solution.py:221
  42.4 8.6 %collective-permute-done.1.c1 = bf16[256,1024]{1,0:T(8,128)(2,1)S(1)} collective-permute-done((bf16[256,1024]{1,0:T(8,128)(2,1)S(1)}, bf16[256,1024]{1,0:T(8,128)(2,1)S(1)}, u32[]{:S(2)}, u32[]{:S(2)}) %collective-permute-start.1) | collective-permute-done | bytes 524320 | tf_op jit(solution)/shard_map/ppermute | solution.py:293
  51.0 0.8 copy-done.3
  51.8 1.0 copy-done.4
  52.9 4.7 %project.1 = (f32[32,32,128]{2,1,0:T(8,128)S(1)}, f32[32,32,128]{2,1,0:T(8,128)S(1)}) custom-call(s32[3]{0:T(128)S(1)} %pad_add_fusion.at, bf16[256,4096]{1,0:T(8,128)(2,1)} %saved.1, bf16[256,4096]{1,0:T(8,128)(2,1)} %layer.1, bf16[32,64,128]{2,1,0:T(8,128)(2,1)S(1)} %all-to-all-done.mine.rest_0_, ...), custom_call_target="tpu_custom_call" | custom-call | tf_op jit(solution)/shard_map/project/pallas_call | solution.py:303
  57.6 0.6 collective-permute-start.4
  58.2 1.2 collective-permute-done.4
  59.4 24.0 %all_to_all.15 = f16[32,32,128]{2,1,0:T(8,128)(2,1)S(1)} all-to-all(f16[32,32,128]{2,1,0:T(8,128)(2,1)S(1)} %add_convert_fusion), channel_id=1, replica_groups=mesh['fs_0'=8,'fs_1'=4,'fs_2'=2,'tp'=4] {'fs_0','fs_1'}, dimensions={0} | all-to-all | bytes 524288 | tf_op jit(solution)/shard_map/all_to_all | solution.py:313
  83.5 1.5 %spread.1 = f32[128,1,1152]{2,1,0:T(1,128)} custom-call(s32[3]{0:T(128)S(1)} %pad_add_fusion.at, f32[32,128]{1,0:T(8,128)S(1)} %convert_reduce_fusion.row), custom_call_target="tpu_custom_call" | custom-call | tf_op jit(solution)/shard_map/spread/pallas_call | solution.py:315
  85.0 6.2 %all-to-all-start.2 = ((f32[128,1,1152]{2,1,0:T(1,128)}), f32[128,1,1152]{2,1,0:T(1,128)S(1)}, u32[]{:S(2)}, u32[]{:S(2)}) async-start(f32[128,1,1152]{2,1,0:T(1,128)} %spread.1), calls=%async_computation.2 | async-start | bytes 1179648 | tf_op jit(solution)/shard_map/all_to_all | solution.py:323
  91.2 1.8 %collective-permute-start.8 = (bf16[32,64,128]{2,1,0:T(8,128)(2,1)S(1)}, bf16[32,64,128]{2,1,0:T(8,128)(2,1)}, u32[]{:S(2)}, u32[]{:S(2)}) collective-permute-start(bf16[32,64,128]{2,1,0:T(8,128)(2,1)S(1)} %all-to-all-done.mine.rest_0_), channel_id=1, source_target_pairs={{0,3},{1,0},{2,1},{3,2},{4,7},{5,4},{6,5},{7,6},{8,11},{9,8},{10,9... | collective-permute-start | bytes 1572872 | tf_op jit(solution)/shard_map/ppermute | solution.py:299
  94.1 21.9 %all-to-all-done.2.mine = f32[128,1,1152]{2,1,0:T(1,128)S(1)} async-done(((f32[128,1,1152]{2,1,0:T(1,128)}), f32[128,1,1152]{2,1,0:T(1,128)S(1)}, u32[]{:S(2)}, u32[]{:S(2)}) %all-to-all-start.2) | async-done | bytes 589856 | tf_op jit(solution)/shard_map/all_to_all | solution.py:323
  115.9 2.5 %collective-permute-start.5 = (f32[128,1,1152]{2,1,0:T(1,128)S(1)}, f32[128,1,1152]{2,1,0:T(1,128)S(1)}, u32[]{:S(2)}, u32[]{:S(2)}) collective-permute-start(f32[128,1,1152]{2,1,0:T(1,128)S(1)} %all-to-all-done.2.mine), channel_id=1, source_target_pairs={{0,4},{4,0},{1,5},{5,1},{2,6},{6,2},{3,7},{7,3},{8,12},{12,8},{9,1... | collective-permute-start | bytes 1769480 | tf_op jit(solution)/shard_map/ppermute | solution.py:221
  118.4 3.9 %collective-permute-start.11 = (bf16[32,64,128]{2,1,0:T(8,128)(2,1)}, bf16[32,64,128]{2,1,0:T(8,128)(2,1)S(1)}, u32[]{:S(2)}, u32[]{:S(2)}) collective-permute-start(bf16[32,64,128]{2,1,0:T(8,128)(2,1)} %collective-permute-done.8.rest_3_), channel_id=1, source_target_pairs={{0,4},{4,0},{1,5},{5,1},{2,6},{6,2},{3,7},{7,3},{8,12},{12,8},{9,1... | collective-permute-start | bytes 1572872 | tf_op jit(solution)/shard_map/ppermute | solution.py:221
  122.4 2.9 %collective-permute-done.6.rest_1_ = bf16[32,64,128]{2,1,0:T(8,128)(2,1)} collective-permute-done((bf16[32,64,128]{2,1,0:T(8,128)(2,1)S(1)}, bf16[32,64,128]{2,1,0:T(8,128)(2,1)}, u32[]{:S(2)}, u32[]{:S(2)}) %collective-permute-start.6) | collective-permute-done | bytes 524320 | tf_op jit(solution)/shard_map/ppermute | solution.py:299
  125.7 1.7 %update.1 = (f32[256,1024]{1,0:T(8,128)S(1)}, f32[8,128]{1,0:T(8,128)S(1)}, f32[4,512]{1,0:T(4,128)}, f32[4,512]{1,0:T(4,128)}, f32[4,512]{1,0:T(4,128)}, /*index=5*/f32[4,512]{1,0:T(4,128)}) custom-call(s32[3]{0:T(128)S(1)} %pad_add_fusion.at, f32[128,1,1152]{2,1,0:T(1,128)S(1)} %all-to-all-done.2.mine, f32[128,1,1152]{2,1,0:T(1,128)S(1)} %collective-permute-done.5.theirs, ...), custom_call_target="tpu_custom_call" | custom-call | tf_op jit(solution)/shard_map/update/pallas_call | solution.py:325
  127.5 0.8 copy-done.1
  128.3 1.0 copy-done.2
  129.3 11.2 %finish.1 = (f32[64,512]{1,0:T(8,128)}, f32[64,512]{1,0:T(8,128)}, f32[64,512]{1,0:T(8,128)}, f32[64,512]{1,0:T(8,128)}, bf16[4096,512]{1,0:T(8,128)(2,1)}, /*index=5*/bf16[4096,512]{1,0:T(8,128)(2,1)}) custom-call(s32[3]{0:T(128)S(1)} %pad_add_fusion.at, f32[8,128]{1,0:T(8,128)S(1)} %get-tuple-element.31.factor, f32[256,1024]{1,0:T(8,128)S(1)} %get-tuple-element.32.low, ...), custom_call_target="tpu_custom_call" | custom-call | tf_op jit(solution)/shard_map/finish/pallas_call | solution.py:231
  (27 shorter events, 2.4 us)
Async XLA Ops:
  7.2 121.1 %all-gather.3.cloned.1.call-start = ((), (), s32[]{:S(2)}) async-start(), calls=%async_computation.3 | async-start | bytes 10117120 | tf_op jit(solution)/shard_map/all_gather | solution.py:292
  9.8 28.8 %all-to-all-start = ((bf16[32,64,128]{2,1,0:T(8,128)(2,1)}), bf16[32,64,128]{2,1,0:T(8,128)(2,1)S(1)}, u32[]{:S(2)}, u32[]{:S(2)}) async-start(bf16[32,64,128]{2,1,0:T(8,128)(2,1)} %get-tuple-element.27), calls=%async_computation | async-start | bytes 1048576 | tf_op jit(solution)/shard_map/all_to_all | solution.py:295
  21.6 20.8 %collective-permute-start.3 = (bf16[256,1024]{1,0:T(8,128)(2,1)S(1)}, bf16[256,1024]{1,0:T(8,128)(2,1)S(1)}, u32[]{:S(2)}, u32[]{:S(2)}) collective-permute-start(bf16[256,1024]{1,0:T(8,128)(2,1)S(1)} %get-tuple-element.28.c0), channel_id=1, source_target_pairs={{0,3},{1,0},{2,1},{3,2},{4,7},{5,4},{6,5},{7,6},{8,11},{9,8},{10,9... | collective-permute-start | bytes 1572872 | tf_op jit(solution)/shard_map/ppermute | solution.py:293
  24.4 18.0 %collective-permute-start.2 = (bf16[256,1024]{1,0:T(8,128)(2,1)S(1)}, bf16[256,1024]{1,0:T(8,128)(2,1)S(1)}, u32[]{:S(2)}, u32[]{:S(2)}) collective-permute-start(bf16[256,1024]{1,0:T(8,128)(2,1)S(1)} %get-tuple-element.28.c0), channel_id=1, source_target_pairs={{0,2},{1,3},{2,0},{3,1},{4,6},{5,7},{6,4},{7,5},{8,10},{9,11},{10,... | collective-permute-start | bytes 1572872 | tf_op jit(solution)/shard_map/ppermute | solution.py:293
  24.8 26.2 %collective-permute-start.1 = (bf16[256,1024]{1,0:T(8,128)(2,1)S(1)}, bf16[256,1024]{1,0:T(8,128)(2,1)S(1)}, u32[]{:S(2)}, u32[]{:S(2)}) collective-permute-start(bf16[256,1024]{1,0:T(8,128)(2,1)S(1)} %get-tuple-element.28.c0), channel_id=1, source_target_pairs={{0,1},{1,2},{2,3},{3,0},{4,5},{5,6},{6,7},{7,4},{8,9},{9,10},{10,1... | collective-permute-start | bytes 1572872 | tf_op jit(solution)/shard_map/ppermute | solution.py:293
  38.6 54.9 %copy-start = (bf16[32,64,128]{2,1,0:T(8,128)(2,1)}, bf16[32,64,128]{2,1,0:T(8,128)(2,1)S(1)}, u32[]{:S(2)}) copy-start(bf16[32,64,128]{2,1,0:T(8,128)(2,1)S(1)} %all-to-all-done.mine.rest_0_) | copy-start | bytes 1572868
  38.6 13.3 %collective-permute-start = (bf16[32,64,128]{2,1,0:T(8,128)(2,1)S(1)}, bf16[32,64,128]{2,1,0:T(8,128)(2,1)S(1)}, u32[]{:S(2)}, u32[]{:S(2)}) collective-permute-start(bf16[32,64,128]{2,1,0:T(8,128)(2,1)S(1)} %all-to-all-done.mine.rest_0_), channel_id=1, source_target_pairs={{0,4},{4,0},{1,5},{5,1},{2,6},{6,2},{3,7},{7,3},{8,12},{12,8},{9,1... | collective-permute-start | bytes 1572872 | tf_op jit(solution)/shard_map/ppermute | solution.py:221
  51.0 0.8 copy-start.3
  51.8 1.0 copy-start.4
  57.6 1.7 %collective-permute-start.4 = (f16[32,32,128]{2,1,0:T(8,128)(2,1)S(1)}, f16[32,32,128]{2,1,0:T(8,128)(2,1)S(1)}, u32[]{:S(2)}, u32[]{:S(2)}) collective-permute-start(f16[32,32,128]{2,1,0:T(8,128)(2,1)S(1)} %convert_element_type.12), channel_id=1, source_target_pairs={{0,4},{4,0},{1,5},{5,1},{2,6},{6,2},{3,7},{7,3},{8,12},{12,8},{9,1... | collective-permute-start | bytes 786440 | tf_op jit(solution)/shard_map/ppermute | solution.py:221
  85.0 31.0 %all-to-all-start.2 = ((f32[128,1,1152]{2,1,0:T(1,128)}), f32[128,1,1152]{2,1,0:T(1,128)S(1)}, u32[]{:S(2)}, u32[]{:S(2)}) async-start(f32[128,1,1152]{2,1,0:T(1,128)} %spread.1), calls=%async_computation.2 | async-start | bytes 1179648 | tf_op jit(solution)/shard_map/all_to_all | solution.py:323
  91.2 27.2 %collective-permute-start.8 = (bf16[32,64,128]{2,1,0:T(8,128)(2,1)S(1)}, bf16[32,64,128]{2,1,0:T(8,128)(2,1)}, u32[]{:S(2)}, u32[]{:S(2)}) collective-permute-start(bf16[32,64,128]{2,1,0:T(8,128)(2,1)S(1)} %all-to-all-done.mine.rest_0_), channel_id=1, source_target_pairs={{0,3},{1,0},{2,1},{3,2},{4,7},{5,4},{6,5},{7,6},{8,11},{9,8},{10,9... | collective-permute-start | bytes 1572872 | tf_op jit(solution)/shard_map/ppermute | solution.py:299
  92.9 29.4 %collective-permute-start.7 = (bf16[32,64,128]{2,1,0:T(8,128)(2,1)S(1)}, bf16[32,64,128]{2,1,0:T(8,128)(2,1)}, u32[]{:S(2)}, u32[]{:S(2)}) collective-permute-start(bf16[32,64,128]{2,1,0:T(8,128)(2,1)S(1)} %all-to-all-done.mine.rest_0_), channel_id=1, source_target_pairs={{0,2},{1,3},{2,0},{3,1},{4,6},{5,7},{6,4},{7,5},{8,10},{9,11},{10,... | collective-permute-start | bytes 1572872 | tf_op jit(solution)/shard_map/ppermute | solution.py:299
  93.5 31.7 %collective-permute-start.6 = (bf16[32,64,128]{2,1,0:T(8,128)(2,1)S(1)}, bf16[32,64,128]{2,1,0:T(8,128)(2,1)}, u32[]{:S(2)}, u32[]{:S(2)}) collective-permute-start(bf16[32,64,128]{2,1,0:T(8,128)(2,1)S(1)} %all-to-all-done.mine.rest_0_), channel_id=1, source_target_pairs={{0,1},{1,2},{2,3},{3,0},{4,5},{5,6},{6,7},{7,4},{8,9},{9,10},{10,1... | collective-permute-start | bytes 1572872 | tf_op jit(solution)/shard_map/ppermute | solution.py:299
  115.9 9.8 %collective-permute-start.5 = (f32[128,1,1152]{2,1,0:T(1,128)S(1)}, f32[128,1,1152]{2,1,0:T(1,128)S(1)}, u32[]{:S(2)}, u32[]{:S(2)}) collective-permute-start(f32[128,1,1152]{2,1,0:T(1,128)S(1)} %all-to-all-done.2.mine), channel_id=1, source_target_pairs={{0,4},{4,0},{1,5},{5,1},{2,6},{6,2},{3,7},{7,3},{8,12},{12,8},{9,1... | collective-permute-start | bytes 1769480 | tf_op jit(solution)/shard_map/ppermute | solution.py:221
  118.4 9.0 %collective-permute-start.11 = (bf16[32,64,128]{2,1,0:T(8,128)(2,1)}, bf16[32,64,128]{2,1,0:T(8,128)(2,1)S(1)}, u32[]{:S(2)}, u32[]{:S(2)}) collective-permute-start(bf16[32,64,128]{2,1,0:T(8,128)(2,1)} %collective-permute-done.8.rest_3_), channel_id=1, source_target_pairs={{0,4},{4,0},{1,5},{5,1},{2,6},{6,2},{3,7},{7,3},{8,12},{12,8},{9,1... | collective-permute-start | bytes 1572872 | tf_op jit(solution)/shard_map/ppermute | solution.py:221
  122.4 5.1 %collective-permute-start.10 = (bf16[32,64,128]{2,1,0:T(8,128)(2,1)}, bf16[32,64,128]{2,1,0:T(8,128)(2,1)S(1)}, u32[]{:S(2)}, u32[]{:S(2)}) collective-permute-start(bf16[32,64,128]{2,1,0:T(8,128)(2,1)} %collective-permute-done.7.rest_2_), channel_id=1, source_target_pairs={{0,4},{4,0},{1,5},{5,1},{2,6},{6,2},{3,7},{7,3},{8,12},{12,8},{9,1... | collective-permute-start | bytes 1572872 | tf_op jit(solution)/shard_map/ppermute | solution.py:221
  125.2 3.0 %collective-permute-start.9 = (bf16[32,64,128]{2,1,0:T(8,128)(2,1)}, bf16[32,64,128]{2,1,0:T(8,128)(2,1)S(1)}, u32[]{:S(2)}, u32[]{:S(2)}) collective-permute-start(bf16[32,64,128]{2,1,0:T(8,128)(2,1)} %collective-permute-done.6.rest_1_), channel_id=1, source_target_pairs={{0,4},{4,0},{1,5},{5,1},{2,6},{6,2},{3,7},{7,3},{8,12},{12,8},{9,1... | collective-permute-start | bytes 1572872 | tf_op jit(solution)/shard_map/ppermute | solution.py:221
  127.5 0.8 copy-start.1
  128.3 1.0 copy-start.2
Sparse Core Ops, SparseCore 0:
  11.3 102.0 all-gather.2
